TPU v7x, 256 devices: a whole 4x4x8 slice. The times are simulated.
256 devices in a mesh: sp: 32 (over z, y), tp: 8 (over x, core).
Axes of the slice: x: 4, y: 4, z: 8, core: 2. Of those that a mesh axis runs over, the one named last changes fastest.
Arguments:
- residual_in: bfloat16 [12288, 2048], P(('sp', 'tp')), may hold values from -6 to 6
- queries: bfloat16 [12288, 2048], P('sp', 'tp'), may hold values from -180 to 180
- keys: bfloat16 [12288, 2048], P('sp', 'tp'), may hold values from -9 to 9
- values: bfloat16 [12288, 2048], P('sp', 'tp'), may hold values from -6 to 6
- mix_lambda: float32 [16], P('tp'), may hold values from 0.3 to 0.8
- head_gain: float32 [128], replicated, may hold values from 0.1 to 1.9
- out_weight: bfloat16 [2048, 2048], P('tp'), may hold values from -0.125 to 0.125
- norm_gain: float32 [2048], replicated, may hold values from 0.1 to 1.9
- gate_weight: bfloat16 [2048, 5632], P('sp', 'tp'), may hold values from -0.125 to 0.125
- up_weight: bfloat16 [2048, 5632], P('sp', 'tp'), may hold values from -0.125 to 0.125
- down_weight: bfloat16 [5632, 2048], P('tp', 'sp'), may hold values from -0.078125 to 0.078125
Outputs:
- layer_out: bfloat16 [12288, 2048], P(('sp', 'tp'))
All inputs are finite; a program needn't handle non-finite values.
Results may differ from a plain program's by a relative error of at most 0.014.
Values may be sent and summed in bfloat16 or wider, within the bound.
No kernel may reach another device: no remote copies, remote signals or barrier semaphores. Data moves between devices by JAX's collectives and lax.ppermute only.
A program may use at most 128 MiB of HBM per device.

v0:
```python
import math

import jax
import jax.numpy as jnp
from jax import lax
from jax.sharding import PartitionSpec as P

DH = 64
VD = 128


def cut_along(value, dim, devices):
    shape = value.shape
    parts = value.reshape(*shape[:dim], devices, shape[dim] // devices, *shape[dim + 1 :])
    return jnp.moveaxis(parts, dim, 0)


def sent_and_summed(value, axis, dim):
    parts = cut_along(value, dim, lax.axis_size(axis))
    arrived = lax.all_to_all(parts, axis, split_axis=0, concat_axis=0, tiled=True)
    return arrived.astype(jnp.float32).sum(axis=0)


def sent_to_all(value, axis):
    copies = jnp.broadcast_to(value, (lax.axis_size(axis), *value.shape))
    return lax.all_to_all(copies, axis, split_axis=0, concat_axis=0, tiled=True)


def joined_along(parts, dim):
    shape = list(parts.shape[1:])
    shape[dim] *= parts.shape[0]
    return jnp.moveaxis(parts, 0, dim).reshape(shape)


def collect(value, axis, dim):
    parts = sent_to_all(value, axis)
    return joined_along(parts, dim)


def rows_first(arrays, axis, dims):
    turned = [jnp.moveaxis(a, dim, 0) for a, dim in zip(arrays, dims)]
    widths = [t[0].size for t in turned]
    both = jnp.concatenate([t.reshape(-1, w) for t, w in zip(turned, widths)], axis=1)
    result = lax.all_gather(both, axis, axis=0, tiled=True)
    parts = jnp.split(result, [sum(widths[:k]) for k in range(1, len(widths))], axis=1)
    return tuple(
        (
            jnp.moveaxis(b.reshape(-1, *t.shape[1:]), 0, dim)
            for b, t, dim in zip(parts, turned, dims)
        )
    )


def body(
    residual_in,
    queries,
    keys,
    values,
    mix_lambda,
    head_gain,
    out_weight,
    norm_gain,
    gate_weight,
    up_weight,
    down_weight,
):
    tok_local = queries.shape[0]
    heads_local = mix_lambda.shape[0]
    query_four = queries.reshape(tok_local, heads_local, 2, DH)
    inverse_root = 1.0 / math.sqrt(DH)

    def one_block(state, block):
        top, total, weighted = state
        key_block, value_block = block
        scores = (
            jnp.einsum("qhcd,khcd->hcqk", query_four, key_block, preferred_element_type=jnp.float32)
            * inverse_root
        )
        new_top = jnp.maximum(top, jnp.max(scores, axis=-1))
        rescale = jnp.exp(top - new_top)
        expo = jnp.exp(scores - new_top[..., None])
        total = total * rescale + jnp.sum(expo, axis=-1)
        weighted = weighted * rescale[..., None] + jnp.einsum(
            "hcqk,khe->hcqe",
            expo.astype(jnp.bfloat16),
            value_block,
            preferred_element_type=jnp.float32,
        )
        return ((new_top, total, weighted), None)

    start_state = (
        jnp.full((heads_local, 2, tok_local), -1e30, jnp.float32),
        jnp.zeros((heads_local, 2, tok_local), jnp.float32),
        jnp.zeros((heads_local, 2, tok_local, VD), jnp.float32),
    )
    key_piece = lax.all_gather(keys, "sp", axis=0, tiled=True)
    value_piece = lax.all_gather(values, "sp", axis=0, tiled=True)
    count = key_piece.shape[0]
    shards = max(count // tok_local, 1)
    unit = count // shards
    group = max(
        (g for g in range(1, shards + 1) if shards % g == 0 and g * unit <= max(1536, unit))
    )
    width = group * unit
    blocks = count // width
    key_blocks = key_piece.reshape(blocks, width, heads_local, 2, DH)
    value_blocks = value_piece.reshape(blocks, width, heads_local, VD)
    state, unused = lax.scan(one_block, start_state, (key_blocks, value_blocks))
    top, total, weighted = state
    maps = weighted / total[..., None]
    mixed = maps[:, 0] - mix_lambda[:, None, None] * maps[:, 1]
    head_scale = lax.rsqrt(jnp.mean(mixed * mixed, axis=-1, keepdims=True) + 1e-06)
    head_out = (mixed * head_scale * head_gain).astype(jnp.bfloat16)
    attended = jnp.transpose(head_out, (1, 0, 2)).reshape(tok_local, heads_local * VD)
    picked = attended
    projected = sent_and_summed(
        jnp.dot(picked, out_weight, preferred_element_type=jnp.float32).astype(jnp.bfloat16),
        "tp",
        0,
    )
    after_mix = residual_in.astype(jnp.float32) + projected
    row_scale = lax.rsqrt(jnp.mean(after_mix * after_mix, axis=-1, keepdims=True) + 1e-06)
    normed = (after_mix * row_scale * norm_gain).astype(jnp.bfloat16)
    all_rows = collect(normed, "tp", 0)
    gate_all, up_all, down_all = rows_first((gate_weight, up_weight, down_weight), "sp", (0, 0, 1))
    gate = jnp.dot(all_rows, gate_all, preferred_element_type=jnp.float32)
    up = jnp.dot(all_rows, up_all, preferred_element_type=jnp.float32)
    hidden = (jax.nn.silu(gate) * up).astype(jnp.bfloat16)
    picked = hidden
    mixer = sent_and_summed(
        jnp.dot(picked, down_all, preferred_element_type=jnp.float32).astype(jnp.bfloat16), "tp", 0
    )
    return (after_mix + 0.5 * mixer).astype(jnp.bfloat16)


def solution(mesh):
    return jax.shard_map(
        body,
        mesh=mesh,
        in_specs=(
            P(("sp", "tp"), None),
            P("sp", "tp"),
            P("sp", "tp"),
            P("sp", "tp"),
            P("tp"),
            P(),
            P("tp", None),
            P(),
            P("sp", "tp"),
            P("sp", "tp"),
            P("tp", "sp"),
        ),
        out_specs=P(("sp", "tp"), None),
        check_vma=False,
    )
```

profile of v0, /device:TPU:8, one launch (start us, length us, event | category | flops | bytes accessed | tf_op | source)
XLA Modules:
  0.0 423.4 jit_solution(3736161622382868444)
XLA Ops:
  6.5 0.7 all-gather.4.cloned.1.call-update
  7.3 0.0 all-gather.6.cloned.1.call-start
  7.3 0.7 all-gather.6.cloned.1.call-update
  8.0 0.0 all-gather.8.cloned.1.call-start
  8.1 1.9 concatenate.3
  9.9 0.0 all-gather.8.cloned.1.call-update
  10.0 1.1 copy.17
  11.1 88.7 %all-gather.4.cloned.1.call-done = bf16[12288,256]{1,0:T(8,128)(2,1)} async-done(((bf16[384,256]{1,0:T(8,128)(2,1)}), bf16[12288,256]{1,0:T(8,128)(2,1)}) %all-gather.4.cloned.1.call-update) | async-done | bytes 6291472 | tf_op jit(solution)/shard_map/all_gather | solution.py:96
  99.8 21.8 %reshape.51 = bf16[8,1536,2,2,64]{4,3,2,1,0:T(2,128)(2,1)} reshape(bf16[12288,256]{1,0:T(8,128)(2,1)} %all-gather.4.cloned.1.call-done) | data formatting | bytes 12582912 | tf_op jit(solution)/shard_map/reshape | solution.py:106
  121.6 29.8 %copy.19 = bf16[8,1536,2,2,64]{1,4,3,2,0:T(8,128)(2,1)} copy(bf16[8,1536,2,2,64]{4,3,2,1,0:T(2,128)(2,1)} %reshape.51) | data formatting | bytes 12582912
  151.3 36.1 %all-gather.6.cloned.1.call-done = bf16[12288,256]{1,0:T(8,128)(2,1)} async-done(((bf16[384,256]{1,0:T(8,128)(2,1)}), bf16[12288,256]{1,0:T(8,128)(2,1)}) %all-gather.6.cloned.1.call-update) | async-done | bytes 6291472 | tf_op jit(solution)/shard_map/all_gather | solution.py:97
  187.5 9.7 %reshape.52 = bf16[8,1536,2,128]{3,2,1,0:T(2,128)(2,1)} reshape(bf16[12288,256]{1,0:T(8,128)(2,1)} %all-gather.6.cloned.1.call-done) | data formatting | bytes 12582912 | tf_op jit(solution)/shard_map/reshape | solution.py:107
  197.2 128.2 %while.15 = (s32[]{:T(128)}, f32[2,2,384]{2,1,0:T(2,128)S(1)}, f32[2,2,384]{2,1,0:T(2,128)S(1)}, f32[2,2,384,128]{3,2,1,0:T(8,128)S(1)}, bf16[8,1536,2,2,64]{1,4...) while((s32[]{:T(128)}, f32[2,2,384]{2,1,0:T(2,128)S(1)}, ...), condition=%wide.region_3.4_spmd.clone, body=%wide.region_0.3_spmd.clone.sunk | while | flops 925441536 | bytes 71074440 | solution.py:108
  197.2 6.2 %bitcast_reduce_fusion.2 = (f32[2,2,384]{2,1,0:T(2,128)S(1)}, f32[2,2,1536,384]{3,2,1,0:T(8,128)}) fusion(bf16[384,2,2,64]{0,3,2,1:T(8,128)(2,1)S(1)} %get-tuple-element.168, bf16[8,1536,2,2,64]{1,4,3,2,0:T(8,128)(2,1)} %get-tuple-element.167, s32[]{:T(128)} %get-tuple-element.154), kind=kOutput, calls=%fused_computation.1.clone.1 | convolution fusion | flops 306706944 | bytes 10426880 | tf_op jit(solution)/shard_map/while/body/eval_jaxpr/qhcd,khcd->hcqk/dot_general | solution.py:76
  203.4 5.4 %fusion.55 = f32[2,2,384]{2,1,0:T(2,128)S(1)} fusion(f32[2,2,1536,384]{3,2,1,0:T(8,128)} %get-tuple-element.142, f32[2,2,384]{2,1,0:T(2,128)S(1)} %fusion.54), kind=kLoop, calls=%fused_computation.4.clone.1 | loop fusion | flops 7076352 | bytes 9449472 | tf_op jit(solution)/shard_map/while/body/eval_jaxpr/reduce_sum | solution.py:82
  208.8 1.6 constant_dynamic-slice_fusion.2
  210.5 2.6 fusion.57
  213.1 6.2 %bitcast_reduce_fusion.2 = (f32[2,2,384]{2,1,0:T(2,128)S(1)}, f32[2,2,1536,384]{3,2,1,0:T(8,128)}) fusion(bf16[384,2,2,64]{0,3,2,1:T(8,128)(2,1)S(1)} %get-tuple-element.168, bf16[8,1536,2,2,64]{1,4,3,2,0:T(8,128)(2,1)} %get-tuple-element.167, s32[]{:T(128)} %get-tuple-element.154), kind=kOutput, calls=%fused_computation.1.clone.1 | convolution fusion | flops 306706944 | bytes 10426880 | tf_op jit(solution)/shard_map/while/body/eval_jaxpr/qhcd,khcd->hcqk/dot_general | solution.py:76
  219.4 5.4 %fusion.55 = f32[2,2,384]{2,1,0:T(2,128)S(1)} fusion(f32[2,2,1536,384]{3,2,1,0:T(8,128)} %get-tuple-element.142, f32[2,2,384]{2,1,0:T(2,128)S(1)} %fusion.54), kind=kLoop, calls=%fused_computation.4.clone.1 | loop fusion | flops 7076352 | bytes 9449472 | tf_op jit(solution)/shard_map/while/body/eval_jaxpr/reduce_sum | solution.py:82
  224.8 1.6 constant_dynamic-slice_fusion.2
  226.4 2.6 fusion.57
  229.1 6.2 %bitcast_reduce_fusion.2 = (f32[2,2,384]{2,1,0:T(2,128)S(1)}, f32[2,2,1536,384]{3,2,1,0:T(8,128)}) fusion(bf16[384,2,2,64]{0,3,2,1:T(8,128)(2,1)S(1)} %get-tuple-element.168, bf16[8,1536,2,2,64]{1,4,3,2,0:T(8,128)(2,1)} %get-tuple-element.167, s32[]{:T(128)} %get-tuple-element.154), kind=kOutput, calls=%fused_computation.1.clone.1 | convolution fusion | flops 306706944 | bytes 10426880 | tf_op jit(solution)/shard_map/while/body/eval_jaxpr/qhcd,khcd->hcqk/dot_general | solution.py:76
  235.3 5.4 %fusion.55 = f32[2,2,384]{2,1,0:T(2,128)S(1)} fusion(f32[2,2,1536,384]{3,2,1,0:T(8,128)} %get-tuple-element.142, f32[2,2,384]{2,1,0:T(2,128)S(1)} %fusion.54), kind=kLoop, calls=%fused_computation.4.clone.1 | loop fusion | flops 7076352 | bytes 9449472 | tf_op jit(solution)/shard_map/while/body/eval_jaxpr/reduce_sum | solution.py:82
  240.7 2.1 constant_dynamic-slice_fusion.2
  242.8 2.6 fusion.57
  245.5 6.2 %bitcast_reduce_fusion.2 = (f32[2,2,384]{2,1,0:T(2,128)S(1)}, f32[2,2,1536,384]{3,2,1,0:T(8,128)}) fusion(bf16[384,2,2,64]{0,3,2,1:T(8,128)(2,1)S(1)} %get-tuple-element.168, bf16[8,1536,2,2,64]{1,4,3,2,0:T(8,128)(2,1)} %get-tuple-element.167, s32[]{:T(128)} %get-tuple-element.154), kind=kOutput, calls=%fused_computation.1.clone.1 | convolution fusion | flops 306706944 | bytes 10426880 | tf_op jit(solution)/shard_map/while/body/eval_jaxpr/qhcd,khcd->hcqk/dot_general | solution.py:76
  251.7 5.6 %fusion.55 = f32[2,2,384]{2,1,0:T(2,128)S(1)} fusion(f32[2,2,1536,384]{3,2,1,0:T(8,128)} %get-tuple-element.142, f32[2,2,384]{2,1,0:T(2,128)S(1)} %fusion.54), kind=kLoop, calls=%fused_computation.4.clone.1 | loop fusion | flops 7076352 | bytes 9449472 | tf_op jit(solution)/shard_map/while/body/eval_jaxpr/reduce_sum | solution.py:82
  257.4 1.6 constant_dynamic-slice_fusion.2
  259.0 2.6 fusion.57
  261.7 6.2 %bitcast_reduce_fusion.2 = (f32[2,2,384]{2,1,0:T(2,128)S(1)}, f32[2,2,1536,384]{3,2,1,0:T(8,128)}) fusion(bf16[384,2,2,64]{0,3,2,1:T(8,128)(2,1)S(1)} %get-tuple-element.168, bf16[8,1536,2,2,64]{1,4,3,2,0:T(8,128)(2,1)} %get-tuple-element.167, s32[]{:T(128)} %get-tuple-element.154), kind=kOutput, calls=%fused_computation.1.clone.1 | convolution fusion | flops 306706944 | bytes 10426880 | tf_op jit(solution)/shard_map/while/body/eval_jaxpr/qhcd,khcd->hcqk/dot_general | solution.py:76
  267.9 5.5 %fusion.55 = f32[2,2,384]{2,1,0:T(2,128)S(1)} fusion(f32[2,2,1536,384]{3,2,1,0:T(8,128)} %get-tuple-element.142, f32[2,2,384]{2,1,0:T(2,128)S(1)} %fusion.54), kind=kLoop, calls=%fused_computation.4.clone.1 | loop fusion | flops 7076352 | bytes 9449472 | tf_op jit(solution)/shard_map/while/body/eval_jaxpr/reduce_sum | solution.py:82
  273.4 1.6 constant_dynamic-slice_fusion.2
  275.0 2.6 fusion.57
  277.7 6.2 %bitcast_reduce_fusion.2 = (f32[2,2,384]{2,1,0:T(2,128)S(1)}, f32[2,2,1536,384]{3,2,1,0:T(8,128)}) fusion(bf16[384,2,2,64]{0,3,2,1:T(8,128)(2,1)S(1)} %get-tuple-element.168, bf16[8,1536,2,2,64]{1,4,3,2,0:T(8,128)(2,1)} %get-tuple-element.167, s32[]{:T(128)} %get-tuple-element.154), kind=kOutput, calls=%fused_computation.1.clone.1 | convolution fusion | flops 306706944 | bytes 10426880 | tf_op jit(solution)/shard_map/while/body/eval_jaxpr/qhcd,khcd->hcqk/dot_general | solution.py:76
  283.9 5.4 %fusion.55 = f32[2,2,384]{2,1,0:T(2,128)S(1)} fusion(f32[2,2,1536,384]{3,2,1,0:T(8,128)} %get-tuple-element.142, f32[2,2,384]{2,1,0:T(2,128)S(1)} %fusion.54), kind=kLoop, calls=%fused_computation.4.clone.1 | loop fusion | flops 7076352 | bytes 9449472 | tf_op jit(solution)/shard_map/while/body/eval_jaxpr/reduce_sum | solution.py:82
  289.3 1.6 constant_dynamic-slice_fusion.2
  290.9 2.6 fusion.57
  293.6 6.2 %bitcast_reduce_fusion.2 = (f32[2,2,384]{2,1,0:T(2,128)S(1)}, f32[2,2,1536,384]{3,2,1,0:T(8,128)}) fusion(bf16[384,2,2,64]{0,3,2,1:T(8,128)(2,1)S(1)} %get-tuple-element.168, bf16[8,1536,2,2,64]{1,4,3,2,0:T(8,128)(2,1)} %get-tuple-element.167, s32[]{:T(128)} %get-tuple-element.154), kind=kOutput, calls=%fused_computation.1.clone.1 | convolution fusion | flops 306706944 | bytes 10426880 | tf_op jit(solution)/shard_map/while/body/eval_jaxpr/qhcd,khcd->hcqk/dot_general | solution.py:76
  299.8 5.4 %fusion.55 = f32[2,2,384]{2,1,0:T(2,128)S(1)} fusion(f32[2,2,1536,384]{3,2,1,0:T(8,128)} %get-tuple-element.142, f32[2,2,384]{2,1,0:T(2,128)S(1)} %fusion.54), kind=kLoop, calls=%fused_computation.4.clone.1 | loop fusion | flops 7076352 | bytes 9449472 | tf_op jit(solution)/shard_map/while/body/eval_jaxpr/reduce_sum | solution.py:82
  305.2 1.6 constant_dynamic-slice_fusion.2
  306.8 2.6 fusion.57
  309.5 6.2 %bitcast_reduce_fusion.2 = (f32[2,2,384]{2,1,0:T(2,128)S(1)}, f32[2,2,1536,384]{3,2,1,0:T(8,128)}) fusion(bf16[384,2,2,64]{0,3,2,1:T(8,128)(2,1)S(1)} %get-tuple-element.168, bf16[8,1536,2,2,64]{1,4,3,2,0:T(8,128)(2,1)} %get-tuple-element.167, s32[]{:T(128)} %get-tuple-element.154), kind=kOutput, calls=%fused_computation.1.clone.1 | convolution fusion | flops 306706944 | bytes 10426880 | tf_op jit(solution)/shard_map/while/body/eval_jaxpr/qhcd,khcd->hcqk/dot_general | solution.py:76
  315.7 5.4 %fusion.55 = f32[2,2,384]{2,1,0:T(2,128)S(1)} fusion(f32[2,2,1536,384]{3,2,1,0:T(8,128)} %get-tuple-element.142, f32[2,2,384]{2,1,0:T(2,128)S(1)} %fusion.54), kind=kLoop, calls=%fused_computation.4.clone.1 | loop fusion | flops 7076352 | bytes 9449472 | tf_op jit(solution)/shard_map/while/body/eval_jaxpr/reduce_sum | solution.py:82
  321.1 1.6 constant_dynamic-slice_fusion.2
  322.7 2.6 fusion.57
  325.4 0.0 copy-start.5
  325.4 0.3 copy.22
  325.7 0.1 broadcast_divide_fusion
  325.8 0.3 copy-done.4
  326.1 0.1 multiply_reduce_fusion.1
  326.2 0.1 multiply_convert_fusion.1
  326.4 0.6 convolution_convert_fusion
  327.0 0.0 copy-start.3
  327.0 25.8 %all_to_all.15 = bf16[8,48,2048]{2,1,0:T(8,128)(2,1)S(1)} all-to-all(bf16[8,48,2048]{2,1,0:T(8,128)(2,1)S(1)} %bitcast.67), channel_id=1, replica_groups=mesh['sp'=32,'tp'=8] {'tp'}, dimensions={0} | all-to-all | bytes 3145728 | tf_op jit(solution)/shard_map/all_to_all | solution.py:20
  352.8 0.2 convert_reduce_fusion.1
  353.0 0.2 multiply_reduce_fusion
  353.2 0.1 multiply_convert_fusion
  353.3 0.2 broadcast_in_dim.13
  353.5 24.0 %all_to_all.16 = bf16[8,48,2048]{2,1,0:T(8,128)(2,1)S(1)} all-to-all(bf16[8,48,2048]{2,1,0:T(8,128)(2,1)S(1)} %broadcast_in_dim.13), channel_id=1, replica_groups=mesh['sp'=32,'tp'=8] {'tp'}, dimensions={0} | all-to-all | bytes 3145728 | tf_op jit(solution)/shard_map/all_to_all | solution.py:26
  377.5 4.6 %fusion.21 = f32[384,704]{0,1:T(8,128)} fusion(bf16[384,2048]{1,0:T(8,128)(2,1)S(1)} %bitcast.68, bf16[2048,2112]{1,0:T(8,128)(2,1)} %all-gather.8.cloned.1.call-done), kind=kOutput, calls=%fused_computation.26 | convolution fusion | flops 1107296256 | bytes 5799936 | tf_op jit(solution)/shard_map/dot_general | solution.py:126
  382.1 8.8 %fusion.23 = bf16[384,2048]{1,0:T(8,128)(2,1)} fusion(bf16[2048,2112]{1,0:T(8,128)(2,1)} %all-gather.8.cloned.1.call-done, bf16[384,2048]{1,0:T(8,128)(2,1)S(1)} %bitcast.69, f32[384,704]{0,1:T(8,128)} %fusion.21), kind=kOutput, calls=%fused_computation.30 | convolution fusion | flops 2217000960 | bytes 10518528 | tf_op jit(solution)/shard_map/dot_general | solution.py:131
  390.8 25.1 %all_to_all.17 = bf16[8,48,2048]{2,1,0:T(8,128)(2,1)S(1)} all-to-all(bf16[8,48,2048]{2,1,0:T(8,128)(2,1)} %bitcast.70), channel_id=1, replica_groups=mesh['sp'=32,'tp'=8] {'tp'}, dimensions={0} | all-to-all | bytes 3145728 | tf_op jit(solution)/shard_map/all_to_all | solution.py:20
  415.9 0.2 convert_reduce_fusion
  416.2 0.8 add_convert_fusion
  (55 shorter events, 0.4 us)
Async XLA Ops:
  6.5 319.8 %copy-start = (bf16[256,2048]{1,0:T(8,128)(2,1)S(1)}, bf16[256,2048]{1,0:T(8,128)(2,1)}, u32[]{:S(2)}) copy-start(bf16[256,2048]{1,0:T(8,128)(2,1)} %param.19) | copy-start | bytes 3145732
  6.5 93.2 %all-gather.4.cloned.1.call-start = ((), (), s32[]{:S(2)}) async-start(), calls=%async_computation.3 | async-start | bytes 6488064 | tf_op jit(solution)/shard_map/all_gather | solution.py:96
  7.3 180.2 %all-gather.6.cloned.1.call-start = ((), (), s32[]{:S(2)}) async-start(), calls=%async_computation.4 | async-start | bytes 6488064 | tf_op jit(solution)/shard_map/all_gather | solution.py:97
  8.0 369.5 %all-gather.8.cloned.1.call-start = ((), (), s32[]{:S(2)}) async-start(), calls=%async_computation.5 | async-start | bytes 9191424 | tf_op jit(solution)/shard_map/all_gather | solution.py:44
  203.4 7.1 %copy-start.1 = (f32[2,2,1536,384]{3,2,1,0:T(8,128)S(1)}, f32[2,2,1536,384]{3,2,1,0:T(8,128)}, u32[]{:S(2)}) copy-start(f32[2,2,1536,384]{3,2,1,0:T(8,128)} %get-tuple-element.142) | copy-start | bytes 28311556 | tf_op jit(solution)/shard_map/while
  219.3 7.1 %copy-start.1 = (f32[2,2,1536,384]{3,2,1,0:T(8,128)S(1)}, f32[2,2,1536,384]{3,2,1,0:T(8,128)}, u32[]{:S(2)}) copy-start(f32[2,2,1536,384]{3,2,1,0:T(8,128)} %get-tuple-element.142) | copy-start | bytes 28311556 | tf_op jit(solution)/shard_map/while
  235.3 7.5 %copy-start.1 = (f32[2,2,1536,384]{3,2,1,0:T(8,128)S(1)}, f32[2,2,1536,384]{3,2,1,0:T(8,128)}, u32[]{:S(2)}) copy-start(f32[2,2,1536,384]{3,2,1,0:T(8,128)} %get-tuple-element.142) | copy-start | bytes 28311556 | tf_op jit(solution)/shard_map/while
  251.7 7.2 %copy-start.1 = (f32[2,2,1536,384]{3,2,1,0:T(8,128)S(1)}, f32[2,2,1536,384]{3,2,1,0:T(8,128)}, u32[]{:S(2)}) copy-start(f32[2,2,1536,384]{3,2,1,0:T(8,128)} %get-tuple-element.142) | copy-start | bytes 28311556 | tf_op jit(solution)/shard_map/while
  267.9 7.1 %copy-start.1 = (f32[2,2,1536,384]{3,2,1,0:T(8,128)S(1)}, f32[2,2,1536,384]{3,2,1,0:T(8,128)}, u32[]{:S(2)}) copy-start(f32[2,2,1536,384]{3,2,1,0:T(8,128)} %get-tuple-element.142) | copy-start | bytes 28311556 | tf_op jit(solution)/shard_map/while
  283.9 7.0 %copy-start.1 = (f32[2,2,1536,384]{3,2,1,0:T(8,128)S(1)}, f32[2,2,1536,384]{3,2,1,0:T(8,128)}, u32[]{:S(2)}) copy-start(f32[2,2,1536,384]{3,2,1,0:T(8,128)} %get-tuple-element.142) | copy-start | bytes 28311556 | tf_op jit(solution)/shard_map/while
  299.8 7.0 %copy-start.1 = (f32[2,2,1536,384]{3,2,1,0:T(8,128)S(1)}, f32[2,2,1536,384]{3,2,1,0:T(8,128)}, u32[]{:S(2)}) copy-start(f32[2,2,1536,384]{3,2,1,0:T(8,128)} %get-tuple-element.142) | copy-start | bytes 28311556 | tf_op jit(solution)/shard_map/while
  315.7 7.0 %copy-start.1 = (f32[2,2,1536,384]{3,2,1,0:T(8,128)S(1)}, f32[2,2,1536,384]{3,2,1,0:T(8,128)}, u32[]{:S(2)}) copy-start(f32[2,2,1536,384]{3,2,1,0:T(8,128)} %get-tuple-element.142) | copy-start | bytes 28311556 | tf_op jit(solution)/shard_map/while
  325.4 0.7 copy-start.4
  325.4 0.8 copy-start.5
  327.0 26.0 %copy-start.2 = (bf16[48,2048]{1,0:T(8,128)(2,1)S(1)}, bf16[48,2048]{1,0:T(8,128)(2,1)}, u32[]{:S(2)}) copy-start(bf16[48,2048]{1,0:T(8,128)(2,1)} %param.13) | copy-start | bytes 589828
  327.0 26.2 %copy-start.3 = (f32[2048]{0:T(1024)S(1)}, f32[2048]{0:T(1024)}, u32[]{:S(2)}) copy-start(f32[2048]{0:T(1024)} %param.20) | copy-start | bytes 24580
Sparse Core Ops, SparseCore 0:
  9.9 89.7 all-gather.3
  102.3 85.0 all-gather.5
  190.1 97.3 all-gather.7
where the time goes:
time: 428 us; the launch traced here: 423 us
  waiting for transfers between devices  126 us (29%)
  matrix products  84.7 us (20%)
  local copies, waits for them, and re-layouts  78.3 us (18%)
  blocking collectives  74.9 us (18%)
  other arithmetic  45.5 us (11%)
  between operations  13.3 us (3%)
    all_gather x1, waiting for transfers between devices, body(): key_piece = lax.all_gather(keys, 'sp', axis=0, tiled=True)  88.7 us
    all_to_all x2, blocking collectives, sent_and_summed(): lax.all_to_all(parts, axis, split_axis=0, concat_axis=0, tiled=True)  50.9 us
    dot_general x8, matrix products, one_block(): jnp.einsum('qhcd,khcd->hcqk', query_four, key_block, preferred_element_ty...  49.6 us
    reduce_sum x8, other arithmetic, one_block(): total = total * rescale + jnp.sum(expo, axis=-1)  43.5 us
    all_gather x1, waiting for transfers between devices, body(): value_piece = lax.all_gather(values, 'sp', axis=0, tiled=True)  36.1 us
    unnamed x12, local copies, waits for them, and re-layouts  31.2 us
    all_to_all x1, blocking collectives, sent_to_all(): return lax.all_to_all(copies, axis, split_axis=0, concat_axis=0, tiled=True)  24 us
    reshape x1, local copies, waits for them, and re-layouts, body(): key_blocks = key_piece.reshape(blocks, width, heads_local, 2, DH)  21.8 us
  transfers between devices with their start and end apart: 3, of which 2 were waited for; matrix products, arithmetic and copies ran while one was open for 46% of the time, Pallas kernels for 0%

commit v1 on v0

v1 whole, which is shorter than its diff:
```python
import functools

import jax
import jax.numpy as jnp
from jax import lax
from jax.experimental import pallas as pl
from jax.experimental.pallas import tpu as pltpu
from jax.sharding import Mesh, PartitionSpec as P

BF = jnp.bfloat16
F32 = jnp.float32
Z, Y, X, C = 8, 4, 4, 2
TQ = 256


def whole(n):
    return [pl.BlockSpec(memory_space=pltpu.VMEM)] * n


def attend_body(*refs, pieces, first):
    count = 1 + max(p[0] for p in pieces)
    q_ref, kv_refs = refs[0], refs[1 : 1 + count]
    old_ref = None if first else refs[1 + count]
    new_ref, sa, sb = refs[-3:]
    tiles = q_ref.shape[0] // TQ
    keys = 384 * len(pieces)

    def scores(t, s):
        q = q_ref[pl.ds(pl.multiple_of(t * TQ, TQ), TQ), :]
        top = None
        for j, (which, row, _) in enumerate(pieces):
            d = lax.dot_general(
                kv_refs[which][row : row + 384, :], q, (((1,), (1,)), ((), ())), preferred_element_type=F32
            )
            s[384 * j : 384 * (j + 1), :] = d
            m = jnp.max(d.reshape(48, 8, TQ), axis=0)
            top = m if top is None else jnp.maximum(top, m)
        return jnp.max(top, axis=0, keepdims=True)

    def add(t, s, top):
        at = pl.ds(pl.multiple_of(t * TQ, TQ), TQ)
        if not first:
            old_top = old_ref[136:137, at]
            top = jnp.maximum(old_top, top)
        total = None
        for j in range(0, len(pieces), 2):
            p = jnp.exp(s[384 * j : 384 * (j + 2), :] - top).astype(BF)
            v = jnp.concatenate(
                [kv_refs[w][row + 128 * i : row + 128 * (i + 1), :] for w, _, row in pieces[j : j + 2] for i in range(3)],
                axis=1,
            )
            ones = jnp.ones((16, 768), BF)
            d = jnp.dot(jnp.concatenate([v, ones], axis=0), p, preferred_element_type=F32)
            total = d if total is None else total + d
        total = total[:136]
        if not first:
            total = old_ref[0:136, at] * jnp.exp(old_top - top) + total
        new_ref[0:136, at] = total
        new_ref[136:144, at] = jnp.broadcast_to(top, (8, TQ))

    def body(i, top):
        t = 2 * i
        top_b = scores(t + 1, sb)
        add(t, sa, top)
        top_a = scores(jnp.minimum(t + 2, tiles - 1), sa)
        add(t + 1, sb, top_b)
        return top_a

    lax.fori_loop(0, tiles // 2, body, scores(0, sa))


def attend(q, arrays, pieces, state):
    first = state is None
    n = q.shape[0]
    keys = 384 * len(pieces)
    out = jax.ShapeDtypeStruct((144, n), F32)
    args = [q, *arrays] + ([] if first else [state])
    return pl.pallas_call(
        functools.partial(attend_body, pieces=pieces, first=first),
        in_specs=whole(len(args)),
        out_specs=pl.BlockSpec(memory_space=pltpu.VMEM),
        out_shape=out,
        scratch_shapes=[pltpu.VMEM((keys, TQ), F32)] * 2,
        input_output_aliases={} if first else {len(args) - 1: 0},
        compiler_params=pltpu.CompilerParams(vmem_limit_bytes=20 * 2**20),
        cost_estimate=pl.CostEstimate(flops=8 * 256 * n * keys, bytes_accessed=2**22, transcendentals=n * keys),
        name="attend",
    )(*args)


def block_body(kv_ref, out_ref):
    for half in range(2):
        out_ref[768 * half : 768 * half + 384, :] = kv_ref[384 * half : 384 * (half + 1), 0:128]
        for i in range(3):
            row = 384 * half + 128 * i
            out_ref[768 * half + 384 + 128 * i : 768 * half + 512 + 128 * i, :] = kv_ref[row : row + 128, 128:256].T


def make_block(kv):
    return pl.pallas_call(
        block_body,
        in_specs=whole(1),
        out_specs=pl.BlockSpec(memory_space=pltpu.VMEM),
        out_shape=jax.ShapeDtypeStruct((1536, 128), BF),
        cost_estimate=pl.CostEstimate(flops=10**7, bytes_accessed=2**20, transcendentals=0),
        name="block",
    )(kv)


def finish_body(mine_ref, other_ref, lam_ref, gain_ref, out_ref):
    n = out_ref.shape[0]
    lam = lam_ref[0]
    gain = gain_ref[...]
    for t in range(n // 128):
        maps = []
        for comp in range(2):
            at = slice(n * comp + 128 * t, n * comp + 128 * (t + 1))
            m0, m1 = mine_ref[136:137, at], other_ref[136:137, at]
            top = jnp.maximum(m0, m1)
            w0, w1 = jnp.exp(m0 - top), jnp.exp(m1 - top)
            total = mine_ref[128:129, at] * w0 + other_ref[128:129, at] * w1
            maps.append((mine_ref[0:128, at] * w0 + other_ref[0:128, at] * w1) / total)
        mixed = maps[0] - lam * maps[1]
        scale = lax.rsqrt(jnp.mean(mixed * mixed, axis=0, keepdims=True) + 1e-06)
        out_ref[128 * t : 128 * (t + 1), :] = ((mixed * scale).T * gain).astype(BF)


def finish(mine, other, lam, gain):
    n = mine.shape[1] // 2
    return pl.pallas_call(
        finish_body,
        in_specs=[*whole(2), pl.BlockSpec(memory_space=pltpu.SMEM), *whole(1)],
        out_specs=pl.BlockSpec(memory_space=pltpu.VMEM),
        out_shape=jax.ShapeDtypeStruct((n, 128), BF),
        cost_estimate=pl.CostEstimate(flops=10**8, bytes_accessed=2**21, transcendentals=0),
        name="finish",
    )(mine, other, lam, gain)


def mixer_body(x_ref, w_ref, out_ref, gu, down, hid):
    k = pl.program_id(0)
    x = x_ref[:, pl.ds(pl.multiple_of(k * 256, 256), 256)]
    for c in range(2):
        d = jnp.dot(x, w_ref[:, c, :, 0:1408].reshape(256, 1408), preferred_element_type=F32)

        @pl.when(k == 0)
        def _():
            gu[c] = d

        @pl.when(k > 0)
        def _():
            gu[c] += d

        down[c, pl.ds(pl.multiple_of(k * 256, 256), 256), :] = w_ref[:, c, :, 1408:2176].reshape(256, 768)

    @pl.when(k == pl.num_programs(0) - 1)
    def _():
        for c in range(2):
            for a, b in ((0, 640), (128, 768), (256, 896), (384, 1024), (512, 1152)):
                hid[:, 768 * c + a : 768 * c + a + 128] = (
                    jax.nn.silu(gu[c, :, a : a + 128]) * gu[c, :, b : b + 128]
                ).astype(BF)
            tail = gu[c, :, 1280:1408]
            both = jax.nn.silu(tail) * pltpu.roll(tail, 64, 1)
            lane = lax.broadcasted_iota(jnp.int32, both.shape, 1)
            hid[:, 768 * c + 640 : 768 * c + 768] = jnp.where(lane < 64, both, 0.0).astype(BF)
        for n in range(8):
            rows = slice(256 * n, 256 * (n + 1))
            total = None
            for c in range(2):
                d = lax.dot_general(
                    hid[:, 768 * c : 768 * (c + 1)], down[c, rows, :], (((1,), (1,)), ((), ())), preferred_element_type=F32
                )
                total = d if total is None else total + d
            out_ref[:, rows] = total.astype(BF)


def mixer(x, w):
    rows = x.shape[0]
    return pl.pallas_call(
        mixer_body,
        grid=(8,),
        in_specs=[
            pl.BlockSpec((rows, 2048), lambda k: (0, 0)),
            pl.BlockSpec((4, 2, 64, 2176), lambda k: (k, 0, 0, 0)),
        ],
        out_specs=pl.BlockSpec((rows, 2048), lambda k: (0, 0)),
        out_shape=jax.ShapeDtypeStruct((rows, 2048), BF),
        scratch_shapes=[pltpu.VMEM((2, rows, 1408), F32), pltpu.VMEM((2, 2048, 768), BF), pltpu.VMEM((rows, 1536), BF)],
        compiler_params=pltpu.CompilerParams(vmem_limit_bytes=40 * 2**20),
        cost_estimate=pl.CostEstimate(flops=6 * rows * 2048 * 1408, bytes_accessed=18 * 2**20, transcendentals=0),
        name="mixer",
    )(x, w)


def swap(v):
    return lax.ppermute(v, "c", [(0, 1), (1, 0)])


def around(v, step):
    return lax.ppermute(v, "z", [(i, (i + step) % Z) for i in range(Z)])


def exchange(v, axis):
    return lax.all_to_all(v, axis, split_axis=0, concat_axis=0, tiled=True)


def body(residual, queries, keys, values, mix_lambda, head_gain, out_weight, norm_gain, gate, up, down):
    x, y, c = lax.axis_index("x"), lax.axis_index("y"), lax.axis_index("c")
    tokens = queries.shape[0]
    half = tokens // 2

    packed = jnp.concatenate(
        [gate[:, :640], up[:, :640], gate[:, 640:], up[:, 640:], down.T, jnp.zeros((64, 64), BF)], axis=1
    )
    weights = lax.all_gather(packed, ("z", "y", "c"), axis=0, tiled=False).reshape(32, 2, 64, 2176)

    kv = jnp.concatenate([keys, values], axis=1)
    mine = lax.dynamic_slice_in_dim(kv, c * half, half, 0)
    got = swap(lax.dynamic_slice_in_dim(kv, (1 - c) * half, half, 0))
    low, high = jnp.where(c == 0, mine, got), jnp.where(c == 0, got, mine)
    heads = [
        jnp.concatenate([d[:, 128 * j : 128 * (j + 1)], d[:, 256 + 128 * j : 256 + 128 * (j + 1)]], axis=1)
        for d in (low, high)
        for j in range(2)
    ]
    kv_head = exchange(jnp.stack(heads), "y").reshape(4 * half, 256)
    block = make_block(kv_head)
    right, left = around(block, 1), around(block, -1)

    q_got = swap(queries)
    low, high = jnp.where(c == 0, queries, q_got), jnp.where(c == 0, q_got, queries)
    q_head = exchange(jnp.stack([d[:, 128 * j : 128 * (j + 1)] for d in (low, high) for j in range(2)]), "y")
    q_head = q_head.reshape(Y, X, C, 48, 128) * BF(0.125)
    lane = lax.broadcasted_iota(jnp.int32, (1, 128), 1)
    q_cols = []
    for sub in range(2):
        part = q_head[:, :, sub].reshape(768, 128)
        q_cols += [jnp.where(lane < 64, part, BF(0)), jnp.where(lane < 64, BF(0), part)]
    q_all = jnp.concatenate(q_cols, axis=0)

    one = [(0, 0, 384), (0, 768, 1152)]
    two = one + [(1, 0, 384), (1, 768, 1152)]
    state = attend(q_all, [block], one, None)
    right2, left2 = around(right, 1), around(left, -1)
    state = attend(q_all, [right, left], two, state)
    right3, left3 = around(right2, 1), around(left2, -1)
    state = attend(q_all, [right2, left2], two, state)
    last_r, last_l = around(right3[:768], 1), around(left3[768:], -1)
    state = attend(q_all, [right3, left3], two, state)
    state = attend(q_all, [last_r, last_l], [(0, 0, 384), (1, 0, 384)], state)

    own = lax.dynamic_slice_in_dim(state, c * 1536, 1536, 1)
    other = swap(lax.dynamic_slice_in_dim(state, (1 - c) * 1536, 1536, 1))
    lam_got = swap(mix_lambda)
    lam4 = jnp.where(c == 0, jnp.concatenate([mix_lambda, lam_got]), jnp.concatenate([lam_got, mix_lambda]))
    lam = lax.dynamic_slice_in_dim(lam4, y, 1, 0)
    attended = finish(own, other, lam, head_gain.reshape(1, 128))

    heads = exchange(attended.reshape(Y, 192, 128), "y")
    w_got = swap(out_weight)
    a_mine = lax.dynamic_slice_in_dim(heads, 2 * c, 2, 0)
    a_other = lax.dynamic_slice_in_dim(heads, 2 - 2 * c, 2, 0)
    side = lambda a: jnp.concatenate([a[0], a[1]], axis=1)
    part = jnp.dot(side(a_mine), out_weight, preferred_element_type=F32) + jnp.dot(
        side(a_other), w_got, preferred_element_type=F32
    )
    projected = exchange(part.astype(BF).reshape(X, 48, 2048), "x").astype(F32).sum(axis=0)
    after_mix = residual.astype(F32) + projected
    scale = lax.rsqrt(jnp.mean(after_mix * after_mix, axis=-1, keepdims=True) + 1e-06)
    normed = (after_mix * scale * norm_gain).astype(BF)
    rows = exchange(jnp.broadcast_to(normed, (X, 48, 2048)), "x").reshape(192, 2048)
    mixed = exchange(mixer(rows, weights).reshape(X, 48, 2048), "x").astype(F32).sum(axis=0)
    return (after_mix + 0.5 * mixed).astype(BF)


def solution(mesh):
    split = Mesh(mesh.devices.reshape(Z, Y, X, C), ("z", "y", "x", "c"))
    sp, tp = ("z", "y"), ("x", "c")
    return jax.shard_map(
        body,
        mesh=split,
        in_specs=(
            P(("z", "y", "x", "c"), None),
            P(sp, tp),
            P(sp, tp),
            P(sp, tp),
            P(tp),
            P(),
            P(tp, None),
            P(),
            P(sp, tp),
            P(sp, tp),
            P(tp, sp),
        ),
        out_specs=P(("z", "y", "x", "c"), None),
        check_vma=False,
    )
```

time: 428 us -> 187 us (0.44)
  waiting for transfers between devices: 126 us -> 33.6 us
  matrix products: 84.7 us -> 0.76 us
  local copies, waits for them, and re-layouts: 78.3 us -> 10.3 us
  Pallas kernels: 0 us -> 50.9 us
  other arithmetic: 45.5 us -> 3.31 us
  blocking collectives: 74.9 us -> 40.8 us
  starting transfers between devices: 0.08 us -> 32.4 us
    all_gather x3 -> x1, waiting for transfers between devices: 125 us -> 0.01 us  [body(): lax.all_gather(packed, ('z', 'y', 'c'), axis=0, tiled=False)]
    dot_general x19 -> x2, matrix products: 84.7 us -> 0.76 us  [the longest x1 0.38 us: body(): jnp.dot(side(a_other), w_got, preferred_element_type=F32)]
    pallas_call x0 -> x8, Pallas kernels: none -> 50.9 us  [the longest x5 32.2 us: attend(): pl.pallas_call(functools.partial(attend_body, pieces=pieces, first=first)...]
    reduce_sum x11 -> x2, other arithmetic: 44 us -> 0.25 us  [the longest x1 0.12 us: body(): exchange(part.astype(BF).reshape(X, 48, 2048), 'x').astype(F32).sum(axis=0)]
    all_to_all x3, blocking collectives: 74.9 us -> 40.8 us  [exchange(): return lax.all_to_all(v, axis, split_axis=0, concat_axis=0, tiled=True)]
    reshape x2 -> x0, local copies, waits for them, and re-layouts: 31.5 us -> none  [the longest x1 21.8 us: body(): key_blocks = key_piece.reshape(blocks, width, heads_local, 2, DH)]
    unnamed x12 -> x19, local copies, waits for them, and re-layouts: 31.2 us -> 3.02 us
    ppermute x0 -> x13, waiting for transfers between devices: none -> 21.5 us  [the longest x8 16.8 us: around(): return lax.ppermute(v, 'z', [(i, (i + step) % Z) for i in range(Z)])]
  transfers between devices with their start and end apart: 3 -> 17, of which waited for: 2 -> 9; matrix products, arithmetic and copies ran while one was open for 46% -> 3% of each run, Pallas kernels for 0% -> 20%
where the time goes in v1:
time: 187 us; the launch traced here: 186 us
  Pallas kernels  50.9 us (27%)
  blocking collectives  40.8 us (22%)
  waiting for transfers between devices  33.6 us (18%)
  starting transfers between devices  32.4 us (17%)
  between operations  13.7 us (7%)
  local copies, waits for them, and re-layouts  10.3 us (6%)
  other arithmetic  3.31 us (2%)
    all_to_all x3, blocking collectives, exchange(): return lax.all_to_all(v, axis, split_axis=0, concat_axis=0, tiled=True)  40.8 us
    pallas_call x5, Pallas kernels, attend(): pl.pallas_call(functools.partial(attend_body, pieces=pieces, first=first)...  32.2 us
    ppermute x8, waiting for transfers between devices, around(): return lax.ppermute(v, 'z', [(i, (i + step) % Z) for i in range(Z)])  16.8 us
    all_to_all x3, starting transfers between devices, exchange(): return lax.all_to_all(v, axis, split_axis=0, concat_axis=0, tiled=True)  15.8 us
    ppermute x8, starting transfers between devices, around(): return lax.ppermute(v, 'z', [(i, (i + step) % Z) for i in range(Z)])  15.5 us
    pallas_call x1, Pallas kernels, mixer(): pl.pallas_call(mixer_body, grid=(8,), in_specs=[pl.BlockSpec((rows, 2048)...  13.7 us
    all_to_all x3, waiting for transfers between devices, exchange(): return lax.all_to_all(v, axis, split_axis=0, concat_axis=0, tiled=True)  12.1 us
    ppermute x5, waiting for transfers between devices, swap(): return lax.ppermute(v, 'c', [(0, 1), (1, 0)])  4.7 us
  transfers between devices with their start and end apart: 17, of which 9 were waited for; matrix products, arithmetic and copies ran while one was open for 3% of the time, Pallas kernels for 20%

profile of v1, /device:TPU:8, one launch (start us, length us, event | category | flops | bytes accessed | tf_op | source)
XLA Modules:
  0.0 185.8 jit_solution(10790584553000592208)
XLA Ops:
  6.5 0.9 slice.92
  7.5 0.7 slice.94
  8.2 0.9 slice.93
  9.1 0.7 slice.95
  9.8 1.7 concatenate.43
  11.5 0.0 all-gather.3.cloned.1.call-update
  11.6 0.9 constant_dynamic-update-slice_fusion.1
  12.6 0.1 collective-permute-start.1
  12.7 0.5 collective-permute-start
  13.2 0.9 collective-permute-done.1
  14.1 0.1 broadcast_select_fusion.1
  14.2 0.1 fusion.11
  14.4 0.8 pad_maximum_fusion.2
  15.2 5.6 %all-to-all-start.1 = ((bf16[4,192,256]{2,1,0:T(8,128)(2,1)}), bf16[4,192,256]{2,1,0:T(8,128)(2,1)S(1)}, u32[]{:S(2)}, u32[]{:S(2)}) async-start(bf16[4,192,256]{2,1,0:T(8,128)(2,1)} %pad_maximum_fusion.2), calls=%async_computation.1 | async-start | bytes 786432 | tf_op jit(solution)/shard_map/all_to_all | solution.py:205
  20.8 0.1 slice_bitcast_fusion.1
  20.9 0.8 pad_maximum_fusion.1
  21.7 6.3 %all-to-all-done.1 = bf16[4,192,256]{2,1,0:T(8,128)(2,1)S(1)} async-done(((bf16[4,192,256]{2,1,0:T(8,128)(2,1)}), bf16[4,192,256]{2,1,0:T(8,128)(2,1)S(1)}, u32[]{:S(2)}, u32[]{:S(2)}) %all-to-all-start.1) | async-done | bytes 393248 | tf_op jit(solution)/shard_map/all_to_all | solution.py:205
  28.0 4.9 %all-to-all-start = ((bf16[4,384,128]{2,1,0:T(8,128)(2,1)}), bf16[4,384,128]{2,1,0:T(8,128)(2,1)S(1)}, u32[]{:S(2)}, u32[]{:S(2)}) async-start(bf16[4,384,128]{2,1,0:T(8,128)(2,1)} %pad_maximum_fusion.1), calls=%async_computation | async-start | bytes 786432 | tf_op jit(solution)/shard_map/all_to_all | solution.py:205
  32.9 1.9 %block.1.refs_1_ = bf16[1536,128]{1,0:T(8,128)(2,1)} custom-call(bf16[768,256]{1,0:T(8,128)(2,1)} %bitcast.49), custom_call_target="tpu_custom_call" | custom-call | flops 10000000 | bytes 1048576 | tf_op jit(solution)/shard_map/block/pallas_call | solution.py:100
  34.7 0.9 collective-permute-start.2
  35.7 3.9 %collective-permute-start.6 = (bf16[1536,128]{1,0:T(8,128)(2,1)}, bf16[1536,128]{1,0:T(8,128)(2,1)S(1)}, u32[]{:S(2)}, u32[]{:S(2)}) collective-permute-start(bf16[1536,128]{1,0:T(8,128)(2,1)} %block.1.refs_1_), channel_id=1, source_target_pairs={{0,224},{32,0},{64,32},{96,64},{128,96},{160,128},{192,160},{224,1... | collective-permute-start | bytes 1179656 | tf_op jit(solution)/shard_map/ppermute | solution.py:201
  39.6 1.0 all-to-all-done
  40.7 0.1 bitcast_select_fusion.3
  40.8 0.1 pad_maximum_fusion.refs_0_
  40.8 0.9 copy-done
  41.7 4.0 %attend.5.refs_3_ = f32[144,3072]{1,0:T(8,128)S(1)} custom-call(bf16[3072,128]{1,0:T(8,128)(2,1)S(1)} %pad_maximum_fusion.refs_0_, bf16[1536,128]{1,0:T(8,128)(2,1)S(1)} %copy-done), custom_call_target="tpu_custom_call" | custom-call | flops 4831838208 | bytes 4194304 | tf_op jit(solution)/shard_map/attend/pallas_call | solution.py:78
  45.7 7.9 %collective-permute-done.2.refs_1_ = bf16[1536,128]{1,0:T(8,128)(2,1)S(1)} collective-permute-done((bf16[1536,128]{1,0:T(8,128)(2,1)}, bf16[1536,128]{1,0:T(8,128)(2,1)S(1)}, u32[]{:S(2)}, u32[]{:S(2)}) %collective-permute-start.2) | collective-permute-done | bytes 393248 | tf_op jit(solution)/shard_map/ppermute | solution.py:201
  53.6 3.2 %collective-permute-start.7 = (bf16[1536,128]{1,0:T(8,128)(2,1)S(1)}, bf16[1536,128]{1,0:T(8,128)(2,1)S(1)}, u32[]{:S(2)}, u32[]{:S(2)}) collective-permute-start(bf16[1536,128]{1,0:T(8,128)(2,1)S(1)} %collective-permute-done.6.refs_2_), channel_id=1, source_target_pairs={{0,224},{32,0},{64,32},{96,64},{128,96},{160,128},{192,160},{224,1... | collective-permute-start | bytes 1179656 | tf_op jit(solution)/shard_map/ppermute | solution.py:201
  56.8 7.9 %attend.6.refs_3_ = f32[144,3072]{1,0:T(8,128)S(1)} custom-call(bf16[3072,128]{1,0:T(8,128)(2,1)S(1)} %pad_maximum_fusion.refs_0_, bf16[1536,128]{1,0:T(8,128)(2,1)S(1)} %collective-permute-done.2.refs_1_, bf16[1536,128]{1,0:T(8,128)(2,1)S(1)} %collective-permute-done.6.refs_2_, f32[144,3072]{1,0:T(8,128)S(1)} %attend.5.refs_3_), custom_call_target="tpu_custom_call", output_to_operand_aliasing={{}: (3, {})} | custom-call | flops 9663676416 | bytes 4194304 | tf_op jit(solution)/shard_map/attend/pallas_call | solution.py:78
  64.7 0.1 collective-permute-start.4
  64.8 3.2 %collective-permute-start.8 = (bf16[1536,128]{1,0:T(8,128)(2,1)S(1)}, bf16[1536,128]{1,0:T(8,128)(2,1)S(1)}, u32[]{:S(2)}, u32[]{:S(2)}) collective-permute-start(bf16[1536,128]{1,0:T(8,128)(2,1)S(1)} %collective-permute-done.7.refs_2_), channel_id=1, source_target_pairs={{0,224},{32,0},{64,32},{96,64},{128,96},{160,128},{192,160},{224,1... | collective-permute-start | bytes 1179656 | tf_op jit(solution)/shard_map/ppermute | solution.py:201
  68.1 7.9 %attend.7.refs_3_ = f32[144,3072]{1,0:T(8,128)S(1)} custom-call(bf16[3072,128]{1,0:T(8,128)(2,1)S(1)} %pad_maximum_fusion.refs_0_, bf16[1536,128]{1,0:T(8,128)(2,1)S(1)} %collective-permute-done.3.refs_1_, bf16[1536,128]{1,0:T(8,128)(2,1)S(1)} %collective-permute-done.7.refs_2_, f32[144,3072]{1,0:T(8,128)S(1)} %attend.6.refs_3_), custom_call_target="tpu_custom_call", output_to_operand_aliasing={{}: (3, {})} | custom-call | flops 9663676416 | bytes 4194304 | tf_op jit(solution)/shard_map/attend/pallas_call | solution.py:78
  75.9 8.6 %collective-permute-done.4.refs_1_ = bf16[1536,128]{1,0:T(8,128)(2,1)S(1)} collective-permute-done((bf16[1536,128]{1,0:T(8,128)(2,1)S(1)}, bf16[1536,128]{1,0:T(8,128)(2,1)S(1)}, u32[]{:S(2)}, u32[]{:S(2)}) %collective-permute-start.4) | collective-permute-done | bytes 393248 | tf_op jit(solution)/shard_map/ppermute | solution.py:201
  84.6 0.1 collective-permute-start.5
  84.7 0.1 collective-permute-done.8.refs_2_
  84.8 3.9 %collective-permute-start.9 = (bf16[768,128]{1,0:T(8,128)(2,1)S(1)}, bf16[768,128]{1,0:T(8,128)(2,1)S(1)}, u32[]{:S(2)}, u32[]{:S(2)}) collective-permute-start(bf16[768,128]{1,0:T(8,128)(2,1)S(1)} %slice.111), channel_id=1, source_target_pairs={{0,224},{32,0},{64,32},{96,64},{128,96},{160,128},{192,160},{224,1... | collective-permute-start | bytes 589832 | tf_op jit(solution)/shard_map/ppermute | solution.py:201
  88.7 7.9 %attend.8.refs_3_ = f32[144,3072]{1,0:T(8,128)S(1)} custom-call(bf16[3072,128]{1,0:T(8,128)(2,1)S(1)} %pad_maximum_fusion.refs_0_, bf16[1536,128]{1,0:T(8,128)(2,1)S(1)} %collective-permute-done.4.refs_1_, bf16[1536,128]{1,0:T(8,128)(2,1)S(1)} %collective-permute-done.8.refs_2_, f32[144,3072]{1,0:T(8,128)S(1)} %attend.7.refs_3_), custom_call_target="tpu_custom_call", output_to_operand_aliasing={{}: (3, {})} | custom-call | flops 9663676416 | bytes 4194304 | tf_op jit(solution)/shard_map/attend/pallas_call | solution.py:78
  96.6 0.2 collective-permute-done.9.refs_2_
  96.8 4.5 %attend.9 = f32[144,3072]{1,0:T(8,128)S(1)} custom-call(bf16[3072,128]{1,0:T(8,128)(2,1)S(1)} %pad_maximum_fusion.refs_0_, bf16[768,128]{1,0:T(8,128)(2,1)S(1)} %collective-permute-done.5.refs_1_, bf16[768,128]{1,0:T(8,128)(2,1)S(1)} %collective-permute-done.9.refs_2_, f32[144,3072]{1,0:T(8,128)S(1)} %attend.8.refs_3_), custom_call_target="tpu_custom_call", output_to_operand_aliasing={{}: (3, {})} | custom-call | flops 4831838208 | bytes 4194304 | tf_op jit(solution)/shard_map/attend/pallas_call | solution.py:78
  101.3 0.0 copy-start.3
  101.3 1.3 constant_dynamic-slice_fusion
  102.7 0.3 copy-done.3
  102.9 0.3 collective-permute-start.12
  103.2 0.3 collective-permute-start.11
  103.4 3.8 %collective-permute-done.11 = f32[2]{0:T(128)S(1)} collective-permute-done((f32[2]{0:T(128)S(1)}, f32[2]{0:T(128)S(1)}, u32[]{:S(2)}, u32[]{:S(2)}) %collective-permute-start.11) | collective-permute-done | bytes 40 | tf_op jit(solution)/shard_map/ppermute | solution.py:197
  107.2 0.1 broadcast_select_fusion.4
  107.3 0.6 dynamic_slice.25.lam_ref
  107.9 0.9 copy-done.4
  108.9 3.1 %finish.1 = bf16[768,128]{1,0:T(8,128)(2,1)} custom-call(f32[144,1536]{1,0:T(8,128)} %get-tuple-element.6.mine_ref, f32[144,1536]{1,0:T(8,128)} %copy-done.4, f32[1]{0:T(128)} %dynamic_slice.25.lam_ref, f32[1,128]{1,0:T(1,128)} %bitcast.53), custom_call_target="tpu_custom_call" | custom-call | flops 100000000 | bytes 2097152 | tf_op jit(solution)/shard_map/finish/pallas_call | solution.py:130
  112.0 5.3 %all-to-all-start.2 = ((bf16[4,192,128]{2,1,0:T(8,128)(2,1)}), bf16[4,192,128]{2,1,0:T(8,128)(2,1)S(1)}, u32[]{:S(2)}, u32[]{:S(2)}) async-start(bf16[4,192,128]{2,1,0:T(8,128)(2,1)} %bitcast.51), calls=%async_computation.2 | async-start | bytes 393216 | tf_op jit(solution)/shard_map/all_to_all | solution.py:205
  117.3 4.9 %all-to-all-done.2 = bf16[4,192,128]{2,1,0:T(8,128)(2,1)S(1)} async-done(((bf16[4,192,128]{2,1,0:T(8,128)(2,1)}), bf16[4,192,128]{2,1,0:T(8,128)(2,1)S(1)}, u32[]{:S(2)}, u32[]{:S(2)}) %all-to-all-start.2) | async-done | bytes 196640 | tf_op jit(solution)/shard_map/all_to_all | solution.py:205
  122.2 0.4 fusion.1
  122.6 0.4 fusion
  123.0 0.0 copy-start.1
  123.0 15.6 %all_to_all.30 = bf16[4,48,2048]{2,1,0:T(8,128)(2,1)S(1)} all-to-all(bf16[4,48,2048]{2,1,0:T(8,128)(2,1)S(1)} %bitcast.48), channel_id=1, replica_groups=mesh['z'=8,'y'=4,'x'=4,'c'=2] {'x'}, dimensions={0} | all-to-all | bytes 1572864 | tf_op jit(solution)/shard_map/all_to_all | solution.py:205
  138.6 0.1 convert_reduce_fusion.1
  138.7 0.2 multiply_reduce_fusion
  138.9 0.1 multiply_convert_fusion
  139.0 0.1 broadcast_in_dim.44
  139.1 13.1 %all_to_all.31 = bf16[4,48,2048]{2,1,0:T(8,128)(2,1)S(1)} all-to-all(bf16[4,48,2048]{2,1,0:T(8,128)(2,1)S(1)} %broadcast_in_dim.44), channel_id=1, replica_groups=mesh['z'=8,'y'=4,'x'=4,'c'=2] {'x'}, dimensions={0} | all-to-all | bytes 1572864 | tf_op jit(solution)/shard_map/all_to_all | solution.py:205
  152.2 13.7 %mixer.1 = bf16[192,2048]{1,0:T(8,128)(2,1)S(1)} custom-call(bf16[192,2048]{1,0:T(8,128)(2,1)S(1)} %bitcast.45, bf16[32,2,64,2176]{3,2,1,0:T(8,128)(2,1)} %bitcast.47), custom_call_target="tpu_custom_call" | custom-call | flops 3321888768 | bytes 18874368 | tf_op jit(solution)/shard_map/mixer/pallas_call | solution.py:180
  165.8 12.2 %all_to_all.32 = bf16[4,48,2048]{2,1,0:T(8,128)(2,1)S(1)} all-to-all(bf16[4,48,2048]{2,1,0:T(8,128)(2,1)S(1)} %bitcast.46), channel_id=1, replica_groups=mesh['z'=8,'y'=4,'x'=4,'c'=2] {'x'}, dimensions={0} | all-to-all | bytes 1572864 | tf_op jit(solution)/shard_map/all_to_all | solution.py:205
  178.0 0.1 convert_reduce_fusion
  178.2 0.7 add_convert_fusion
  (39 shorter events, 0.3 us)
Async XLA Ops:
  6.5 6.0 %copy-start.5 = (bf16[384,256]{1,0:T(8,128)(2,1)S(1)}, bf16[384,256]{1,0:T(8,128)(2,1)}, u32[]{:S(2)}) copy-start(bf16[384,256]{1,0:T(8,128)(2,1)} %param.14) | copy-start | bytes 589828
  6.5 6.1 %copy-start.6 = (bf16[384,256]{1,0:T(8,128)(2,1)S(1)}, bf16[384,256]{1,0:T(8,128)(2,1)}, u32[]{:S(2)}) copy-start(bf16[384,256]{1,0:T(8,128)(2,1)} %param.12) | copy-start | bytes 589828
  6.5 145.6 %all-gather.3.cloned.1.call-start = ((), (), s32[]{:S(2)}) async-start(), calls=%async_computation.6 | async-start | bytes 18104320 | tf_op jit(solution)/shard_map/all_gather | solution.py:216
  12.6 1.5 collective-permute-start.1
  12.7 8.1 %collective-permute-start = (bf16[384,256]{1,0:T(8,128)(2,1)S(1)}, bf16[384,256]{1,0:T(8,128)(2,1)S(1)}, u32[]{:S(2)}, u32[]{:S(2)}) collective-permute-start(bf16[384,256]{1,0:T(8,128)(2,1)S(1)} %copy-done.6), channel_id=1, source_target_pairs={{0,1},{1,0},{2,3},{3,2},{4,5},{5,4},{6,7},{7,6},{8,9},{9,8},{10,11... | collective-permute-start | bytes 589832 | tf_op jit(solution)/shard_map/ppermute | solution.py:197
  15.2 12.8 %all-to-all-start.1 = ((bf16[4,192,256]{2,1,0:T(8,128)(2,1)}), bf16[4,192,256]{2,1,0:T(8,128)(2,1)S(1)}, u32[]{:S(2)}, u32[]{:S(2)}) async-start(bf16[4,192,256]{2,1,0:T(8,128)(2,1)} %pad_maximum_fusion.2), calls=%async_computation.1 | async-start | bytes 786432 | tf_op jit(solution)/shard_map/all_to_all | solution.py:205
  28.0 4.9 %copy-start.2 = (bf16[4,192,256]{2,1,0:T(8,128)(2,1)}, bf16[4,192,256]{2,1,0:T(8,128)(2,1)S(1)}, u32[]{:S(2)}) copy-start(bf16[4,192,256]{2,1,0:T(8,128)(2,1)S(1)} %all-to-all-done.1) | copy-start | bytes 1179652
  28.0 12.6 %all-to-all-start = ((bf16[4,384,128]{2,1,0:T(8,128)(2,1)}), bf16[4,384,128]{2,1,0:T(8,128)(2,1)S(1)}, u32[]{:S(2)}, u32[]{:S(2)}) async-start(bf16[4,384,128]{2,1,0:T(8,128)(2,1)} %pad_maximum_fusion.1), calls=%async_computation | async-start | bytes 786432 | tf_op jit(solution)/shard_map/all_to_all | solution.py:205
  34.7 18.9 %collective-permute-start.2 = (bf16[1536,128]{1,0:T(8,128)(2,1)}, bf16[1536,128]{1,0:T(8,128)(2,1)S(1)}, u32[]{:S(2)}, u32[]{:S(2)}) collective-permute-start(bf16[1536,128]{1,0:T(8,128)(2,1)} %block.1.refs_1_), channel_id=1, source_target_pairs={{0,32},{32,64},{64,96},{96,128},{128,160},{160,192},{192,224},{224... | collective-permute-start | bytes 1179656 | tf_op jit(solution)/shard_map/ppermute | solution.py:201
  35.7 17.9 %collective-permute-start.6 = (bf16[1536,128]{1,0:T(8,128)(2,1)}, bf16[1536,128]{1,0:T(8,128)(2,1)S(1)}, u32[]{:S(2)}, u32[]{:S(2)}) collective-permute-start(bf16[1536,128]{1,0:T(8,128)(2,1)} %block.1.refs_1_), channel_id=1, source_target_pairs={{0,224},{32,0},{64,32},{96,64},{128,96},{160,128},{192,160},{224,1... | collective-permute-start | bytes 1179656 | tf_op jit(solution)/shard_map/ppermute | solution.py:201
  40.6 1.0 copy-start
  53.6 11.1 %collective-permute-start.3 = (bf16[1536,128]{1,0:T(8,128)(2,1)S(1)}, bf16[1536,128]{1,0:T(8,128)(2,1)S(1)}, u32[]{:S(2)}, u32[]{:S(2)}) collective-permute-start(bf16[1536,128]{1,0:T(8,128)(2,1)S(1)} %collective-permute-done.2.refs_1_), channel_id=1, source_target_pairs={{0,32},{32,64},{64,96},{96,128},{128,160},{160,192},{192,224},{224... | collective-permute-start | bytes 1179656 | tf_op jit(solution)/shard_map/ppermute | solution.py:201
  53.6 11.2 %collective-permute-start.7 = (bf16[1536,128]{1,0:T(8,128)(2,1)S(1)}, bf16[1536,128]{1,0:T(8,128)(2,1)S(1)}, u32[]{:S(2)}, u32[]{:S(2)}) collective-permute-start(bf16[1536,128]{1,0:T(8,128)(2,1)S(1)} %collective-permute-done.6.refs_2_), channel_id=1, source_target_pairs={{0,224},{32,0},{64,32},{96,64},{128,96},{160,128},{192,160},{224,1... | collective-permute-start | bytes 1179656 | tf_op jit(solution)/shard_map/ppermute | solution.py:201
  64.7 19.8 %collective-permute-start.4 = (bf16[1536,128]{1,0:T(8,128)(2,1)S(1)}, bf16[1536,128]{1,0:T(8,128)(2,1)S(1)}, u32[]{:S(2)}, u32[]{:S(2)}) collective-permute-start(bf16[1536,128]{1,0:T(8,128)(2,1)S(1)} %collective-permute-done.3.refs_1_), channel_id=1, source_target_pairs={{0,32},{32,64},{64,96},{96,128},{128,160},{160,192},{192,224},{224... | collective-permute-start | bytes 1179656 | tf_op jit(solution)/shard_map/ppermute | solution.py:201
  64.8 19.9 %collective-permute-start.8 = (bf16[1536,128]{1,0:T(8,128)(2,1)S(1)}, bf16[1536,128]{1,0:T(8,128)(2,1)S(1)}, u32[]{:S(2)}, u32[]{:S(2)}) collective-permute-start(bf16[1536,128]{1,0:T(8,128)(2,1)S(1)} %collective-permute-done.7.refs_2_), channel_id=1, source_target_pairs={{0,224},{32,0},{64,32},{96,64},{128,96},{160,128},{192,160},{224,1... | collective-permute-start | bytes 1179656 | tf_op jit(solution)/shard_map/ppermute | solution.py:201
  84.6 12.0 %collective-permute-start.5 = (bf16[768,128]{1,0:T(8,128)(2,1)S(1)}, bf16[768,128]{1,0:T(8,128)(2,1)S(1)}, u32[]{:S(2)}, u32[]{:S(2)}) collective-permute-start(bf16[768,128]{1,0:T(8,128)(2,1)S(1)} %slice.110), channel_id=1, source_target_pairs={{0,32},{32,64},{64,96},{96,128},{128,160},{160,192},{192,224},{224... | collective-permute-start | bytes 589832 | tf_op jit(solution)/shard_map/ppermute | solution.py:201
  84.8 12.0 %collective-permute-start.9 = (bf16[768,128]{1,0:T(8,128)(2,1)S(1)}, bf16[768,128]{1,0:T(8,128)(2,1)S(1)}, u32[]{:S(2)}, u32[]{:S(2)}) collective-permute-start(bf16[768,128]{1,0:T(8,128)(2,1)S(1)} %slice.111), channel_id=1, source_target_pairs={{0,224},{32,0},{64,32},{96,64},{128,96},{160,128},{192,160},{224,1... | collective-permute-start | bytes 589832 | tf_op jit(solution)/shard_map/ppermute | solution.py:201
  101.3 1.6 copy-start.3
  101.3 1.9 %copy-start.8 = (f32[2]{0:T(128)S(1)}, f32[2]{0:T(128)}, u32[]{:S(2)}) copy-start(f32[2]{0:T(128)} %param.15) | copy-start | bytes 28
  102.7 5.3 %collective-permute-start.10 = (f32[144,1536]{1,0:T(8,128)}, f32[144,1536]{1,0:T(8,128)S(1)}, u32[]{:S(2)}, u32[]{:S(2)}) collective-permute-start(f32[144,1536]{1,0:T(8,128)} %get-tuple-element.5), channel_id=1, source_target_pairs={{0,1},{1,0},{2,3},{3,2},{4,5},{5,4},{6,7},{7,6},{8,9},{9,8},{10,11... | collective-permute-start | bytes 2654216 | tf_op jit(solution)/shard_map/ppermute | solution.py:197
  102.9 19.7 %collective-permute-start.12 = (bf16[256,2048]{1,0:T(8,128)(2,1)S(1)}, bf16[256,2048]{1,0:T(8,128)(2,1)S(1)}, u32[]{:S(2)}, u32[]{:S(2)}) collective-permute-start(bf16[256,2048]{1,0:T(8,128)(2,1)S(1)} %copy-done.3), channel_id=1, source_target_pairs={{0,1},{1,0},{2,3},{3,2},{4,5},{5,4},{6,7},{7,6},{8,9},{9,8},{10,11... | collective-permute-start | bytes 3145736 | tf_op jit(solution)/shard_map/ppermute | solution.py:197
  103.2 4.0 %collective-permute-start.11 = (f32[2]{0:T(128)S(1)}, f32[2]{0:T(128)S(1)}, u32[]{:S(2)}, u32[]{:S(2)}) collective-permute-start(f32[2]{0:T(128)S(1)} %copy-done.8), channel_id=1, source_target_pairs={{0,1},{1,0},{2,3},{3,2},{4,5},{5,4},{6,7},{7,6},{8,9},{9,8},{10,11... | collective-permute-start | bytes 32 | tf_op jit(solution)/shard_map/ppermute | solution.py:197
  107.9 0.9 copy-start.4
  112.0 10.2 %all-to-all-start.2 = ((bf16[4,192,128]{2,1,0:T(8,128)(2,1)}), bf16[4,192,128]{2,1,0:T(8,128)(2,1)S(1)}, u32[]{:S(2)}, u32[]{:S(2)}) async-start(bf16[4,192,128]{2,1,0:T(8,128)(2,1)} %bitcast.51), calls=%async_computation.2 | async-start | bytes 393216 | tf_op jit(solution)/shard_map/all_to_all | solution.py:205
  123.0 15.7 %copy-start.1 = (bf16[48,2048]{1,0:T(8,128)(2,1)S(1)}, bf16[48,2048]{1,0:T(8,128)(2,1)}, u32[]{:S(2)}) copy-start(bf16[48,2048]{1,0:T(8,128)(2,1)} %param.11) | copy-start | bytes 589828
  123.0 15.9 %copy-start.7 = (f32[2048]{0:T(1024)S(1)}, f32[2048]{0:T(1024)}, u32[]{:S(2)}) copy-start(f32[2048]{0:T(1024)} %param.18) | copy-start | bytes 24580
Sparse Core Ops, SparseCore 0:
  11.7 111.5 all-gather.2

commit v2 on v1

v2 whole, which is shorter than its diff:
```python
import functools

import jax
import jax.numpy as jnp
from jax import lax
from jax.experimental import pallas as pl
from jax.experimental.pallas import tpu as pltpu
from jax.sharding import Mesh, PartitionSpec as P

BF = jnp.bfloat16
F32 = jnp.float32
Z, Y, X, C = 8, 4, 4, 2
TQ = 256


def whole(n):
    return [pl.BlockSpec(memory_space=pltpu.VMEM)] * n


def attend_body(*refs, pieces, first, parts, start):
    count = 1 + max(p[0] for p in pieces)
    q_ref, kv_refs = refs[0], refs[1 : 1 + count]
    old_refs = [None] * parts if first else refs[1 + count : 1 + count + parts]
    new_refs = refs[-2 - parts : -2]
    sa, sb = refs[-2:]
    each = new_refs[0].shape[1] // TQ
    tiles = each * parts

    def scores(t, s):
        q = q_ref[pl.ds(pl.multiple_of((start + t) * TQ, TQ), TQ), :]
        top = None
        for j, (which, row, _) in enumerate(pieces):
            d = lax.dot_general(
                kv_refs[which][row : row + 384, :], q, (((1,), (1,)), ((), ())), preferred_element_type=F32
            )
            s[384 * j : 384 * (j + 1), :] = d
            m = jnp.max(d.reshape(48, 8, TQ), axis=0)
            top = m if top is None else jnp.maximum(top, m)
        return jnp.max(top, axis=0, keepdims=True)

    def add(t, s, top, old_ref, new_ref):
        at = pl.ds(pl.multiple_of(t * TQ, TQ), TQ)
        if not first:
            old_top = old_ref[136:137, at]
            top = jnp.maximum(old_top, top)
        total = None
        for j in range(0, len(pieces), 2):
            p = jnp.exp(s[384 * j : 384 * (j + 2), :] - top).astype(BF)
            v = jnp.concatenate(
                [kv_refs[w][row + 128 * i : row + 128 * (i + 1), :] for w, _, row in pieces[j : j + 2] for i in range(3)],
                axis=1,
            )
            ones = jnp.ones((16, 768), BF)
            d = jnp.dot(jnp.concatenate([v, ones], axis=0), p, preferred_element_type=F32)
            total = d if total is None else total + d
        total = total[:136]
        if not first:
            total = old_ref[0:136, at] * jnp.exp(old_top - top) + total
        new_ref[0:136, at] = total
        new_ref[136:144, at] = jnp.broadcast_to(top, (8, TQ))

    top = scores(0, sa)
    for part in range(parts):

        def body(i, top):
            t = 2 * i
            base = each * part
            top_b = scores(base + t + 1, sb)
            add(t, sa, top, old_refs[part], new_refs[part])
            top_a = scores(jnp.minimum(base + t + 2, tiles - 1), sa)
            add(t + 1, sb, top_b, old_refs[part], new_refs[part])
            return top_a

        top = lax.fori_loop(0, each // 2, body, top)


def attend(q, arrays, pieces, states, parts=2, start=0):
    first = states is None
    n = 1536 * parts
    keys = 384 * len(pieces)
    args = [q, *arrays] + ([] if first else list(states))
    return pl.pallas_call(
        functools.partial(attend_body, pieces=pieces, first=first, parts=parts, start=start),
        in_specs=whole(len(args)),
        out_specs=whole(parts),
        out_shape=[jax.ShapeDtypeStruct((144, n // parts), F32)] * parts,
        scratch_shapes=[pltpu.VMEM((keys, TQ), F32)] * 2,
        input_output_aliases={} if first else {len(args) - parts + i: i for i in range(parts)},
        compiler_params=pltpu.CompilerParams(vmem_limit_bytes=16 * 2**20),
        cost_estimate=pl.CostEstimate(flops=8 * 256 * n * keys, bytes_accessed=2**22, transcendentals=n * keys),
        name="attend",
    )(*args)


def pack_body(gate_ref, up_ref, down_ref, out_ref):
    out_ref[:, 0:640] = gate_ref[:, 0:640]
    out_ref[:, 640:1280] = up_ref[:, 0:640]
    tails = [r[:, 640:704].astype(F32) for r in (gate_ref, up_ref)]
    out_ref[:, 1280:1408] = jnp.concatenate(tails, axis=1).astype(BF)
    row, col = (lax.broadcasted_iota(jnp.int32, (64, 64), i) for i in range(2))
    eye = jnp.where(row == col, 1.0, 0.0).astype(BF)
    turned = lax.dot_general(eye, down_ref[...], (((1,), (1,)), ((), ())), preferred_element_type=F32).astype(BF)
    out_ref[:, 1408:2048] = turned[:, 0:640]
    last = jnp.concatenate([turned[:, 640:704].astype(F32), jnp.zeros((64, 64), F32)], axis=1)
    out_ref[:, 2048:2176] = last.astype(BF)


def small(body, name, shapes, scalars, *args):
    alone = not isinstance(shapes, list)
    return pl.pallas_call(
        body,
        in_specs=[pl.BlockSpec(memory_space=pltpu.SMEM)] * scalars + whole(len(args) - scalars),
        out_specs=pl.BlockSpec(memory_space=pltpu.VMEM) if alone else whole(len(shapes)),
        out_shape=jax.ShapeDtypeStruct(*shapes) if alone else [jax.ShapeDtypeStruct(*sh) for sh in shapes],
        compiler_params=pltpu.CompilerParams(vmem_limit_bytes=8 * 2**20),
        cost_estimate=pl.CostEstimate(flops=10**7, bytes_accessed=2**20, transcendentals=0),
        name=name,
    )(*args)


def send_body(c_ref, q_ref, k_ref, v_ref, out_ref):
    at = pl.ds(pl.multiple_of((1 - c_ref[0]) * 192, 192), 192)
    out_ref[0:384, :] = q_ref[...]
    out_ref[384:576, :] = k_ref[at, :]
    out_ref[576:768, :] = v_ref[at, :]


def heads_body(c_ref, q_ref, k_ref, v_ref, got_ref, out_ref):
    c = c_ref[0]
    at = pl.ds(pl.multiple_of(c * 192, 192), 192)
    for j in range(2):
        lanes = slice(128 * j, 128 * (j + 1))
        out_ref[2 * c + j, 0:384, :] = q_ref[:, lanes]
        out_ref[2 * c + j, 384:576, :] = k_ref[at, lanes]
        out_ref[2 * c + j, 576:768, :] = v_ref[at, lanes]
        out_ref[2 - 2 * c + j] = got_ref[:, lanes]


def block_body(head_ref, out_ref):
    for i in range(4):
        at = 768 * (i // 2) + 192 * (i % 2)
        out_ref[at : at + 192, :] = head_ref[i, 384:576, :]
    values = jnp.concatenate([head_ref[i, 576:768, :] for i in range(4)], axis=0)
    for i in range(6):
        at = 768 * (i // 3) + 384 + 128 * (i % 3)
        out_ref[at : at + 128, :] = values[128 * i : 128 * (i + 1), :].T


def queries_body(c_ref, head_ref, out_ref):
    c = c_ref[0]
    lane = lax.broadcasted_iota(jnp.int32, (48, 128), 1)
    for i in range(2):
        sub = 1 - c if i == 0 else c
        for y in range(4):
            for x in range(4):
                rows = head_ref[y, pl.ds(pl.multiple_of(96 * x + 48 * sub, 48), 48), :].astype(F32) * 0.125
                at = 1536 * i + 192 * y + 48 * x
                out_ref[at : at + 48, :] = jnp.where(lane < 64, rows, 0.0).astype(BF)
                out_ref[at + 768 : at + 816, :] = jnp.where(lane < 64, 0.0, rows).astype(BF)


def finish_body(mine_ref, other_ref, lam_ref, gain_ref, out_ref):
    n = out_ref.shape[0]
    lam = lam_ref[0]
    gain = gain_ref[...]
    for t in range(n // 128):
        maps = []
        for comp in range(2):
            at = slice(n * comp + 128 * t, n * comp + 128 * (t + 1))
            m0, m1 = mine_ref[136:137, at], other_ref[136:137, at]
            top = jnp.maximum(m0, m1)
            w0, w1 = jnp.exp(m0 - top), jnp.exp(m1 - top)
            total = mine_ref[128:129, at] * w0 + other_ref[128:129, at] * w1
            maps.append((mine_ref[0:128, at] * w0 + other_ref[0:128, at] * w1) / total)
        mixed = maps[0] - lam * maps[1]
        scale = lax.rsqrt(jnp.mean(mixed * mixed, axis=0, keepdims=True) + 1e-06)
        out_ref[128 * t : 128 * (t + 1), :] = ((mixed * scale).T * gain).astype(BF)


def finish(mine, other, lam, gain):
    n = mine.shape[1] // 2
    return pl.pallas_call(
        finish_body,
        in_specs=[*whole(2), pl.BlockSpec(memory_space=pltpu.SMEM), *whole(1)],
        out_specs=pl.BlockSpec(memory_space=pltpu.VMEM),
        out_shape=jax.ShapeDtypeStruct((n, 128), BF),
        compiler_params=pltpu.CompilerParams(vmem_limit_bytes=8 * 2**20),
        cost_estimate=pl.CostEstimate(flops=10**8, bytes_accessed=2**21, transcendentals=0),
        name="finish",
    )(mine, other, lam, gain)


def mixer_body(x_ref, w_hbm, out_ref, w_ref, gu, hid, sems):
    parts = sems.shape[0]
    each = 32 // parts
    copies = [
        pltpu.make_async_copy(w_hbm.at[pl.ds(each * i, each)], w_ref.at[pl.ds(each * i, each)], sems.at[i])
        for i in range(parts)
    ]
    for copy in copies:
        copy.start()
    deep = 64 * each
    for i in range(parts):
        copies[i].wait()
        for c in range(2):
            w = w_ref[each * i : each * (i + 1), c, :, 0:1408].reshape(deep, 1408)
            d = jnp.dot(x_ref[:, deep * i : deep * (i + 1)], w, preferred_element_type=F32)
            if i == 0:
                gu[c] = d
            else:
                gu[c] += d
    for c in range(2):
        hid[:, 768 * c : 768 * c + 640] = (jax.nn.silu(gu[c, :, 0:640]) * gu[c, :, 640:1280]).astype(BF)
        tail = gu[c, :, 1280:1408]
        both = jax.nn.silu(tail) * pltpu.roll(tail, 64, 1)
        lane = lax.broadcasted_iota(jnp.int32, both.shape, 1)
        hid[:, 768 * c + 640 : 768 * c + 768] = jnp.where(lane < 64, both, 0.0).astype(BF)
    for n in range(8):
        total = None
        for c in range(2):
            w = w_ref[4 * n : 4 * (n + 1), c, :, 1408:2176].reshape(256, 768)
            d = lax.dot_general(
                hid[:, 768 * c : 768 * (c + 1)], w, (((1,), (1,)), ((), ())), preferred_element_type=F32
            )
            total = d if total is None else total + d
        out_ref[:, 256 * n : 256 * (n + 1)] = total.astype(BF)


def mixer(x, w):
    rows = x.shape[0]
    return pl.pallas_call(
        mixer_body,
        in_specs=[*whole(1), pl.BlockSpec(memory_space=pl.ANY)],
        out_specs=pl.BlockSpec(memory_space=pltpu.VMEM),
        out_shape=jax.ShapeDtypeStruct((rows, 2048), BF),
        scratch_shapes=[
            pltpu.VMEM(w.shape, BF),
            pltpu.VMEM((2, rows, 1408), F32),
            pltpu.VMEM((rows, 1536), BF),
            pltpu.SemaphoreType.DMA((4,)),
        ],
        compiler_params=pltpu.CompilerParams(vmem_limit_bytes=48 * 2**20),
        cost_estimate=pl.CostEstimate(flops=6 * rows * 2048 * 1408, bytes_accessed=18 * 2**20, transcendentals=0),
        name="mixer",
    )(x, w)


def swap(v):
    return lax.ppermute(v, "c", [(0, 1), (1, 0)])


def around(v, step):
    return lax.ppermute(v, "z", [(i, (i + step) % Z) for i in range(Z)])


def exchange(v, axis):
    return lax.all_to_all(v, axis, split_axis=0, concat_axis=0, tiled=True)


def body(residual, queries, keys, values, mix_lambda, head_gain, out_weight, norm_gain, gate, up, down):
    x, y, c = lax.axis_index("x"), lax.axis_index("y"), lax.axis_index("c")

    packed = small(pack_body, "pack", ((64, 2176), BF), 0, gate, up, down)
    weights = lax.all_gather(packed, ("z", "y", "c"), axis=0, tiled=False).reshape(32, 2, 64, 2176)

    core = c.reshape(1)
    got = swap(small(send_body, "send", ((768, 256), BF), 1, core, queries, keys, values))
    heads = small(heads_body, "heads", ((Y, 768, 128), BF), 1, core, queries, keys, values, got)
    head = exchange(heads, "y")
    block = small(block_body, "block", ((1536, 128), BF), 0, head)
    right, left = around(block, 1), around(block, -1)
    q_all = small(queries_body, "queries", ((3072, 128), BF), 1, core, head)

    one = [(0, 0, 384), (0, 768, 1152)]
    two = one + [(1, 0, 384), (1, 768, 1152)]
    states = attend(q_all, [block], one, None)
    right2, left2 = around(right, 1), around(left, -1)
    states = attend(q_all, [right, left], two, states)
    right3, left3 = around(right2, 1), around(left2, -1)
    states = attend(q_all, [right2, left2], two, states)
    last_r, last_l = around(right3[:768], 1), around(left3[768:], -1)
    states = attend(q_all, [right3, left3], two, states)
    ends = [(0, 0, 384), (1, 0, 384)]
    (theirs,) = attend(q_all, [last_r, last_l], ends, states[:1], 1)
    other = swap(theirs)
    (own,) = attend(q_all, [last_r, last_l], ends, states[1:], 1, 6)

    lam_got = swap(mix_lambda)
    lam4 = jnp.where(c == 0, jnp.concatenate([mix_lambda, lam_got]), jnp.concatenate([lam_got, mix_lambda]))
    lam = lax.dynamic_slice_in_dim(lam4, y, 1, 0)
    attended = finish(own, other, lam, head_gain.reshape(1, 128))

    heads = exchange(attended.reshape(Y, 192, 128), "y")
    w_got = swap(out_weight)
    a_mine = lax.dynamic_slice_in_dim(heads, 2 * c, 2, 0)
    a_other = lax.dynamic_slice_in_dim(heads, 2 - 2 * c, 2, 0)
    side = lambda a: jnp.concatenate([a[0], a[1]], axis=1)
    part = jnp.dot(side(a_mine), out_weight, preferred_element_type=F32) + jnp.dot(
        side(a_other), w_got, preferred_element_type=F32
    )
    projected = exchange(part.astype(BF).reshape(X, 48, 2048), "x").astype(F32).sum(axis=0)
    after_mix = residual.astype(F32) + projected
    scale = lax.rsqrt(jnp.mean(after_mix * after_mix, axis=-1, keepdims=True) + 1e-06)
    normed = (after_mix * scale * norm_gain).astype(BF)
    rows = exchange(jnp.broadcast_to(normed, (X, 48, 2048)), "x").reshape(192, 2048)
    mixed = exchange(mixer(rows, weights).reshape(X, 48, 2048), "x").astype(F32).sum(axis=0)
    return (after_mix + 0.5 * mixed).astype(BF)


def solution(mesh):
    split = Mesh(mesh.devices.reshape(Z, Y, X, C), ("z", "y", "x", "c"))
    sp, tp = ("z", "y"), ("x", "c")
    return jax.shard_map(
        body,
        mesh=split,
        in_specs=(
            P(("z", "y", "x", "c"), None),
            P(sp, tp),
            P(sp, tp),
            P(sp, tp),
            P(tp),
            P(),
            P(tp, None),
            P(),
            P(sp, tp),
            P(sp, tp),
            P(tp, sp),
        ),
        out_specs=P(("z", "y", "x", "c"), None),
        check_vma=False,
    )
```

time: 187 us -> 183 us (0.979)
  blocking collectives: 40.8 us -> 60 us
  starting transfers between devices: 32.4 us -> 22.9 us
  Pallas kernels: 50.9 us -> 41.7 us
  matrix products: 0.76 us -> 3.34 us
  waiting for transfers between devices: 33.6 us -> 31.4 us
  local copies, waits for them, and re-layouts: 10.3 us -> 8.29 us
  other arithmetic: 3.31 us -> 1.34 us
    all_to_all x3 -> x4, blocking collectives: 40.8 us -> 60 us  [exchange(): return lax.all_to_all(v, axis, split_axis=0, concat_axis=0, tiled=True)]
    all_to_all x3 -> x1, starting transfers between devices: 15.8 us -> 4.69 us  [exchange(): return lax.all_to_all(v, axis, split_axis=0, concat_axis=0, tiled=True)]
    pallas_call x7 -> x12, Pallas kernels: 47.7 us -> 40 us  [the longest x6 29.7 us: attend(): pl.pallas_call(functools.partial(attend_body, pieces=pieces, first=first,...]
    all_to_all x3 -> x1, waiting for transfers between devices: 12.1 us -> 5.1 us  [exchange(): return lax.all_to_all(v, axis, split_axis=0, concat_axis=0, tiled=True)]
    unnamed x19 -> x27, local copies, waits for them, and re-layouts: 3.02 us -> 7.55 us
    ppermute x8, waiting for transfers between devices: 16.8 us -> 20.7 us  [around(): return lax.ppermute(v, 'z', [(i, (i + step) % Z) for i in range(Z)])]
    slice x6 -> x0, local copies, waits for them, and re-layouts: 3.38 us -> none  [the longest x1 0.94 us: body(): gate[:, :640]]
    ppermute x8, starting transfers between devices: 15.5 us -> 17.4 us  [around(): return lax.ppermute(v, 'z', [(i, (i + step) % Z) for i in range(Z)])]
  transfers between devices with their start and end apart: 17 -> 14, of which waited for: 9 -> 8; matrix products, arithmetic and copies ran while one was open for 3% -> 2% of each run, Pallas kernels for 20% -> 17%
where the time goes in v2:
time: 183 us
  blocking collectives  60 us (33%)
  Pallas kernels  41.7 us (23%)
  waiting for transfers between devices  31.4 us (17%)
  starting transfers between devices  22.9 us (13%)
  between operations  13.7 us (7%)
  local copies, waits for them, and re-layouts  8.29 us (5%)
  matrix products  3.34 us (2%)
    all_to_all x4, blocking collectives, exchange(): return lax.all_to_all(v, axis, split_axis=0, concat_axis=0, tiled=True)  60 us
    pallas_call x6, Pallas kernels, attend(): pl.pallas_call(functools.partial(attend_body, pieces=pieces, first=first,...  29.7 us
    ppermute x8, waiting for transfers between devices, around(): return lax.ppermute(v, 'z', [(i, (i + step) % Z) for i in range(Z)])  20.7 us
    ppermute x8, starting transfers between devices, around(): return lax.ppermute(v, 'z', [(i, (i + step) % Z) for i in range(Z)])  17.4 us
    pallas_call x1, Pallas kernels, mixer(): pl.pallas_call(mixer_body, in_specs=[*whole(1), pl.BlockSpec(memory_space...  9.02 us
    unnamed x27, local copies, waits for them, and re-layouts  7.55 us
    ppermute x4, waiting for transfers between devices, swap(): return lax.ppermute(v, 'c', [(0, 1), (1, 0)])  5.56 us
    all_to_all x1, waiting for transfers between devices, exchange(): return lax.all_to_all(v, axis, split_axis=0, concat_axis=0, tiled=True)  5.1 us
  transfers between devices with their start and end apart: 14, of which 8 were waited for; matrix products, arithmetic and copies ran while one was open for 2% of the time, Pallas kernels for 17%

profile of v2, /device:TPU:8, one launch (start us, length us, event | category | flops | bytes accessed | tf_op | source)
XLA Modules:
  0.0 182.6 jit_solution(15335530284912568751)
XLA Ops:
  6.5 1.1 copy.20.down_ref
  7.6 0.9 copy-done.3
  8.5 0.9 copy-done.4
  9.4 0.9 pack.1
  10.3 0.0 all-gather.3.cloned.1.call-update
  10.3 0.0 copy-start
  10.3 0.9 copy-done
  11.3 0.9 copy-done.1
  12.2 0.9 copy-done.2
  13.1 0.1 collective-permute-start
  13.2 1.7 collective-permute-done.got_ref
  14.9 0.1 heads.1
  15.1 17.7 %all_to_all.25.head_ref = bf16[4,768,128]{2,1,0:T(8,128)(2,1)S(1)} all-to-all(bf16[4,768,128]{2,1,0:T(8,128)(2,1)S(1)} %heads.1), channel_id=1, replica_groups=mesh['z'=8,'y'=4,'x'=4,'c'=2] {'y'}, dimensions={0} | all-to-all | bytes 1572864 | tf_op jit(solution)/shard_map/all_to_all | solution.py:257
  32.8 0.1 block.1.refs_1_
  32.9 2.2 %collective-permute-start.1 = (bf16[1536,128]{1,0:T(8,128)(2,1)S(1)}, bf16[1536,128]{1,0:T(8,128)(2,1)S(1)}, u32[]{:S(2)}, u32[]{:S(2)}) collective-permute-start(bf16[1536,128]{1,0:T(8,128)(2,1)S(1)} %block.1.refs_1_), channel_id=1, source_target_pairs={{0,32},{32,64},{64,96},{96,128},{128,160},{160,192},{192,224},{224... | collective-permute-start | bytes 1179656 | tf_op jit(solution)/shard_map/ppermute | solution.py:253
  35.1 5.0 %collective-permute-start.5 = (bf16[1536,128]{1,0:T(8,128)(2,1)S(1)}, bf16[1536,128]{1,0:T(8,128)(2,1)S(1)}, u32[]{:S(2)}, u32[]{:S(2)}) collective-permute-start(bf16[1536,128]{1,0:T(8,128)(2,1)S(1)} %block.1.refs_1_), channel_id=1, source_target_pairs={{0,224},{32,0},{64,32},{96,64},{128,96},{160,128},{192,160},{224,1... | collective-permute-start | bytes 1179656 | tf_op jit(solution)/shard_map/ppermute | solution.py:253
  40.0 0.1 queries.1.refs_0_
  40.2 3.7 %attend.6 = (f32[144,1536]{1,0:T(8,128)S(1)}, f32[144,1536]{1,0:T(8,128)S(1)}) custom-call(bf16[3072,128]{1,0:T(8,128)(2,1)S(1)} %queries.1.refs_0_, bf16[1536,128]{1,0:T(8,128)(2,1)S(1)} %block.1.refs_1_), custom_call_target="tpu_custom_call" | custom-call | flops 4831838208 | bytes 4194304 | tf_op jit(solution)/shard_map/attend/pallas_call | solution.py:82
  43.9 9.7 %collective-permute-done.1.refs_1_ = bf16[1536,128]{1,0:T(8,128)(2,1)S(1)} collective-permute-done((bf16[1536,128]{1,0:T(8,128)(2,1)S(1)}, bf16[1536,128]{1,0:T(8,128)(2,1)S(1)}, u32[]{:S(2)}, u32[]{:S(2)}) %collective-permute-start.1) | collective-permute-done | bytes 393248 | tf_op jit(solution)/shard_map/ppermute | solution.py:253
  53.7 0.0 collective-permute-start.2
  53.7 0.0 collective-permute-done.5.refs_2_
  53.7 3.2 %collective-permute-start.6 = (bf16[1536,128]{1,0:T(8,128)(2,1)S(1)}, bf16[1536,128]{1,0:T(8,128)(2,1)S(1)}, u32[]{:S(2)}, u32[]{:S(2)}) collective-permute-start(bf16[1536,128]{1,0:T(8,128)(2,1)S(1)} %collective-permute-done.5.refs_2_), channel_id=1, source_target_pairs={{0,224},{32,0},{64,32},{96,64},{128,96},{160,128},{192,160},{224,1... | collective-permute-start | bytes 1179656 | tf_op jit(solution)/shard_map/ppermute | solution.py:253
  56.9 7.0 %attend.7 = (f32[144,1536]{1,0:T(8,128)S(1)}, f32[144,1536]{1,0:T(8,128)S(1)}) custom-call(bf16[3072,128]{1,0:T(8,128)(2,1)S(1)} %queries.1.refs_0_, bf16[1536,128]{1,0:T(8,128)(2,1)S(1)} %collective-permute-done.1.refs_1_, bf16[1536,128]{1,0:T(8,128)(2,1)S(1)} %collective-permute-done.5.refs_2_, ...), custom_call_target="tpu_custom_call", output_to_operand_aliasing={{0}: (3, {}), {1}: (4, {})} | custom-call | flops 9663676416 | bytes 4194304 | tf_op jit(solution)/shard_map/attend/pallas_call | solution.py:82
  64.0 0.6 collective-permute-done.2.refs_1_
  64.6 0.0 collective-permute-start.3
  64.6 0.0 collective-permute-done.6.refs_2_
  64.6 3.2 %collective-permute-start.7 = (bf16[1536,128]{1,0:T(8,128)(2,1)S(1)}, bf16[1536,128]{1,0:T(8,128)(2,1)S(1)}, u32[]{:S(2)}, u32[]{:S(2)}) collective-permute-start(bf16[1536,128]{1,0:T(8,128)(2,1)S(1)} %collective-permute-done.6.refs_2_), channel_id=1, source_target_pairs={{0,224},{32,0},{64,32},{96,64},{128,96},{160,128},{192,160},{224,1... | collective-permute-start | bytes 1179656 | tf_op jit(solution)/shard_map/ppermute | solution.py:253
  67.9 7.0 %attend.8 = (f32[144,1536]{1,0:T(8,128)S(1)}, f32[144,1536]{1,0:T(8,128)S(1)}) custom-call(bf16[3072,128]{1,0:T(8,128)(2,1)S(1)} %queries.1.refs_0_, bf16[1536,128]{1,0:T(8,128)(2,1)S(1)} %collective-permute-done.2.refs_1_, bf16[1536,128]{1,0:T(8,128)(2,1)S(1)} %collective-permute-done.6.refs_2_, ...), custom_call_target="tpu_custom_call", output_to_operand_aliasing={{0}: (3, {}), {1}: (4, {})} | custom-call | flops 9663676416 | bytes 4194304 | tf_op jit(solution)/shard_map/attend/pallas_call | solution.py:82
  74.9 9.6 %collective-permute-done.3.refs_1_ = bf16[1536,128]{1,0:T(8,128)(2,1)S(1)} collective-permute-done((bf16[1536,128]{1,0:T(8,128)(2,1)S(1)}, bf16[1536,128]{1,0:T(8,128)(2,1)S(1)}, u32[]{:S(2)}, u32[]{:S(2)}) %collective-permute-start.3) | collective-permute-done | bytes 393248 | tf_op jit(solution)/shard_map/ppermute | solution.py:253
  84.5 0.1 collective-permute-start.4
  84.6 0.0 collective-permute-done.7.refs_2_
  84.6 3.7 %collective-permute-start.8 = (bf16[768,128]{1,0:T(8,128)(2,1)S(1)}, bf16[768,128]{1,0:T(8,128)(2,1)S(1)}, u32[]{:S(2)}, u32[]{:S(2)}) collective-permute-start(bf16[768,128]{1,0:T(8,128)(2,1)S(1)} %slice.25), channel_id=1, source_target_pairs={{0,224},{32,0},{64,32},{96,64},{128,96},{160,128},{192,160},{224,1... | collective-permute-start | bytes 589832 | tf_op jit(solution)/shard_map/ppermute | solution.py:253
  88.3 7.0 %attend.9 = (f32[144,1536]{1,0:T(8,128)S(1)}, f32[144,1536]{1,0:T(8,128)S(1)}) custom-call(bf16[3072,128]{1,0:T(8,128)(2,1)S(1)} %queries.1.refs_0_, bf16[1536,128]{1,0:T(8,128)(2,1)S(1)} %collective-permute-done.3.refs_1_, bf16[1536,128]{1,0:T(8,128)(2,1)S(1)} %collective-permute-done.7.refs_2_, ...), custom_call_target="tpu_custom_call", output_to_operand_aliasing={{0}: (3, {}), {1}: (4, {})} | custom-call | flops 9663676416 | bytes 4194304 | tf_op jit(solution)/shard_map/attend/pallas_call | solution.py:82
  95.4 0.4 collective-permute-done.4.refs_1_
  95.8 0.3 collective-permute-done.8.refs_2_
  96.1 2.4 %attend.11 = f32[144,1536]{1,0:T(8,128)S(1)} custom-call(bf16[3072,128]{1,0:T(8,128)(2,1)S(1)} %queries.1.refs_0_, bf16[768,128]{1,0:T(8,128)(2,1)S(1)} %collective-permute-done.4.refs_1_, bf16[768,128]{1,0:T(8,128)(2,1)S(1)} %collective-permute-done.8.refs_2_, f32[144,1536]{1,0:T(8,128)S(1)} %get-tuple-element.20.refs_3_), custom_call_target="tpu_custom_call", output_to_operand_aliasing={{}: (3, {})} | custom-call | flops 2415919104 | bytes 4194304 | tf_op jit(solution)/shard_map/attend/pallas_call | solution.py:82
  98.5 0.1 collective-permute-start.9
  98.6 0.5 collective-permute-start.11
  99.1 0.1 collective-permute-start.10
  99.2 3.8 %collective-permute-done.10 = f32[2]{0:T(128)S(1)} collective-permute-done((f32[2]{0:T(128)S(1)}, f32[2]{0:T(128)S(1)}, u32[]{:S(2)}, u32[]{:S(2)}) %collective-permute-start.10) | collective-permute-done | bytes 40 | tf_op jit(solution)/shard_map/ppermute | solution.py:249
  103.1 0.1 broadcast_select_fusion
  103.2 0.6 dynamic_slice.9.lam_ref
  103.8 0.9 copy-done.7
  104.7 1.0 copy-done.9
  105.7 2.4 %attend.10.mine_ref = f32[144,1536]{1,0:T(8,128)S(1)} custom-call(bf16[3072,128]{1,0:T(8,128)(2,1)S(1)} %queries.1.refs_0_, bf16[768,128]{1,0:T(8,128)(2,1)S(1)} %copy-done.7, bf16[768,128]{1,0:T(8,128)(2,1)S(1)} %copy-done.9, f32[144,1536]{1,0:T(8,128)S(1)} %get-tuple-element.19.refs_3_), custom_call_target="tpu_custom_call", output_to_operand_aliasing={{}: (3, {})} | custom-call | flops 2415919104 | bytes 4194304 | tf_op jit(solution)/shard_map/attend/pallas_call | solution.py:82
  108.1 0.0 collective-permute-done.9.other_ref
  108.2 1.7 finish.1
  109.8 4.7 %all-to-all-start.1 = ((bf16[4,192,128]{2,1,0:T(8,128)(2,1)}), bf16[4,192,128]{2,1,0:T(8,128)(2,1)S(1)}, u32[]{:S(2)}, u32[]{:S(2)}) async-start(bf16[4,192,128]{2,1,0:T(8,128)(2,1)} %bitcast.2), calls=%async_computation.1 | async-start | bytes 393216 | tf_op jit(solution)/shard_map/all_to_all | solution.py:257
  114.5 5.1 %all-to-all-done.1 = bf16[4,192,128]{2,1,0:T(8,128)(2,1)S(1)} async-done(((bf16[4,192,128]{2,1,0:T(8,128)(2,1)}), bf16[4,192,128]{2,1,0:T(8,128)(2,1)S(1)}, u32[]{:S(2)}, u32[]{:S(2)}) %all-to-all-start.1) | async-done | bytes 196640 | tf_op jit(solution)/shard_map/all_to_all | solution.py:257
  119.6 1.7 fusion.1
  121.4 0.0 collective-permute-done.11
  121.4 1.6 fusion
  123.0 0.0 copy-start.10
  123.0 0.0 copy-start.11
  123.0 17.0 %all_to_all.26 = bf16[4,48,2048]{2,1,0:T(8,128)(2,1)S(1)} all-to-all(bf16[4,48,2048]{2,1,0:T(8,128)(2,1)S(1)} %bitcast.21), channel_id=1, replica_groups=mesh['z'=8,'y'=4,'x'=4,'c'=2] {'x'}, dimensions={0} | all-to-all | bytes 1572864 | tf_op jit(solution)/shard_map/all_to_all | solution.py:257
  140.1 0.1 convert_reduce_fusion.1
  140.2 0.2 multiply_reduce_fusion
  140.4 0.1 multiply_convert_fusion
  140.5 0.1 broadcast_in_dim.2
  140.6 13.1 %all_to_all.27 = bf16[4,48,2048]{2,1,0:T(8,128)(2,1)S(1)} all-to-all(bf16[4,48,2048]{2,1,0:T(8,128)(2,1)S(1)} %broadcast_in_dim.2), channel_id=1, replica_groups=mesh['z'=8,'y'=4,'x'=4,'c'=2] {'x'}, dimensions={0} | all-to-all | bytes 1572864 | tf_op jit(solution)/shard_map/all_to_all | solution.py:257
  153.7 9.0 %mixer.1 = bf16[192,2048]{1,0:T(8,128)(2,1)S(1)} custom-call(bf16[192,2048]{1,0:T(8,128)(2,1)S(1)} %bitcast.17, bf16[32,2,64,2176]{3,2,1,0:T(8,128)(2,1)} %bitcast.20), custom_call_target="tpu_custom_call" | custom-call | flops 3321888768 | bytes 18874368 | tf_op jit(solution)/shard_map/mixer/pallas_call | solution.py:231
  162.7 12.2 %all_to_all.28 = bf16[4,48,2048]{2,1,0:T(8,128)(2,1)S(1)} all-to-all(bf16[4,48,2048]{2,1,0:T(8,128)(2,1)S(1)} %bitcast.18), channel_id=1, replica_groups=mesh['z'=8,'y'=4,'x'=4,'c'=2] {'x'}, dimensions={0} | all-to-all | bytes 1572864 | tf_op jit(solution)/shard_map/all_to_all | solution.py:257
  174.9 0.1 convert_reduce_fusion
  175.0 0.7 add_convert_fusion
  (23 shorter events, 0.1 us)
Async XLA Ops:
  6.5 147.1 %all-gather.3.cloned.1.call-start = ((), (), s32[]{:S(2)}) async-start(), calls=%async_computation.5 | async-start | bytes 18104320 | tf_op jit(solution)/shard_map/all_gather | solution.py:264
  7.6 0.9 copy-start.3
  8.5 0.9 copy-start.4
  10.3 0.9 copy-start
  11.3 0.9 copy-start.1
  12.2 0.9 copy-start.2
  13.1 1.8 collective-permute-start
  32.9 20.8 %collective-permute-start.1 = (bf16[1536,128]{1,0:T(8,128)(2,1)S(1)}, bf16[1536,128]{1,0:T(8,128)(2,1)S(1)}, u32[]{:S(2)}, u32[]{:S(2)}) collective-permute-start(bf16[1536,128]{1,0:T(8,128)(2,1)S(1)} %block.1.refs_1_), channel_id=1, source_target_pairs={{0,32},{32,64},{64,96},{96,128},{128,160},{160,192},{192,224},{224... | collective-permute-start | bytes 1179656 | tf_op jit(solution)/shard_map/ppermute | solution.py:253
  35.1 18.6 %collective-permute-start.5 = (bf16[1536,128]{1,0:T(8,128)(2,1)S(1)}, bf16[1536,128]{1,0:T(8,128)(2,1)S(1)}, u32[]{:S(2)}, u32[]{:S(2)}) collective-permute-start(bf16[1536,128]{1,0:T(8,128)(2,1)S(1)} %block.1.refs_1_), channel_id=1, source_target_pairs={{0,224},{32,0},{64,32},{96,64},{128,96},{160,128},{192,160},{224,1... | collective-permute-start | bytes 1179656 | tf_op jit(solution)/shard_map/ppermute | solution.py:253
  53.7 10.9 %collective-permute-start.2 = (bf16[1536,128]{1,0:T(8,128)(2,1)S(1)}, bf16[1536,128]{1,0:T(8,128)(2,1)S(1)}, u32[]{:S(2)}, u32[]{:S(2)}) collective-permute-start(bf16[1536,128]{1,0:T(8,128)(2,1)S(1)} %collective-permute-done.1.refs_1_), channel_id=1, source_target_pairs={{0,32},{32,64},{64,96},{96,128},{128,160},{160,192},{192,224},{224... | collective-permute-start | bytes 1179656 | tf_op jit(solution)/shard_map/ppermute | solution.py:253
  53.7 10.9 %collective-permute-start.6 = (bf16[1536,128]{1,0:T(8,128)(2,1)S(1)}, bf16[1536,128]{1,0:T(8,128)(2,1)S(1)}, u32[]{:S(2)}, u32[]{:S(2)}) collective-permute-start(bf16[1536,128]{1,0:T(8,128)(2,1)S(1)} %collective-permute-done.5.refs_2_), channel_id=1, source_target_pairs={{0,224},{32,0},{64,32},{96,64},{128,96},{160,128},{192,160},{224,1... | collective-permute-start | bytes 1179656 | tf_op jit(solution)/shard_map/ppermute | solution.py:253
  64.6 19.9 %collective-permute-start.3 = (bf16[1536,128]{1,0:T(8,128)(2,1)S(1)}, bf16[1536,128]{1,0:T(8,128)(2,1)S(1)}, u32[]{:S(2)}, u32[]{:S(2)}) collective-permute-start(bf16[1536,128]{1,0:T(8,128)(2,1)S(1)} %collective-permute-done.2.refs_1_), channel_id=1, source_target_pairs={{0,32},{32,64},{64,96},{96,128},{128,160},{160,192},{192,224},{224... | collective-permute-start | bytes 1179656 | tf_op jit(solution)/shard_map/ppermute | solution.py:253
  64.6 20.0 %collective-permute-start.7 = (bf16[1536,128]{1,0:T(8,128)(2,1)S(1)}, bf16[1536,128]{1,0:T(8,128)(2,1)S(1)}, u32[]{:S(2)}, u32[]{:S(2)}) collective-permute-start(bf16[1536,128]{1,0:T(8,128)(2,1)S(1)} %collective-permute-done.6.refs_2_), channel_id=1, source_target_pairs={{0,224},{32,0},{64,32},{96,64},{128,96},{160,128},{192,160},{224,1... | collective-permute-start | bytes 1179656 | tf_op jit(solution)/shard_map/ppermute | solution.py:253
  84.5 11.3 %collective-permute-start.4 = (bf16[768,128]{1,0:T(8,128)(2,1)S(1)}, bf16[768,128]{1,0:T(8,128)(2,1)S(1)}, u32[]{:S(2)}, u32[]{:S(2)}) collective-permute-start(bf16[768,128]{1,0:T(8,128)(2,1)S(1)} %slice.24), channel_id=1, source_target_pairs={{0,32},{32,64},{64,96},{96,128},{128,160},{160,192},{192,224},{224... | collective-permute-start | bytes 589832 | tf_op jit(solution)/shard_map/ppermute | solution.py:253
  84.6 11.5 %collective-permute-start.8 = (bf16[768,128]{1,0:T(8,128)(2,1)S(1)}, bf16[768,128]{1,0:T(8,128)(2,1)S(1)}, u32[]{:S(2)}, u32[]{:S(2)}) collective-permute-start(bf16[768,128]{1,0:T(8,128)(2,1)S(1)} %slice.25), channel_id=1, source_target_pairs={{0,224},{32,0},{64,32},{96,64},{128,96},{160,128},{192,160},{224,1... | collective-permute-start | bytes 589832 | tf_op jit(solution)/shard_map/ppermute | solution.py:253
  95.8 2.7 %copy-start.6 = (bf16[768,128]{1,0:T(8,128)(2,1)}, bf16[768,128]{1,0:T(8,128)(2,1)S(1)}, u32[]{:S(2)}) copy-start(bf16[768,128]{1,0:T(8,128)(2,1)S(1)} %collective-permute-done.4.refs_1_) | copy-start | bytes 589828
  96.1 2.4 %copy-start.8 = (bf16[768,128]{1,0:T(8,128)(2,1)}, bf16[768,128]{1,0:T(8,128)(2,1)S(1)}, u32[]{:S(2)}) copy-start(bf16[768,128]{1,0:T(8,128)(2,1)S(1)} %collective-permute-done.8.refs_2_) | copy-start | bytes 589828
  96.1 3.0 %copy-start.12 = (f32[2]{0:T(128)S(1)}, f32[2]{0:T(128)}, u32[]{:S(2)}) copy-start(f32[2]{0:T(128)} %param.15) | copy-start | bytes 28
  98.5 9.6 %collective-permute-start.9 = (f32[144,1536]{1,0:T(8,128)S(1)}, f32[144,1536]{1,0:T(8,128)S(1)}, u32[]{:S(2)}, u32[]{:S(2)}) collective-permute-start(f32[144,1536]{1,0:T(8,128)S(1)} %attend.11), channel_id=1, source_target_pairs={{0,1},{1,0},{2,3},{3,2},{4,5},{5,4},{6,7},{7,6},{8,9},{9,8},{10,11... | collective-permute-start | bytes 2654216 | tf_op jit(solution)/shard_map/ppermute | solution.py:249
  98.6 22.7 %collective-permute-start.11 = (bf16[256,2048]{1,0:T(8,128)(2,1)}, bf16[256,2048]{1,0:T(8,128)(2,1)}, u32[]{:S(2)}, u32[]{:S(2)}) collective-permute-start(bf16[256,2048]{1,0:T(8,128)(2,1)} %param.17), channel_id=1, source_target_pairs={{0,1},{1,0},{2,3},{3,2},{4,5},{5,4},{6,7},{7,6},{8,9},{9,8},{10,11... | collective-permute-start | bytes 3145736 | tf_op jit(solution)/shard_map/ppermute | solution.py:249
  99.1 3.9 %collective-permute-start.10 = (f32[2]{0:T(128)S(1)}, f32[2]{0:T(128)S(1)}, u32[]{:S(2)}, u32[]{:S(2)}) collective-permute-start(f32[2]{0:T(128)S(1)} %copy-done.12), channel_id=1, source_target_pairs={{0,1},{1,0},{2,3},{3,2},{4,5},{5,4},{6,7},{7,6},{8,9},{9,8},{10,11... | collective-permute-start | bytes 32 | tf_op jit(solution)/shard_map/ppermute | solution.py:249
  103.8 0.9 copy-start.7
  104.7 1.0 copy-start.9
  105.7 2.5 %copy-start.5 = (f32[128]{0:T(128)S(1)}, f32[128]{0:T(128)}, u32[]{:S(2)}) copy-start(f32[128]{0:T(128)} %param.16) | copy-start | bytes 1540
  109.8 9.8 %all-to-all-start.1 = ((bf16[4,192,128]{2,1,0:T(8,128)(2,1)}), bf16[4,192,128]{2,1,0:T(8,128)(2,1)S(1)}, u32[]{:S(2)}, u32[]{:S(2)}) async-start(bf16[4,192,128]{2,1,0:T(8,128)(2,1)} %bitcast.2), calls=%async_computation.1 | async-start | bytes 393216 | tf_op jit(solution)/shard_map/all_to_all | solution.py:257
  123.0 17.2 %copy-start.10 = (bf16[48,2048]{1,0:T(8,128)(2,1)S(1)}, bf16[48,2048]{1,0:T(8,128)(2,1)}, u32[]{:S(2)}) copy-start(bf16[48,2048]{1,0:T(8,128)(2,1)} %param.11) | copy-start | bytes 589828
  123.0 17.4 %copy-start.11 = (f32[2048]{0:T(1024)S(1)}, f32[2048]{0:T(1024)}, u32[]{:S(2)}) copy-start(f32[2048]{0:T(1024)} %param.18) | copy-start | bytes 24580
Sparse Core Ops, SparseCore 0:
  10.4 112.3 all-gather.2

commit v3 on v2

v3 whole, which is shorter than its diff:
```python
import functools

import jax
import jax.numpy as jnp
from jax import lax
from jax.experimental import pallas as pl
from jax.experimental.pallas import tpu as pltpu
from jax.sharding import Mesh, PartitionSpec as P


BF = jnp.bfloat16
F32 = jnp.float32
Z, Y, X, C = 8, 4, 4, 2
TQ = 256


def whole(n):
    return [pl.BlockSpec(memory_space=pltpu.VMEM)] * n


def attend_body(*refs, pieces, first, parts, start):
    count = 1 + max(p[0] for p in pieces)
    q_ref, kv_refs = refs[0], refs[1 : 1 + count]
    old_refs = [None] * parts if first else refs[1 + count : 1 + count + parts]
    new_refs = refs[-2 - parts : -2]
    sa, sb = refs[-2:]
    each = new_refs[0].shape[1] // TQ
    tiles = each * parts

    def scores(t, s):
        q = q_ref[pl.ds(pl.multiple_of((start + t) * TQ, TQ), TQ), :]
        top = None
        for j, (which, row, _) in enumerate(pieces):
            d = lax.dot_general(
                kv_refs[which][row : row + 384, :], q, (((1,), (1,)), ((), ())), preferred_element_type=F32
            )
            s[384 * j : 384 * (j + 1), :] = d
            m = jnp.max(d.reshape(48, 8, TQ), axis=0)
            top = m if top is None else jnp.maximum(top, m)
        return jnp.max(top, axis=0, keepdims=True)

    def add(t, s, top, old_ref, new_ref):
        at = pl.ds(pl.multiple_of(t * TQ, TQ), TQ)
        if not first:
            old_top = old_ref[136:137, at]
            top = jnp.maximum(old_top, top)
        total = None
        for j in range(0, len(pieces), 2):
            p = jnp.exp(s[384 * j : 384 * (j + 2), :] - top).astype(BF)
            v = jnp.concatenate(
                [kv_refs[w][row + 128 * i : row + 128 * (i + 1), :] for w, _, row in pieces[j : j + 2] for i in range(3)],
                axis=1,
            )
            ones = jnp.ones((16, 768), BF)
            d = jnp.dot(jnp.concatenate([v, ones], axis=0), p, preferred_element_type=F32)
            total = d if total is None else total + d
        total = total[:136]
        if not first:
            total = old_ref[0:136, at] * jnp.exp(old_top - top) + total
        new_ref[0:136, at] = total
        new_ref[136:144, at] = jnp.broadcast_to(top, (8, TQ))

    top = scores(0, sa)
    for part in range(parts):

        def body(i, top):
            t = 2 * i
            base = each * part
            top_b = scores(base + t + 1, sb)
            add(t, sa, top, old_refs[part], new_refs[part])
            top_a = scores(jnp.minimum(base + t + 2, tiles - 1), sa)
            add(t + 1, sb, top_b, old_refs[part], new_refs[part])
            return top_a

        top = lax.fori_loop(0, each // 2, body, top)


def attend(q, arrays, pieces, states, parts=2, start=0):
    first = states is None
    n = 1536 * parts
    keys = 384 * len(pieces)
    args = [q, *arrays] + ([] if first else list(states))
    return pl.pallas_call(
        functools.partial(attend_body, pieces=pieces, first=first, parts=parts, start=start),
        in_specs=whole(len(args)),
        out_specs=whole(parts),
        out_shape=[jax.ShapeDtypeStruct((144, n // parts), F32)] * parts,
        scratch_shapes=[pltpu.VMEM((keys, TQ), F32)] * 2,
        input_output_aliases={} if first else {len(args) - parts + i: i for i in range(parts)},
        compiler_params=pltpu.CompilerParams(vmem_limit_bytes=16 * 2**20),
        cost_estimate=pl.CostEstimate(flops=8 * 256 * n * keys, bytes_accessed=2**22, transcendentals=n * keys),
        name="attend",
    )(*args)


def pack_body(gate_hbm, up_hbm, down_hbm, out_ref, gate_ref, up_ref, down_ref, sems):
    copies = [
        pltpu.make_async_copy(a, b, sems.at[i])
        for i, (a, b) in enumerate(((gate_hbm, gate_ref), (up_hbm, up_ref), (down_hbm, down_ref)))
    ]
    for copy in copies:
        copy.start()
    for copy in copies:
        copy.wait()
    for i, (a, b) in enumerate(((0, 256), (256, 512), (512, 640))):
        out_ref[:, 512 * i : 512 * i + b - a] = gate_ref[:, a:b]
        out_ref[:, 512 * i + b - a : 512 * i + 2 * (b - a)] = up_ref[:, a:b]
    tails = [r[:, 640:704].astype(F32) for r in (gate_ref, up_ref)]
    out_ref[:, 1280:1408] = jnp.concatenate(tails, axis=1).astype(BF)
    out_ref[:, 1408:2048] = down_ref[:, 0:640]
    last = jnp.concatenate([down_ref[:, 640:704].astype(F32), jnp.zeros((64, 64), F32)], axis=1)
    out_ref[:, 2048:2176] = last.astype(BF)


def pack(gate, up, down):
    return pl.pallas_call(
        pack_body,
        in_specs=[pl.BlockSpec(memory_space=pltpu.HBM)] * 3,
        out_specs=pl.BlockSpec(memory_space=pltpu.VMEM),
        out_shape=jax.ShapeDtypeStruct((64, 2176), BF),
        scratch_shapes=[
            pltpu.VMEM((64, 704), BF),
            pltpu.VMEM((64, 704), BF),
            pltpu.VMEM((64, 704), BF),
            pltpu.SemaphoreType.DMA((3,)),
        ],
        compiler_params=pltpu.CompilerParams(vmem_limit_bytes=63 * 2**20),
        cost_estimate=pl.CostEstimate(flops=10**7, bytes_accessed=2**19, transcendentals=0),
        name="pack",
    )(gate, up, down)


def small(body, shapes, scalars, *args):
    alone = not isinstance(shapes, list)
    return pl.pallas_call(
        body,
        in_specs=[pl.BlockSpec(memory_space=pltpu.SMEM)] * scalars + whole(len(args) - scalars),
        out_specs=pl.BlockSpec(memory_space=pltpu.VMEM) if alone else whole(len(shapes)),
        out_shape=jax.ShapeDtypeStruct(*shapes) if alone else [jax.ShapeDtypeStruct(*sh) for sh in shapes],
        compiler_params=pltpu.CompilerParams(vmem_limit_bytes=8 * 2**20),
        cost_estimate=pl.CostEstimate(flops=10**7, bytes_accessed=2**20, transcendentals=0),
    )(*args)


def send_body(c_ref, q_ref, k_ref, v_ref, out_ref):
    put_half(1 - c_ref[0], q_ref, k_ref, v_ref, lambda rows, ref, at: out_ref.__setitem__((rows, slice(None)), ref[at, :]))


def put_half(sub, q_ref, k_ref, v_ref, put):
    for x in range(4):
        put(slice(48 * x, 48 * (x + 1)), q_ref, pl.ds(pl.multiple_of(96 * x + 48 * sub, 48), 48))
    for i, ref in ((1, k_ref), (2, v_ref)):
        put(slice(192 * i, 192 * (i + 1)), ref, pl.ds(pl.multiple_of(192 * sub, 192), 192))


def heads_body(c_ref, q_ref, k_ref, v_ref, got_ref, out_ref):
    c = c_ref[0]
    for j in range(2):
        lanes = slice(128 * j, 128 * (j + 1))

        def put(rows, ref, at):
            out_ref[2 * c + j, rows, :] = ref[at, lanes]

        put_half(c, q_ref, k_ref, v_ref, put)
        out_ref[2 - 2 * c + j] = got_ref[:, lanes]


def block_body(head_ref, block_ref, q_ref):
    for i in range(4):
        at = 768 * (i // 2) + 192 * (i % 2)
        block_ref[at : at + 192, :] = head_ref[i, 192:384, :]
        q_ref[192 * i : 192 * (i + 1), :] = head_ref[i, 0:192, :]
    values = jnp.concatenate([head_ref[i, 384:576, :] for i in range(4)], axis=0)
    for i in range(6):
        at = 768 * (i // 3) + 384 + 128 * (i % 3)
        block_ref[at : at + 128, :] = values[128 * i : 128 * (i + 1), :].T


def queries_body(other_ref, own_ref, out_ref):
    lane = lax.broadcasted_iota(jnp.int32, (768, 128), 1)
    for i, ref in enumerate((other_ref, own_ref)):
        rows = ref[...].astype(F32) * 0.125
        out_ref[1536 * i : 1536 * i + 768, :] = jnp.where(lane < 64, rows, 0.0).astype(BF)
        out_ref[1536 * i + 768 : 1536 * (i + 1), :] = jnp.where(lane < 64, 0.0, rows).astype(BF)


def carry_body(w_ref, r_ref, out_ref):
    out_ref[0:128, :] = w_ref[0:128, :]
    out_ref[128:160, :] = r_ref[0:32, :]
    out_ref[160:288, :] = w_ref[128:256, :]
    out_ref[288:304, :] = r_ref[32:48, :]


def finish_body(mine_ref, other_ref, lam_ref, gain_ref, out_ref):
    n = 768
    lam = lam_ref[0]
    gain = gain_ref[...]
    for t in range(n // 128):
        maps = []
        for comp in range(2):
            at = slice(n * comp + 128 * t, n * comp + 128 * (t + 1))
            m0, m1 = mine_ref[136:137, at], other_ref[136:137, at]
            top = jnp.maximum(m0, m1)
            w0, w1 = jnp.exp(m0 - top), jnp.exp(m1 - top)
            total = mine_ref[128:129, at] * w0 + other_ref[128:129, at] * w1
            maps.append((mine_ref[0:128, at] * w0 + other_ref[0:128, at] * w1) / total)
        mixed = maps[0] - lam * maps[1]
        scale = lax.rsqrt(jnp.mean(mixed * mixed, axis=0, keepdims=True) + 1e-06)
        rows = ((mixed * scale).T * gain).astype(BF)
        for at in (128 * t, 128 * t + 64):
            for x in range(4):
                out_ref[at // 192, x, at % 192 : at % 192 + 64, :] = rows[at - 128 * t : at - 128 * t + 64]


def finish(mine, other, lam, gain):
    return pl.pallas_call(
        finish_body,
        in_specs=[*whole(2), pl.BlockSpec(memory_space=pltpu.SMEM), *whole(1)],
        out_specs=pl.BlockSpec(memory_space=pltpu.VMEM),
        out_shape=jax.ShapeDtypeStruct((Y, X, 192, 128), BF),
        compiler_params=pltpu.CompilerParams(vmem_limit_bytes=8 * 2**20),
        cost_estimate=pl.CostEstimate(flops=10**8, bytes_accessed=2**21, transcendentals=0),
        name="finish",
    )(mine, other, lam, gain)


def project_body(at_ref, g_ref, gain_ref, *refs):
    hbm, (normed_ref, own_ref, po, acc, sems) = refs[:10], refs[10:]
    x, c = at_ref[0], at_ref[1]
    copies = []
    for half in range(2):
        lanes = slice(1024 * half, 1024 * (half + 1))
        for i, ref in enumerate(hbm):
            k, rows = (i, slice(0, 304)) if i < 6 else (6 + i % 2, slice(0, 160) if i < 8 else slice(160, 304))
            copies.append(pltpu.make_async_copy(ref.at[:, lanes], po.at[k, rows, lanes], sems.at[10 * half + i]))
    for copy in copies:
        copy.start()
    blocks = []
    for k in range(8):
        xk = lax.rem(x + 4 + (0, -1, 1, 2)[k // 2], 4)
        ck = c if k % 2 == 0 else 1 - c
        blocks.append(jnp.concatenate([g_ref[2 * ck, xk], g_ref[2 * ck + 1, xk]], axis=1))
    for half in range(2):
        for i in range(10):
            copies[10 * half + i].wait()
        for n in range(2):
            lanes = slice(1024 * half + 512 * n, 1024 * half + 512 * (n + 1))
            total = None
            for k, a in enumerate(blocks):
                w = jnp.concatenate([po[k, 0:128, lanes], po[k, 160:288, lanes]], axis=0)
                d = jnp.dot(a, w, preferred_element_type=F32)
                total = d if total is None else total + d
            acc[:, lanes] = total
    for k, step in ((0, 0), (2, -1), (4, 1), (6, 2)):
        at = 48 * lax.rem(x + 4 + step, 4)
        acc[pl.ds(pl.multiple_of(at, 16), 32), :] += po[k, 128:160, :].astype(F32)
        acc[pl.ds(pl.multiple_of(at + 32, 16), 16), :] += po[k, 288:304, :].astype(F32)
    own_ref[...] = acc[pl.ds(pl.multiple_of(48 * x, 16), 48), :]
    gain = gain_ref[...]
    for i in range(6):
        rows = acc[32 * i : 32 * (i + 1), :]
        scale = lax.rsqrt(jnp.mean(rows * rows, axis=1, keepdims=True) + 1e-06)
        normed_ref[32 * i : 32 * (i + 1), :] = (rows * scale * gain).astype(BF)


def project(at, g, gain, blocks):
    return pl.pallas_call(
        project_body,
        in_specs=[pl.BlockSpec(memory_space=pltpu.SMEM), *whole(2)] + [pl.BlockSpec(memory_space=pltpu.HBM)] * 10,
        out_specs=whole(2),
        out_shape=[jax.ShapeDtypeStruct((192, 2048), BF), jax.ShapeDtypeStruct((48, 2048), F32)],
        scratch_shapes=[
            pltpu.VMEM((8, 304, 2048), BF),
            pltpu.VMEM((192, 2048), F32),
            pltpu.SemaphoreType.DMA((20,)),
        ],
        compiler_params=pltpu.CompilerParams(vmem_limit_bytes=62 * 2**20),
        cost_estimate=pl.CostEstimate(flops=2 * 192 * 2048 * 2048, bytes_accessed=10 * 2**20, transcendentals=0),
        name="project",
    )(at, g, gain, *blocks)


def mixer_body(x_ref, w_hbm, out_ref, w_ref, hid, sems):
    chunks = [(c, a, b) for c in range(2) for a, b in ((0, 512), (512, 1024), (1024, 1408))]
    views = [(slice(None), c, slice(None), slice(a, b)) for c, a, b in chunks]
    views += [(slice(16 * i, 16 * (i + 1)), slice(None), slice(None), slice(1408, 2176)) for i in range(2)]
    copies = [pltpu.make_async_copy(w_hbm.at[v], w_ref.at[v], sems.at[i]) for i, v in enumerate(views)]
    for copy in copies:
        copy.start()
    for i, (c, a, b) in enumerate(chunks):
        copies[i].wait()
        gu = jnp.dot(x_ref[...], w_ref[:, c, :, a:b].reshape(2048, b - a), preferred_element_type=F32)
        n = 256 if b - a == 512 else 128
        at = 768 * c + a // 2
        hid[:, at : at + n] = (jax.nn.silu(gu[:, 0:n]) * gu[:, n : 2 * n]).astype(BF)
        if n == 128:
            tail = gu[:, 256:384]
            both = jax.nn.silu(tail) * pltpu.roll(tail, 64, 1)
            lane = lax.broadcasted_iota(jnp.int32, both.shape, 1)
            hid[:, at + 128 : at + 256] = jnp.where(lane < 64, both, 0.0).astype(BF)
    for half in range(2):
        copies[6 + half].wait()

        @pl.loop(2 * half, 2 * half + 2)
        def _(m):
            for part in range(2):
                total = None
                for c in range(2):
                    w = w_ref[pl.ds(8 * m + 4 * part, 4), c, :, 1408:2176].reshape(256, 768)
                    d = lax.dot_general(
                        hid[:, 768 * c : 768 * (c + 1)], w, (((1,), (1,)), ((), ())), preferred_element_type=F32
                    )
                    total = d if total is None else total + d
                out_ref[:, pl.ds(pl.multiple_of(512 * m + 256 * part, 256), 256)] = total.astype(BF)


def mixer(x, w):
    rows = x.shape[0]
    return pl.pallas_call(
        mixer_body,
        in_specs=[*whole(1), pl.BlockSpec(memory_space=pltpu.HBM)],
        out_specs=pl.BlockSpec(memory_space=pltpu.VMEM),
        out_shape=jax.ShapeDtypeStruct((rows, 2048), BF),
        scratch_shapes=[pltpu.VMEM(w.shape, BF), pltpu.VMEM((rows, 1536), BF), pltpu.SemaphoreType.DMA((8,))],
        compiler_params=pltpu.CompilerParams(vmem_limit_bytes=62 * 2**20),
        cost_estimate=pl.CostEstimate(flops=6 * rows * 2048 * 1408, bytes_accessed=18 * 2**20, transcendentals=0),
        name="mixer",
    )(x, w)


def swap(v):
    return lax.ppermute(v, "c", [(0, 1), (1, 0)])


def around(v, step, axis="z", n=Z):
    return lax.ppermute(v, axis, [(i, (i + step) % n) for i in range(n)])


def exchange(v, axis):
    return lax.all_to_all(v, axis, split_axis=0, concat_axis=0, tiled=True)


def inner(residual, queries, keys, values, mix_lambda, head_gain, out_weight, norm_gain, gate, up, down):
    x, y, c = lax.axis_index("x"), lax.axis_index("y"), lax.axis_index("c")

    packed = pack(gate, up, down.T)
    weights = lax.all_gather(packed, ("z", "y", "c"), axis=0, tiled=False).reshape(32, 2, 64, 2176)

    core = c.reshape(1)
    lam_got = swap(mix_lambda)
    got = swap(small(send_body, ((576, 256), BF), 1, core, queries, keys, values))
    heads = small(heads_body, ((Y, 576, 128), BF), 1, core, queries, keys, values, got)
    head = exchange(heads, "y")
    block, q_own = small(block_body, [((1536, 128), BF), ((768, 128), BF)], 0, head)
    right, left = around(block, 1), around(block, -1)
    q_all = small(queries_body, ((3072, 128), BF), 0, swap(q_own), q_own)
    lam4 = jnp.where(c == 0, jnp.concatenate([mix_lambda, lam_got]), jnp.concatenate([lam_got, mix_lambda]))
    lam = lax.dynamic_slice_in_dim(lam4, y, 1, 0)

    at = jnp.stack([x, c])
    q_all, lam, at, out_weight, residual = lax.optimization_barrier((q_all, lam, at, out_weight, residual))
    carry = small(carry_body, ((304, 2048), BF), 0, out_weight, residual)
    from_left, from_right = around(carry, 1, "x", X), around(carry, -1, "x", X)
    carry_c = swap(carry)

    one = [(0, 0, 384), (0, 768, 1152)]
    two = one + [(1, 0, 384), (1, 768, 1152)]
    after = lax.optimization_barrier
    states = attend(q_all, [block], one, None)
    states, right, left = after((states, right, left))
    right2, left2 = around(right, 1), around(left, -1)
    states = attend(q_all, [right, left], two, states)
    states, right2, left2 = after((states, right2, left2))
    right3, left3 = around(right2, 1), around(left2, -1)
    states, from_left, from_right, carry_c = after((states, from_left, from_right, carry_c))
    far_a, far_b = around(from_left[:160], 1, "x", X), around(from_right[160:], -1, "x", X)
    left_c, right_c = swap(from_left), swap(from_right)
    states = attend(q_all, [right2, left2], two, states)
    states, right3, left3 = after((states, right3, left3))
    last_r, last_l = around(right3[:768], 1), around(left3[768:], -1)
    states, far_a, far_b, left_c, right_c = after((states, far_a, far_b, left_c, right_c))
    far_a_c, far_b_c = swap(far_a), swap(far_b)
    states = attend(q_all, [right3, left3], two, states)
    states, last_r, last_l, far_a_c, far_b_c = after((states, last_r, last_l, far_a_c, far_b_c))
    ends = [(0, 0, 384), (1, 0, 384)]
    (theirs,) = attend(q_all, [last_r, last_l], ends, states[:1], 1)
    other = swap(theirs)
    (own,) = attend(q_all, [last_r, last_l], ends, states[1:], 1, 6)

    attended = finish(own, other, lam, head_gain.reshape(1, 128)).reshape(Y * X, 192, 128)
    spread = exchange(attended, ("y", "x")).reshape(Y, X, 192, 128)
    blocks = [carry, carry_c, from_left, left_c, from_right, right_c, far_a, far_a_c, far_b, far_b_c]
    spread, weights = after((spread, weights))
    rows, after_mix = project(at, spread, norm_gain.reshape(1, 2048), blocks)
    mixed = mixer(rows, weights)
    mixed = exchange(mixed.reshape(X, 48, 2048), "x").astype(F32).sum(axis=0)
    return (after_mix + 0.5 * mixed).astype(BF)


def solution(mesh):
    split = Mesh(mesh.devices.reshape(Z, Y, X, C), ("z", "y", "x", "c"))
    sp, tp = ("z", "y"), ("x", "c")
    return jax.shard_map(
        inner,
        mesh=split,
        in_specs=(
            P(("z", "y", "x", "c"), None),
            P(sp, tp),
            P(sp, tp),
            P(sp, tp),
            P(tp),
            P(),
            P(tp, None),
            P(),
            P(sp, tp),
            P(sp, tp),
            P(tp, sp),
        ),
        out_specs=P(("z", "y", "x", "c"), None),
        check_vma=False,
    )
```

time: 183 us -> 179 us (0.978)
  blocking collectives: 60 us -> 34.4 us
  waiting for transfers between devices: 31.4 us -> 42 us
  Pallas kernels: 41.7 us -> 51.4 us
  starting transfers between devices: 22.9 us -> 28.3 us
  matrix products: 3.34 us -> 0 us
  local copies, waits for them, and re-layouts: 8.29 us -> 5.62 us
    all_to_all x4 -> x2, blocking collectives: 60 us -> 34.4 us  [exchange(): return lax.all_to_all(v, axis, split_axis=0, concat_axis=0, tiled=True)]
    ppermute x8 -> x12, waiting for transfers between devices: 20.7 us -> 30.8 us  [around(): return lax.ppermute(v, axis, [(i, (i + step) % n) for i in range(n)])]
    pallas_call x0 -> x2, Pallas kernels: none -> 9.32 us  [the longest x1 7.51 us: project(): pl.pallas_call(project_body, in_specs=[pl.BlockSpec(memory_space=pltpu.SM...]
    all_to_all x1, waiting for transfers between devices: 5.1 us -> 9.37 us  [exchange(): return lax.all_to_all(v, axis, split_axis=0, concat_axis=0, tiled=True)]
    ppermute x4 -> x9, waiting for transfers between devices: 5.56 us -> 1.8 us  [swap(): return lax.ppermute(v, 'c', [(0, 1), (1, 0)])]
    ppermute x8 -> x12, starting transfers between devices: 17.4 us -> 20.9 us  [around(): return lax.ppermute(v, axis, [(i, (i + step) % n) for i in range(n)])]
    dot_general x2 -> x0, matrix products: 3.34 us -> none  [the longest x1 1.74 us: body(): jnp.dot(side(a_mine), out_weight, preferred_element_type=F32)]
    unnamed x27 -> x36, local copies, waits for them, and re-layouts: 7.55 us -> 4.91 us
  transfers between devices with their start and end apart: 14 -> 23, of which waited for: 8 -> 9; matrix products, arithmetic and copies ran while one was open for 2% -> 1% of each run, Pallas kernels for 17% -> 18%
where the time goes in v3:
time: 179 us; the launch traced here: 177 us
  Pallas kernels  51.4 us (29%)
  waiting for transfers between devices  42 us (23%)
  blocking collectives  34.4 us (19%)
  starting transfers between devices  28.3 us (16%)
  between operations  13.8 us (8%)
  local copies, waits for them, and re-layouts  5.62 us (3%)
    all_to_all x2, blocking collectives, exchange(): return lax.all_to_all(v, axis, split_axis=0, concat_axis=0, tiled=True)  34.4 us
    ppermute x12, waiting for transfers between devices, around(): return lax.ppermute(v, axis, [(i, (i + step) % n) for i in range(n)])  30.8 us
    pallas_call x6, Pallas kernels, attend(): pl.pallas_call(functools.partial(attend_body, pieces=pieces, first=first,...  29.7 us
    ppermute x12, starting transfers between devices, around(): return lax.ppermute(v, axis, [(i, (i + step) % n) for i in range(n)])  20.9 us
    pallas_call x1, Pallas kernels, mixer(): pl.pallas_call(mixer_body, in_specs=[*whole(1), pl.BlockSpec(memory_space...  10.1 us
    all_to_all x1, waiting for transfers between devices, exchange(): return lax.all_to_all(v, axis, split_axis=0, concat_axis=0, tiled=True)  9.37 us
    pallas_call x1, Pallas kernels, project(): pl.pallas_call(project_body, in_specs=[pl.BlockSpec(memory_space=pltpu.SM...  7.51 us
    all_to_all x1, starting transfers between devices, exchange(): return lax.all_to_all(v, axis, split_axis=0, concat_axis=0, tiled=True)  5.73 us
  transfers between devices with their start and end apart: 23, of which 9 were waited for; matrix products, arithmetic and copies ran while one was open for 1% of the time, Pallas kernels for 18%

profile of v3, /device:TPU:8, one launch (start us, length us, event | category | flops | bytes accessed | tf_op | source)
XLA Modules:
  0.0 177.0 jit_solution(18038414155415170427)
XLA Ops:
  6.5 1.8 %pack.1 = bf16[64,2176]{1,0:T(8,128)(2,1)} custom-call(bf16[64,704]{1,0:T(8,128)(2,1)} %gate_hbm.1, bf16[64,704]{1,0:T(8,128)(2,1)} %up_hbm.1, bf16[64,704]{1,0:T(8,128)(2,1)} %bitcast.14), custom_call_target="tpu_custom_call" | custom-call | flops 10000000 | bytes 524288 | tf_op jit(solution)/shard_map/pack/pallas_call | solution.py:116
  8.4 0.0 all-gather.3.cloned.1.call-update
  8.4 0.0 copy-start.2
  8.4 0.9 copy-done.2
  9.3 0.9 copy-done.3
  10.2 0.9 copy-done.4
  11.2 0.0 copy-start.17
  11.2 0.1 collective-permute-start
  11.3 1.6 collective-permute-done.got_ref
  12.9 0.9 shard_map.110
  13.8 5.7 %all-to-all-start = ((bf16[4,576,128]{2,1,0:T(8,128)(2,1)}), bf16[4,576,128]{2,1,0:T(8,128)(2,1)S(1)}, u32[]{:S(2)}, u32[]{:S(2)}) async-start(bf16[4,576,128]{2,1,0:T(8,128)(2,1)} %shard_map.110), calls=%async_computation | async-start | bytes 1179648 | tf_op jit(solution)/shard_map/all_to_all | solution.py:340
  19.6 9.4 %all-to-all-done.head_ref = bf16[4,576,128]{2,1,0:T(8,128)(2,1)S(1)} async-done(((bf16[4,576,128]{2,1,0:T(8,128)(2,1)}), bf16[4,576,128]{2,1,0:T(8,128)(2,1)S(1)}, u32[]{:S(2)}, u32[]{:S(2)}) %all-to-all-start) | async-done | bytes 589856 | tf_op jit(solution)/shard_map/all_to_all | solution.py:340
  28.9 0.1 shard_map.111
  29.0 0.1 collective-permute-start.1
  29.1 0.6 pad_add_fusion.at_ref
  29.7 0.1 broadcast_select_fusion
  29.8 0.6 dynamic_slice.3.lam_ref
  30.4 0.9 collective-permute-start.3
  31.3 5.6 %collective-permute-start.4 = (bf16[1536,128]{1,0:T(8,128)(2,1)S(1)}, bf16[1536,128]{1,0:T(8,128)(2,1)S(1)}, u32[]{:S(2)}, u32[]{:S(2)}) collective-permute-start(bf16[1536,128]{1,0:T(8,128)(2,1)S(1)} %get-tuple-element.56.refs_1_), channel_id=1, source_target_pairs={{0,224},{32,0},{64,32},{96,64},{128,96},{160,128},{192,160},{224,1... | collective-permute-start | bytes 1179656 | tf_op jit(solution)/shard_map/ppermute | solution.py:336
  36.9 0.1 shard_map.112.refs_0_
  37.0 0.0 copy-start.1
  37.0 1.2 copy-done.1
  38.3 0.1 shard_map.113.refs_0_
  38.4 1.6 collective-permute-start.7
  39.9 1.7 collective-permute-start.8
  41.7 0.0 collective-permute-start.9
  41.7 3.8 %attend.6 = (f32[144,1536]{1,0:T(8,128)S(1)}, f32[144,1536]{1,0:T(8,128)S(1)}) custom-call(bf16[3072,128]{1,0:T(8,128)(2,1)S(1)} %shard_map.112.refs_0_, bf16[1536,128]{1,0:T(8,128)(2,1)S(1)} %get-tuple-element.56.refs_1_), custom_call_target="tpu_custom_call" | custom-call | flops 4831838208 | bytes 4194304 | tf_op jit(solution)/shard_map/attend/pallas_call | solution.py:83
  45.5 7.7 %collective-permute-done.3.refs_1_ = bf16[1536,128]{1,0:T(8,128)(2,1)S(1)} collective-permute-done((bf16[1536,128]{1,0:T(8,128)(2,1)S(1)}, bf16[1536,128]{1,0:T(8,128)(2,1)S(1)}, u32[]{:S(2)}, u32[]{:S(2)}) %collective-permute-start.3) | collective-permute-done | bytes 393248 | tf_op jit(solution)/shard_map/ppermute | solution.py:336
  53.1 0.0 collective-permute-done.4.refs_2_
  53.1 0.0 collective-permute-start.5
  53.1 3.2 %collective-permute-start.6 = (bf16[1536,128]{1,0:T(8,128)(2,1)S(1)}, bf16[1536,128]{1,0:T(8,128)(2,1)S(1)}, u32[]{:S(2)}, u32[]{:S(2)}) collective-permute-start(bf16[1536,128]{1,0:T(8,128)(2,1)S(1)} %collective-permute-done.4.refs_2_), channel_id=1, source_target_pairs={{0,224},{32,0},{64,32},{96,64},{128,96},{160,128},{192,160},{224,1... | collective-permute-start | bytes 1179656 | tf_op jit(solution)/shard_map/ppermute | solution.py:336
  56.4 7.0 %attend.7 = (f32[144,1536]{1,0:T(8,128)S(1)}, f32[144,1536]{1,0:T(8,128)S(1)}) custom-call(bf16[3072,128]{1,0:T(8,128)(2,1)S(1)} %shard_map.112.refs_0_, bf16[1536,128]{1,0:T(8,128)(2,1)S(1)} %collective-permute-done.3.refs_1_, bf16[1536,128]{1,0:T(8,128)(2,1)S(1)} %collective-permute-done.4.refs_2_, ...), custom_call_target="tpu_custom_call", output_to_operand_aliasing={{0}: (3, {}), {1}: (4, {})} | custom-call | flops 9663676416 | bytes 4194304 | tf_op jit(solution)/shard_map/attend/pallas_call | solution.py:83
  63.4 2.1 %collective-permute-done.5.refs_1_ = bf16[1536,128]{1,0:T(8,128)(2,1)S(1)} collective-permute-done((bf16[1536,128]{1,0:T(8,128)(2,1)S(1)}, bf16[1536,128]{1,0:T(8,128)(2,1)S(1)}, u32[]{:S(2)}, u32[]{:S(2)}) %collective-permute-start.5) | collective-permute-done | bytes 393248 | tf_op jit(solution)/shard_map/ppermute | solution.py:336
  65.6 0.4 collective-permute-start.10
  65.9 3.2 %collective-permute-done.7.refs_2_ = bf16[304,2048]{1,0:T(8,128)(2,1)S(1)} collective-permute-done((bf16[304,2048]{1,0:T(8,128)(2,1)S(1)}, bf16[304,2048]{1,0:T(8,128)(2,1)S(1)}, u32[]{:S(2)}, u32[]{:S(2)}) %collective-permute-start.7) | collective-permute-done | bytes 1245216 | tf_op jit(solution)/shard_map/ppermute | solution.py:336
  69.2 0.0 collective-permute-done.9.refs_1_
  69.2 0.3 collective-permute-start.14
  69.5 0.5 collective-permute-start.15
  70.0 1.7 collective-permute-start.11
  71.7 0.1 slice.12
  71.8 1.6 collective-permute-start.12
  73.4 13.0 %collective-permute-done.10.refs_1_ = bf16[1536,128]{1,0:T(8,128)(2,1)S(1)} collective-permute-done((bf16[1536,128]{1,0:T(8,128)(2,1)S(1)}, bf16[1536,128]{1,0:T(8,128)(2,1)S(1)}, u32[]{:S(2)}, u32[]{:S(2)}) %collective-permute-start.10) | collective-permute-done | bytes 393248 | tf_op jit(solution)/shard_map/ppermute | solution.py:336
  86.4 2.5 %collective-permute-start.13 = (bf16[144,2048]{1,0:T(8,128)(2,1)S(1)}, bf16[144,2048]{1,0:T(8,128)(2,1)S(1)}, u32[]{:S(2)}, u32[]{:S(2)}) collective-permute-start(bf16[144,2048]{1,0:T(8,128)(2,1)S(1)} %slice.13), channel_id=1, source_target_pairs={{0,6},{2,0},{4,2},{6,4},{1,7},{3,1},{5,3},{7,5},{8,14},{10,8},{12,... | collective-permute-start | bytes 1769480 | tf_op jit(solution)/shard_map/ppermute | solution.py:336
  88.9 7.1 %attend.8 = (f32[144,1536]{1,0:T(8,128)S(1)}, f32[144,1536]{1,0:T(8,128)S(1)}) custom-call(bf16[3072,128]{1,0:T(8,128)(2,1)S(1)} %shard_map.112.refs_0_, bf16[1536,128]{1,0:T(8,128)(2,1)S(1)} %collective-permute-done.5.refs_1_, bf16[1536,128]{1,0:T(8,128)(2,1)S(1)} %collective-permute-done.6.refs_2_, ...), custom_call_target="tpu_custom_call", output_to_operand_aliasing={{0}: (3, {}), {1}: (4, {})} | custom-call | flops 9663676416 | bytes 4194304 | tf_op jit(solution)/shard_map/attend/pallas_call | solution.py:83
  96.0 0.1 collective-permute-start.16
  96.1 3.4 %collective-permute-done.13.refs_8_ = bf16[144,2048]{1,0:T(8,128)(2,1)S(1)} collective-permute-done((bf16[144,2048]{1,0:T(8,128)(2,1)S(1)}, bf16[144,2048]{1,0:T(8,128)(2,1)S(1)}, u32[]{:S(2)}, u32[]{:S(2)}) %collective-permute-start.13) | collective-permute-done | bytes 589856 | tf_op jit(solution)/shard_map/ppermute | solution.py:336
  99.5 1.6 collective-permute-start.17
  101.1 0.1 collective-permute-start.18
  101.2 0.5 collective-permute-start.19
  101.7 7.0 %attend.9 = (f32[144,1536]{1,0:T(8,128)S(1)}, f32[144,1536]{1,0:T(8,128)S(1)}) custom-call(bf16[3072,128]{1,0:T(8,128)(2,1)S(1)} %shard_map.112.refs_0_, bf16[1536,128]{1,0:T(8,128)(2,1)S(1)} %collective-permute-done.10.refs_1_, bf16[1536,128]{1,0:T(8,128)(2,1)S(1)} %collective-permute-done.11.refs_2_, ...), custom_call_target="tpu_custom_call", output_to_operand_aliasing={{0}: (3, {}), {1}: (4, {})} | custom-call | flops 9663676416 | bytes 4194304 | tf_op jit(solution)/shard_map/attend/pallas_call | solution.py:83
  108.8 1.4 collective-permute-done.17.refs_2_
  110.3 0.8 copy-done.13
  111.1 2.4 %attend.11 = f32[144,1536]{1,0:T(8,128)S(1)} custom-call(bf16[3072,128]{1,0:T(8,128)(2,1)S(1)} %shard_map.112.refs_0_, bf16[768,128]{1,0:T(8,128)(2,1)S(1)} %collective-permute-done.16.refs_1_, bf16[768,128]{1,0:T(8,128)(2,1)S(1)} %collective-permute-done.17.refs_2_, f32[144,1536]{1,0:T(8,128)S(1)} %get-tuple-element.90.refs_3_), custom_call_target="tpu_custom_call", output_to_operand_aliasing={{}: (3, {})} | custom-call | flops 2415919104 | bytes 4194304 | tf_op jit(solution)/shard_map/attend/pallas_call | solution.py:83
  113.5 0.0 copy-start.6
  113.5 0.1 collective-permute-start.20
  113.6 2.4 %attend.10.mine_ref = f32[144,1536]{1,0:T(8,128)S(1)} custom-call(bf16[3072,128]{1,0:T(8,128)(2,1)S(1)} %shard_map.112.refs_0_, bf16[768,128]{1,0:T(8,128)(2,1)S(1)} %collective-permute-done.16.refs_1_, bf16[768,128]{1,0:T(8,128)(2,1)S(1)} %collective-permute-done.17.refs_2_, f32[144,1536]{1,0:T(8,128)S(1)} %get-tuple-element.89.refs_3_), custom_call_target="tpu_custom_call", output_to_operand_aliasing={{}: (3, {})} | custom-call | flops 2415919104 | bytes 4194304 | tf_op jit(solution)/shard_map/attend/pallas_call | solution.py:83
  116.0 0.2 collective-permute-done.20.other_ref
  116.2 1.0 finish.1
  117.2 19.7 %all_to_all.15 = bf16[16,192,128]{2,1,0:T(8,128)(2,1)} all-to-all(bf16[16,192,128]{2,1,0:T(8,128)(2,1)S(1)} %bitcast.9), channel_id=1, replica_groups=mesh['z'=8,'y'=4,'x'=4,'c'=2] {'y','x'}, dimensions={0} | all-to-all | bytes 1572864 | tf_op jit(solution)/shard_map/all_to_all | solution.py:340
  136.9 7.5 %project.1 = (bf16[192,2048]{1,0:T(8,128)(2,1)}, f32[48,2048]{1,0:T(8,128)}) custom-call(s32[2]{0:T(128)} %pad_add_fusion.at_ref, bf16[4,4,192,128]{3,2,1,0:T(8,128)(2,1)} %bitcast.13, f32[1,2048]{1,0:T(1,128)} %bitcast.15, bf16[304,2048]{1,0:T(8,128)(2,1)} %copy-done, bf16[304,2048]{1,0:T(8,128)(2,1)} %copy-done.9, bf16[304,2048]{1,0:T(8,128)(2,1)} %copy-done.7, ...), custom_call_target="tpu_custom_call" | custom-call | flops 1610612736 | bytes 10485760 | tf_op jit(solution)/shard_map/project/pallas_call | solution.py:267
  144.4 10.1 %mixer.1 = bf16[192,2048]{1,0:T(8,128)(2,1)} custom-call(bf16[192,2048]{1,0:T(8,128)(2,1)} %get-tuple-element.99.x_ref, bf16[32,2,64,2176]{3,2,1,0:T(8,128)(2,1)} %bitcast.11), custom_call_target="tpu_custom_call" | custom-call | flops 3321888768 | bytes 18874368 | tf_op jit(solution)/shard_map/mixer/pallas_call | solution.py:319
  154.6 14.7 %all_to_all.16 = bf16[4,48,2048]{2,1,0:T(8,128)(2,1)S(1)} all-to-all(bf16[4,48,2048]{2,1,0:T(8,128)(2,1)} %bitcast.12), channel_id=1, replica_groups=mesh['z'=8,'y'=4,'x'=4,'c'=2] {'x'}, dimensions={0} | all-to-all | bytes 1572864 | tf_op jit(solution)/shard_map/all_to_all | solution.py:340
  169.3 0.1 convert_reduce_fusion
  169.5 0.7 add_convert_fusion
  (45 shorter events, 0.2 us)
Async XLA Ops:
  6.5 130.4 %all-gather.3.cloned.1.call-start = ((), (), s32[]{:S(2)}) async-start(), calls=%async_computation.3 | async-start | bytes 18104320 | tf_op jit(solution)/shard_map/all_gather | solution.py:347
  8.4 0.9 copy-start.2
  9.3 0.9 copy-start.3
  10.2 0.9 copy-start.4
  11.2 8.4 %copy-start.17 = (f32[2]{0:T(128)S(1)}, f32[2]{0:T(128)}, u32[]{:S(2)}) copy-start(f32[2]{0:T(128)} %param.15) | copy-start | bytes 28
  11.2 1.7 collective-permute-start
  13.8 23.2 %copy-start.5 = (bf16[48,2048]{1,0:T(8,128)(2,1)S(1)}, bf16[48,2048]{1,0:T(8,128)(2,1)}, u32[]{:S(2)}) copy-start(bf16[48,2048]{1,0:T(8,128)(2,1)} %r_ref) | copy-start | bytes 589828
  13.8 15.1 %all-to-all-start = ((bf16[4,576,128]{2,1,0:T(8,128)(2,1)}), bf16[4,576,128]{2,1,0:T(8,128)(2,1)S(1)}, u32[]{:S(2)}, u32[]{:S(2)}) async-start(bf16[4,576,128]{2,1,0:T(8,128)(2,1)} %shard_map.110), calls=%async_computation | async-start | bytes 1179648 | tf_op jit(solution)/shard_map/all_to_all | solution.py:340
  19.6 10.2 %collective-permute-start.2 = (f32[2]{0:T(128)S(1)}, f32[2]{0:T(128)S(1)}, u32[]{:S(2)}, u32[]{:S(2)}) collective-permute-start(f32[2]{0:T(128)S(1)} %copy-done.17), channel_id=1, source_target_pairs={{0,1},{1,0},{2,3},{3,2},{4,5},{5,4},{6,7},{7,6},{8,9},{9,8},{10,11... | collective-permute-start | bytes 32 | tf_op jit(solution)/shard_map/ppermute | solution.py:332
  29.0 7.9 %collective-permute-start.1 = (bf16[768,128]{1,0:T(8,128)(2,1)S(1)}, bf16[768,128]{1,0:T(8,128)(2,1)S(1)}, u32[]{:S(2)}, u32[]{:S(2)}) collective-permute-start(bf16[768,128]{1,0:T(8,128)(2,1)S(1)} %get-tuple-element.53.own_ref), channel_id=1, source_target_pairs={{0,1},{1,0},{2,3},{3,2},{4,5},{5,4},{6,7},{7,6},{8,9},{9,8},{10,11... | collective-permute-start | bytes 589832 | tf_op jit(solution)/shard_map/ppermute | solution.py:332
  30.4 22.8 %collective-permute-start.3 = (bf16[1536,128]{1,0:T(8,128)(2,1)S(1)}, bf16[1536,128]{1,0:T(8,128)(2,1)S(1)}, u32[]{:S(2)}, u32[]{:S(2)}) collective-permute-start(bf16[1536,128]{1,0:T(8,128)(2,1)S(1)} %get-tuple-element.56.refs_1_), channel_id=1, source_target_pairs={{0,32},{32,64},{64,96},{96,128},{128,160},{160,192},{192,224},{224... | collective-permute-start | bytes 1179656 | tf_op jit(solution)/shard_map/ppermute | solution.py:336
  31.3 21.9 %collective-permute-start.4 = (bf16[1536,128]{1,0:T(8,128)(2,1)S(1)}, bf16[1536,128]{1,0:T(8,128)(2,1)S(1)}, u32[]{:S(2)}, u32[]{:S(2)}) collective-permute-start(bf16[1536,128]{1,0:T(8,128)(2,1)S(1)} %get-tuple-element.56.refs_1_), channel_id=1, source_target_pairs={{0,224},{32,0},{64,32},{96,64},{128,96},{160,128},{192,160},{224,1... | collective-permute-start | bytes 1179656 | tf_op jit(solution)/shard_map/ppermute | solution.py:336
  37.0 1.2 copy-start.1
  38.4 7.1 %copy-start = (bf16[304,2048]{1,0:T(8,128)(2,1)}, bf16[304,2048]{1,0:T(8,128)(2,1)S(1)}, u32[]{:S(2)}) copy-start(bf16[304,2048]{1,0:T(8,128)(2,1)S(1)} %shard_map.113.refs_0_) | copy-start | bytes 3735556
  38.4 30.8 %collective-permute-start.7 = (bf16[304,2048]{1,0:T(8,128)(2,1)S(1)}, bf16[304,2048]{1,0:T(8,128)(2,1)S(1)}, u32[]{:S(2)}, u32[]{:S(2)}) collective-permute-start(bf16[304,2048]{1,0:T(8,128)(2,1)S(1)} %shard_map.113.refs_0_), channel_id=1, source_target_pairs={{0,2},{2,4},{4,6},{6,0},{1,3},{3,5},{5,7},{7,1},{8,10},{10,12},{12... | collective-permute-start | bytes 3735560 | tf_op jit(solution)/shard_map/ppermute | solution.py:336
  39.9 29.2 %collective-permute-start.8 = (bf16[304,2048]{1,0:T(8,128)(2,1)S(1)}, bf16[304,2048]{1,0:T(8,128)(2,1)S(1)}, u32[]{:S(2)}, u32[]{:S(2)}) collective-permute-start(bf16[304,2048]{1,0:T(8,128)(2,1)S(1)} %shard_map.113.refs_0_), channel_id=1, source_target_pairs={{0,6},{2,0},{4,2},{6,4},{1,7},{3,1},{5,3},{7,5},{8,14},{10,8},{12,... | collective-permute-start | bytes 3735560 | tf_op jit(solution)/shard_map/ppermute | solution.py:336
  41.7 27.5 %collective-permute-start.9 = (bf16[304,2048]{1,0:T(8,128)(2,1)S(1)}, bf16[304,2048]{1,0:T(8,128)(2,1)S(1)}, u32[]{:S(2)}, u32[]{:S(2)}) collective-permute-start(bf16[304,2048]{1,0:T(8,128)(2,1)S(1)} %shard_map.113.refs_0_), channel_id=1, source_target_pairs={{0,1},{1,0},{2,3},{3,2},{4,5},{5,4},{6,7},{7,6},{8,9},{9,8},{10,11... | collective-permute-start | bytes 3735560 | tf_op jit(solution)/shard_map/ppermute | solution.py:332
  53.1 12.4 %collective-permute-start.5 = (bf16[1536,128]{1,0:T(8,128)(2,1)S(1)}, bf16[1536,128]{1,0:T(8,128)(2,1)S(1)}, u32[]{:S(2)}, u32[]{:S(2)}) collective-permute-start(bf16[1536,128]{1,0:T(8,128)(2,1)S(1)} %collective-permute-done.3.refs_1_), channel_id=1, source_target_pairs={{0,32},{32,64},{64,96},{96,128},{128,160},{160,192},{192,224},{224... | collective-permute-start | bytes 1179656 | tf_op jit(solution)/shard_map/ppermute | solution.py:336
  53.1 12.4 %collective-permute-start.6 = (bf16[1536,128]{1,0:T(8,128)(2,1)S(1)}, bf16[1536,128]{1,0:T(8,128)(2,1)S(1)}, u32[]{:S(2)}, u32[]{:S(2)}) collective-permute-start(bf16[1536,128]{1,0:T(8,128)(2,1)S(1)} %collective-permute-done.4.refs_2_), channel_id=1, source_target_pairs={{0,224},{32,0},{64,32},{96,64},{128,96},{160,128},{192,160},{224,1... | collective-permute-start | bytes 1179656 | tf_op jit(solution)/shard_map/ppermute | solution.py:336
  65.6 20.8 %collective-permute-start.10 = (bf16[1536,128]{1,0:T(8,128)(2,1)S(1)}, bf16[1536,128]{1,0:T(8,128)(2,1)S(1)}, u32[]{:S(2)}, u32[]{:S(2)}) collective-permute-start(bf16[1536,128]{1,0:T(8,128)(2,1)S(1)} %collective-permute-done.5.refs_1_), channel_id=1, source_target_pairs={{0,32},{32,64},{64,96},{96,128},{128,160},{160,192},{192,224},{224... | collective-permute-start | bytes 1179656 | tf_op jit(solution)/shard_map/ppermute | solution.py:336
  69.2 2.6 %copy-start.7 = (bf16[304,2048]{1,0:T(8,128)(2,1)}, bf16[304,2048]{1,0:T(8,128)(2,1)S(1)}, u32[]{:S(2)}) copy-start(bf16[304,2048]{1,0:T(8,128)(2,1)S(1)} %collective-permute-done.7.refs_2_) | copy-start | bytes 3735556
  69.2 2.6 %copy-start.8 = (bf16[304,2048]{1,0:T(8,128)(2,1)}, bf16[304,2048]{1,0:T(8,128)(2,1)S(1)}, u32[]{:S(2)}) copy-start(bf16[304,2048]{1,0:T(8,128)(2,1)S(1)} %collective-permute-done.8.refs_4_) | copy-start | bytes 3735556
  69.2 26.8 %copy-start.9 = (bf16[304,2048]{1,0:T(8,128)(2,1)}, bf16[304,2048]{1,0:T(8,128)(2,1)S(1)}, u32[]{:S(2)}) copy-start(bf16[304,2048]{1,0:T(8,128)(2,1)S(1)} %collective-permute-done.9.refs_1_) | copy-start | bytes 3735556
  69.2 31.9 %collective-permute-start.14 = (bf16[304,2048]{1,0:T(8,128)(2,1)S(1)}, bf16[304,2048]{1,0:T(8,128)(2,1)S(1)}, u32[]{:S(2)}, u32[]{:S(2)}) collective-permute-start(bf16[304,2048]{1,0:T(8,128)(2,1)S(1)} %collective-permute-done.7.refs_2_), channel_id=1, source_target_pairs={{0,1},{1,0},{2,3},{3,2},{4,5},{5,4},{6,7},{7,6},{8,9},{9,8},{10,11... | collective-permute-start | bytes 3735560 | tf_op jit(solution)/shard_map/ppermute | solution.py:332
  69.5 31.6 %collective-permute-start.15 = (bf16[304,2048]{1,0:T(8,128)(2,1)S(1)}, bf16[304,2048]{1,0:T(8,128)(2,1)S(1)}, u32[]{:S(2)}, u32[]{:S(2)}) collective-permute-start(bf16[304,2048]{1,0:T(8,128)(2,1)S(1)} %collective-permute-done.8.refs_4_), channel_id=1, source_target_pairs={{0,1},{1,0},{2,3},{3,2},{4,5},{5,4},{6,7},{7,6},{8,9},{9,8},{10,11... | collective-permute-start | bytes 3735560 | tf_op jit(solution)/shard_map/ppermute | solution.py:332
  70.0 26.0 %collective-permute-start.11 = (bf16[1536,128]{1,0:T(8,128)(2,1)S(1)}, bf16[1536,128]{1,0:T(8,128)(2,1)S(1)}, u32[]{:S(2)}, u32[]{:S(2)}) collective-permute-start(bf16[1536,128]{1,0:T(8,128)(2,1)S(1)} %collective-permute-done.6.refs_2_), channel_id=1, source_target_pairs={{0,224},{32,0},{64,32},{96,64},{128,96},{160,128},{192,160},{224,1... | collective-permute-start | bytes 1179656 | tf_op jit(solution)/shard_map/ppermute | solution.py:336
  71.8 29.3 %collective-permute-start.12 = (bf16[160,2048]{1,0:T(8,128)(2,1)S(1)}, bf16[160,2048]{1,0:T(8,128)(2,1)S(1)}, u32[]{:S(2)}, u32[]{:S(2)}) collective-permute-start(bf16[160,2048]{1,0:T(8,128)(2,1)S(1)} %slice.12), channel_id=1, source_target_pairs={{0,2},{2,4},{4,6},{6,0},{1,3},{3,5},{5,7},{7,1},{8,10},{10,12},{12... | collective-permute-start | bytes 1966088 | tf_op jit(solution)/shard_map/ppermute | solution.py:336
  86.4 13.1 %collective-permute-start.13 = (bf16[144,2048]{1,0:T(8,128)(2,1)S(1)}, bf16[144,2048]{1,0:T(8,128)(2,1)S(1)}, u32[]{:S(2)}, u32[]{:S(2)}) collective-permute-start(bf16[144,2048]{1,0:T(8,128)(2,1)S(1)} %slice.13), channel_id=1, source_target_pairs={{0,6},{2,0},{4,2},{6,4},{1,7},{3,1},{5,3},{7,5},{8,14},{10,8},{12,... | collective-permute-start | bytes 1769480 | tf_op jit(solution)/shard_map/ppermute | solution.py:336
  96.0 12.8 %collective-permute-start.16 = (bf16[768,128]{1,0:T(8,128)(2,1)S(1)}, bf16[768,128]{1,0:T(8,128)(2,1)S(1)}, u32[]{:S(2)}, u32[]{:S(2)}) collective-permute-start(bf16[768,128]{1,0:T(8,128)(2,1)S(1)} %slice.14), channel_id=1, source_target_pairs={{0,32},{32,64},{64,96},{96,128},{128,160},{160,192},{192,224},{224... | collective-permute-start | bytes 589832 | tf_op jit(solution)/shard_map/ppermute | solution.py:336
  99.5 9.3 %copy-start.14 = (bf16[144,2048]{1,0:T(8,128)(2,1)}, bf16[144,2048]{1,0:T(8,128)(2,1)S(1)}, u32[]{:S(2)}) copy-start(bf16[144,2048]{1,0:T(8,128)(2,1)S(1)} %collective-permute-done.13.refs_8_) | copy-start | bytes 1769476
  99.5 10.8 %collective-permute-start.17 = (bf16[768,128]{1,0:T(8,128)(2,1)S(1)}, bf16[768,128]{1,0:T(8,128)(2,1)S(1)}, u32[]{:S(2)}, u32[]{:S(2)}) collective-permute-start(bf16[768,128]{1,0:T(8,128)(2,1)S(1)} %slice.15), channel_id=1, source_target_pairs={{0,224},{32,0},{64,32},{96,64},{128,96},{160,128},{192,160},{224,1... | collective-permute-start | bytes 589832 | tf_op jit(solution)/shard_map/ppermute | solution.py:336
  101.1 7.7 %copy-start.12 = (bf16[160,2048]{1,0:T(8,128)(2,1)}, bf16[160,2048]{1,0:T(8,128)(2,1)S(1)}, u32[]{:S(2)}) copy-start(bf16[160,2048]{1,0:T(8,128)(2,1)S(1)} %collective-permute-done.12.refs_6_) | copy-start | bytes 1966084
  101.1 7.7 %copy-start.10 = (bf16[304,2048]{1,0:T(8,128)(2,1)}, bf16[304,2048]{1,0:T(8,128)(2,1)S(1)}, u32[]{:S(2)}) copy-start(bf16[304,2048]{1,0:T(8,128)(2,1)S(1)} %collective-permute-done.14.refs_3_) | copy-start | bytes 3735556
  101.1 7.7 %copy-start.11 = (bf16[304,2048]{1,0:T(8,128)(2,1)}, bf16[304,2048]{1,0:T(8,128)(2,1)S(1)}, u32[]{:S(2)}) copy-start(bf16[304,2048]{1,0:T(8,128)(2,1)S(1)} %collective-permute-done.15.refs_5_) | copy-start | bytes 3735556
  101.1 9.1 %collective-permute-start.18 = (bf16[160,2048]{1,0:T(8,128)(2,1)S(1)}, bf16[160,2048]{1,0:T(8,128)(2,1)S(1)}, u32[]{:S(2)}, u32[]{:S(2)}) collective-permute-start(bf16[160,2048]{1,0:T(8,128)(2,1)S(1)} %collective-permute-done.12.refs_6_), channel_id=1, source_target_pairs={{0,1},{1,0},{2,3},{3,2},{4,5},{5,4},{6,7},{7,6},{8,9},{9,8},{10,11... | collective-permute-start | bytes 1966088 | tf_op jit(solution)/shard_map/ppermute | solution.py:332
  101.2 9.0 %collective-permute-start.19 = (bf16[144,2048]{1,0:T(8,128)(2,1)S(1)}, bf16[144,2048]{1,0:T(8,128)(2,1)S(1)}, u32[]{:S(2)}, u32[]{:S(2)}) collective-permute-start(bf16[144,2048]{1,0:T(8,128)(2,1)S(1)} %collective-permute-done.13.refs_8_), channel_id=1, source_target_pairs={{0,1},{1,0},{2,3},{3,2},{4,5},{5,4},{6,7},{7,6},{8,9},{9,8},{10,11... | collective-permute-start | bytes 1769480 | tf_op jit(solution)/shard_map/ppermute | solution.py:332
  110.2 3.2 %copy-start.15 = (bf16[144,2048]{1,0:T(8,128)(2,1)}, bf16[144,2048]{1,0:T(8,128)(2,1)S(1)}, u32[]{:S(2)}) copy-start(bf16[144,2048]{1,0:T(8,128)(2,1)S(1)} %collective-permute-done.19.refs_9_) | copy-start | bytes 1769476
  110.3 0.8 copy-start.13
  113.5 2.7 %copy-start.6 = (f32[128]{0:T(128)S(1)}, f32[128]{0:T(128)}, u32[]{:S(2)}) copy-start(f32[128]{0:T(128)} %param.16) | copy-start | bytes 1540
  113.5 2.7 %collective-permute-start.20 = (f32[144,1536]{1,0:T(8,128)S(1)}, f32[144,1536]{1,0:T(8,128)S(1)}, u32[]{:S(2)}, u32[]{:S(2)}) collective-permute-start(f32[144,1536]{1,0:T(8,128)S(1)} %attend.11), channel_id=1, source_target_pairs={{0,1},{1,0},{2,3},{3,2},{4,5},{5,4},{6,7},{7,6},{8,9},{9,8},{10,11... | collective-permute-start | bytes 2654216 | tf_op jit(solution)/shard_map/ppermute | solution.py:332
  154.6 14.9 %copy-start.16 = (f32[48,2048]{1,0:T(8,128)S(1)}, f32[48,2048]{1,0:T(8,128)}, u32[]{:S(2)}) copy-start(f32[48,2048]{1,0:T(8,128)} %get-tuple-element.98) | copy-start | bytes 1179652
Sparse Core Ops, SparseCore 0:
  10.1 115.1 all-gather.2

commit v4 on v3

--- a/solution.py
+++ b/solution.py
@@ -86,7 +86,7 @@
         out_specs=whole(parts),
         out_shape=[jax.ShapeDtypeStruct((144, n // parts), F32)] * parts,
         scratch_shapes=[pltpu.VMEM((keys, TQ), F32)] * 2,
-        input_output_aliases={} if first else {len(args) - parts + i: i for i in range(parts)},
+        input_output_aliases={} if first or parts == 1 else {len(args) - parts + i: i for i in range(parts)},
         compiler_params=pltpu.CompilerParams(vmem_limit_bytes=16 * 2**20),
         cost_estimate=pl.CostEstimate(flops=8 * 256 * n * keys, bytes_accessed=2**22, transcendentals=n * keys),
         name="attend",
@@ -142,26 +142,41 @@
     )(*args)
 
 
-def send_body(c_ref, q_ref, k_ref, v_ref, out_ref):
-    put_half(1 - c_ref[0], q_ref, k_ref, v_ref, lambda rows, ref, at: out_ref.__setitem__((rows, slice(None)), ref[at, :]))
-
-
-def put_half(sub, q_ref, k_ref, v_ref, put):
-    for x in range(4):
-        put(slice(48 * x, 48 * (x + 1)), q_ref, pl.ds(pl.multiple_of(96 * x + 48 * sub, 48), 48))
-    for i, ref in ((1, k_ref), (2, v_ref)):
-        put(slice(192 * i, 192 * (i + 1)), ref, pl.ds(pl.multiple_of(192 * sub, 192), 192))
-
-
-def heads_body(c_ref, q_ref, k_ref, v_ref, got_ref, out_ref):
+def send_body(c_ref, q_hbm, k_hbm, v_hbm, own_ref, out_ref, q_ref, k_ref, v_ref, sems):
+    pairs = ((q_hbm, q_ref), (k_hbm, k_ref), (v_hbm, v_ref))
+    copies = [pltpu.make_async_copy(a, b, sems.at[i]) for i, (a, b) in enumerate(pairs)]
+    for copy in copies:
+        copy.start()
+    for copy in copies:
+        copy.wait()
+    c = c_ref[0]
+    for sub, to_ref in ((c, own_ref), (1 - c, out_ref)):
+        for x in range(4):
+            to_ref[48 * x : 48 * (x + 1), :] = q_ref[pl.ds(pl.multiple_of(96 * x + 48 * sub, 48), 48), :]
+        at = pl.ds(pl.multiple_of(192 * sub, 192), 192)
+        to_ref[192:384, :] = k_ref[at, :]
+        to_ref[384:576, :] = v_ref[at, :]
+
+
+def send(core, q, k, v):
+    half = jax.ShapeDtypeStruct((576, 256), BF)
+    return pl.pallas_call(
+        send_body,
+        in_specs=[pl.BlockSpec(memory_space=pltpu.SMEM)] + [pl.BlockSpec(memory_space=pltpu.HBM)] * 3,
+        out_specs=whole(2),
+        out_shape=[half, half],
+        scratch_shapes=[pltpu.VMEM((384, 256), BF)] * 3 + [pltpu.SemaphoreType.DMA((3,))],
+        compiler_params=pltpu.CompilerParams(vmem_limit_bytes=63 * 2**20),
+        cost_estimate=pl.CostEstimate(flops=10**7, bytes_accessed=2**20, transcendentals=0),
+        name="send",
+    )(core, q, k, v)
+
+
+def heads_body(c_ref, own_ref, got_ref, out_ref):
     c = c_ref[0]
     for j in range(2):
         lanes = slice(128 * j, 128 * (j + 1))
-
-        def put(rows, ref, at):
-            out_ref[2 * c + j, rows, :] = ref[at, lanes]
-
-        put_half(c, q_ref, k_ref, v_ref, put)
+        out_ref[2 * c + j] = own_ref[:, lanes]
         out_ref[2 - 2 * c + j] = got_ref[:, lanes]
 
 
@@ -191,9 +206,10 @@
     out_ref[288:304, :] = r_ref[32:48, :]
 
 
-def finish_body(mine_ref, other_ref, lam_ref, gain_ref, out_ref):
+def finish_body(y_ref, c_ref, lam_ref, lam_got_ref, mine_ref, other_ref, gain_ref, out_ref):
     n = 768
-    lam = lam_ref[0]
+    y, c = y_ref[0], c_ref[0]
+    lam = jnp.where(c == y // 2, lam_ref[y % 2], lam_got_ref[y % 2])
     gain = gain_ref[...]
     for t in range(n // 128):
         maps = []
@@ -212,37 +228,43 @@
                 out_ref[at // 192, x, at % 192 : at % 192 + 64, :] = rows[at - 128 * t : at - 128 * t + 64]
 
 
-def finish(mine, other, lam, gain):
+def finish(y, c, lam, lam_got, mine, other, gain):
     return pl.pallas_call(
         finish_body,
-        in_specs=[*whole(2), pl.BlockSpec(memory_space=pltpu.SMEM), *whole(1)],
+        in_specs=[pl.BlockSpec(memory_space=pltpu.SMEM)] * 4 + whole(3),
         out_specs=pl.BlockSpec(memory_space=pltpu.VMEM),
         out_shape=jax.ShapeDtypeStruct((Y, X, 192, 128), BF),
         compiler_params=pltpu.CompilerParams(vmem_limit_bytes=8 * 2**20),
         cost_estimate=pl.CostEstimate(flops=10**8, bytes_accessed=2**21, transcendentals=0),
         name="finish",
-    )(mine, other, lam, gain)
-
-
-def project_body(at_ref, g_ref, gain_ref, *refs):
-    hbm, (normed_ref, own_ref, po, acc, sems) = refs[:10], refs[10:]
-    x, c = at_ref[0], at_ref[1]
+    )(y, c, lam, lam_got, mine, other, gain)
+
+
+def layer_body(x_ref, c_ref, g_ref, gain_ref, *refs):
+    hbm, w_hbm = refs[:10], refs[10]
+    out_ref, own_ref, po, wf, acc, xn, hid, sems = refs[11:]
+    x, c = x_ref[0], c_ref[0]
     copies = []
     for half in range(2):
         lanes = slice(1024 * half, 1024 * (half + 1))
         for i, ref in enumerate(hbm):
             k, rows = (i, slice(0, 304)) if i < 6 else (6 + i % 2, slice(0, 160) if i < 8 else slice(160, 304))
             copies.append(pltpu.make_async_copy(ref.at[:, lanes], po.at[k, rows, lanes], sems.at[10 * half + i]))
-    for copy in copies:
+    chunks = [(c2, a, b) for c2 in range(2) for a, b in ((0, 512), (512, 1024), (1024, 1408))]
+    views = [(slice(None), c2, slice(None), slice(a, b)) for c2, a, b in chunks]
+    views += [(slice(16 * i, 16 * (i + 1)), slice(None), slice(None), slice(1408, 2176)) for i in range(2)]
+    streams = [pltpu.make_async_copy(w_hbm.at[v], wf.at[v], sems.at[20 + i]) for i, v in enumerate(views)]
+    for copy in copies + streams:
         copy.start()
+
     blocks = []
     for k in range(8):
         xk = lax.rem(x + 4 + (0, -1, 1, 2)[k // 2], 4)
         ck = c if k % 2 == 0 else 1 - c
         blocks.append(jnp.concatenate([g_ref[2 * ck, xk], g_ref[2 * ck + 1, xk]], axis=1))
     for half in range(2):
-        for i in range(10):
-            copies[10 * half + i].wait()
+        for copy in copies[10 * half : 10 * half + 10]:
+            copy.wait()
         for n in range(2):
             lanes = slice(1024 * half + 512 * n, 1024 * half + 512 * (n + 1))
             total = None
@@ -260,38 +282,13 @@
     for i in range(6):
         rows = acc[32 * i : 32 * (i + 1), :]
         scale = lax.rsqrt(jnp.mean(rows * rows, axis=1, keepdims=True) + 1e-06)
-        normed_ref[32 * i : 32 * (i + 1), :] = (rows * scale * gain).astype(BF)
-
-
-def project(at, g, gain, blocks):
-    return pl.pallas_call(
-        project_body,
-        in_specs=[pl.BlockSpec(memory_space=pltpu.SMEM), *whole(2)] + [pl.BlockSpec(memory_space=pltpu.HBM)] * 10,
-        out_specs=whole(2),
-        out_shape=[jax.ShapeDtypeStruct((192, 2048), BF), jax.ShapeDtypeStruct((48, 2048), F32)],
-        scratch_shapes=[
-            pltpu.VMEM((8, 304, 2048), BF),
-            pltpu.VMEM((192, 2048), F32),
-            pltpu.SemaphoreType.DMA((20,)),
-        ],
-        compiler_params=pltpu.CompilerParams(vmem_limit_bytes=62 * 2**20),
-        cost_estimate=pl.CostEstimate(flops=2 * 192 * 2048 * 2048, bytes_accessed=10 * 2**20, transcendentals=0),
-        name="project",
-    )(at, g, gain, *blocks)
-
-
-def mixer_body(x_ref, w_hbm, out_ref, w_ref, hid, sems):
-    chunks = [(c, a, b) for c in range(2) for a, b in ((0, 512), (512, 1024), (1024, 1408))]
-    views = [(slice(None), c, slice(None), slice(a, b)) for c, a, b in chunks]
-    views += [(slice(16 * i, 16 * (i + 1)), slice(None), slice(None), slice(1408, 2176)) for i in range(2)]
-    copies = [pltpu.make_async_copy(w_hbm.at[v], w_ref.at[v], sems.at[i]) for i, v in enumerate(views)]
-    for copy in copies:
-        copy.start()
-    for i, (c, a, b) in enumerate(chunks):
-        copies[i].wait()
-        gu = jnp.dot(x_ref[...], w_ref[:, c, :, a:b].reshape(2048, b - a), preferred_element_type=F32)
+        xn[32 * i : 32 * (i + 1), :] = (rows * scale * gain).astype(BF)
+
+    for i, (c2, a, b) in enumerate(chunks):
+        streams[i].wait()
+        gu = jnp.dot(xn[...], wf[:, c2, :, a:b].reshape(2048, b - a), preferred_element_type=F32)
         n = 256 if b - a == 512 else 128
-        at = 768 * c + a // 2
+        at = 768 * c2 + a // 2
         hid[:, at : at + n] = (jax.nn.silu(gu[:, 0:n]) * gu[:, n : 2 * n]).astype(BF)
         if n == 128:
             tail = gu[:, 256:384]
@@ -299,33 +296,41 @@
             lane = lax.broadcasted_iota(jnp.int32, both.shape, 1)
             hid[:, at + 128 : at + 256] = jnp.where(lane < 64, both, 0.0).astype(BF)
     for half in range(2):
-        copies[6 + half].wait()
+        streams[6 + half].wait()
 
         @pl.loop(2 * half, 2 * half + 2)
         def _(m):
             for part in range(2):
                 total = None
-                for c in range(2):
-                    w = w_ref[pl.ds(8 * m + 4 * part, 4), c, :, 1408:2176].reshape(256, 768)
+                for c2 in range(2):
+                    w = wf[pl.ds(8 * m + 4 * part, 4), c2, :, 1408:2176].reshape(256, 768)
                     d = lax.dot_general(
-                        hid[:, 768 * c : 768 * (c + 1)], w, (((1,), (1,)), ((), ())), preferred_element_type=F32
+                        hid[:, 768 * c2 : 768 * (c2 + 1)], w, (((1,), (1,)), ((), ())), preferred_element_type=F32
                     )
                     total = d if total is None else total + d
                 out_ref[:, pl.ds(pl.multiple_of(512 * m + 256 * part, 256), 256)] = total.astype(BF)
 
 
-def mixer(x, w):
-    rows = x.shape[0]
-    return pl.pallas_call(
-        mixer_body,
-        in_specs=[*whole(1), pl.BlockSpec(memory_space=pltpu.HBM)],
-        out_specs=pl.BlockSpec(memory_space=pltpu.VMEM),
-        out_shape=jax.ShapeDtypeStruct((rows, 2048), BF),
-        scratch_shapes=[pltpu.VMEM(w.shape, BF), pltpu.VMEM((rows, 1536), BF), pltpu.SemaphoreType.DMA((8,))],
+def layer(x, c, g, gain, blocks, w):
+    return pl.pallas_call(
+        layer_body,
+        in_specs=[pl.BlockSpec(memory_space=pltpu.SMEM)] * 2
+        + whole(2)
+        + [pl.BlockSpec(memory_space=pltpu.HBM)] * 11,
+        out_specs=whole(2),
+        out_shape=[jax.ShapeDtypeStruct((192, 2048), BF), jax.ShapeDtypeStruct((48, 2048), F32)],
+        scratch_shapes=[
+            pltpu.VMEM((8, 304, 2048), BF),
+            pltpu.VMEM(w.shape, BF),
+            pltpu.VMEM((192, 2048), F32),
+            pltpu.VMEM((192, 2048), BF),
+            pltpu.VMEM((192, 1536), BF),
+            pltpu.SemaphoreType.DMA((28,)),
+        ],
         compiler_params=pltpu.CompilerParams(vmem_limit_bytes=62 * 2**20),
-        cost_estimate=pl.CostEstimate(flops=6 * rows * 2048 * 1408, bytes_accessed=18 * 2**20, transcendentals=0),
-        name="mixer",
-    )(x, w)
+        cost_estimate=pl.CostEstimate(flops=8 * 192 * 2048 * 2048, bytes_accessed=28 * 2**20, transcendentals=0),
+        name="layer",
+    )(x, c, g, gain, *blocks, w)
 
 
 def swap(v):
@@ -346,26 +351,26 @@
     packed = pack(gate, up, down.T)
     weights = lax.all_gather(packed, ("z", "y", "c"), axis=0, tiled=False).reshape(32, 2, 64, 2176)
 
-    core = c.reshape(1)
-    lam_got = swap(mix_lambda)
-    got = swap(small(send_body, ((576, 256), BF), 1, core, queries, keys, values))
-    heads = small(heads_body, ((Y, 576, 128), BF), 1, core, queries, keys, values, got)
+    core, x, y = c.reshape(1), x.reshape(1), y.reshape(1)
+    after = lax.optimization_barrier
+    kept, sent = send(core, queries, keys, values)
+    heads = small(heads_body, ((Y, 576, 128), BF), 1, core, kept, swap(sent))
     head = exchange(heads, "y")
-    block, q_own = small(block_body, [((1536, 128), BF), ((768, 128), BF)], 0, head)
-    right, left = around(block, 1), around(block, -1)
-    q_all = small(queries_body, ((3072, 128), BF), 0, swap(q_own), q_own)
-    lam4 = jnp.where(c == 0, jnp.concatenate([mix_lambda, lam_got]), jnp.concatenate([lam_got, mix_lambda]))
-    lam = lax.dynamic_slice_in_dim(lam4, y, 1, 0)
-
-    at = jnp.stack([x, c])
-    q_all, lam, at, out_weight, residual = lax.optimization_barrier((q_all, lam, at, out_weight, residual))
+
+    heads, out_weight, residual = after((heads, out_weight, residual))
     carry = small(carry_body, ((304, 2048), BF), 0, out_weight, residual)
     from_left, from_right = around(carry, 1, "x", X), around(carry, -1, "x", X)
     carry_c = swap(carry)
 
+    block, q_own = small(block_body, [((1536, 128), BF), ((768, 128), BF)], 0, head)
+    right, left = around(block, 1), around(block, -1)
+    q_other = swap(q_own)
+    lam_got = swap(mix_lambda)
+    q_all = small(queries_body, ((3072, 128), BF), 0, q_other, q_own)
+    q_all, lam_got = after((q_all, lam_got))
+
     one = [(0, 0, 384), (0, 768, 1152)]
     two = one + [(1, 0, 384), (1, 768, 1152)]
-    after = lax.optimization_barrier
     states = attend(q_all, [block], one, None)
     states, right, left = after((states, right, left))
     right2, left2 = around(right, 1), around(left, -1)
@@ -387,12 +392,11 @@
     other = swap(theirs)
     (own,) = attend(q_all, [last_r, last_l], ends, states[1:], 1, 6)
 
-    attended = finish(own, other, lam, head_gain.reshape(1, 128)).reshape(Y * X, 192, 128)
+    attended = finish(y, core, mix_lambda, lam_got, own, other, head_gain.reshape(1, 128)).reshape(Y * X, 192, 128)
     spread = exchange(attended, ("y", "x")).reshape(Y, X, 192, 128)
     blocks = [carry, carry_c, from_left, left_c, from_right, right_c, far_a, far_a_c, far_b, far_b_c]
     spread, weights = after((spread, weights))
-    rows, after_mix = project(at, spread, norm_gain.reshape(1, 2048), blocks)
-    mixed = mixer(rows, weights)
+    mixed, after_mix = layer(x, core, spread, norm_gain.reshape(1, 2048), blocks, weights)
     mixed = exchange(mixed.reshape(X, 48, 2048), "x").astype(F32).sum(axis=0)
     return (after_mix + 0.5 * mixed).astype(BF)
 

time: 179 us -> 177 us (0.989)
  waiting for transfers between devices: 42 us -> 50.8 us
  blocking collectives: 34.4 us -> 29.9 us
  local copies, waits for them, and re-layouts: 5.62 us -> 3.19 us
  Pallas kernels: 51.4 us -> 49.3 us
    ppermute x12, waiting for transfers between devices: 30.8 us -> 36.6 us  [around(): return lax.ppermute(v, axis, [(i, (i + step) % n) for i in range(n)])]
    all_to_all x2, blocking collectives: 34.4 us -> 29.9 us  [exchange(): return lax.all_to_all(v, axis, split_axis=0, concat_axis=0, tiled=True)]
    all_to_all x1, waiting for transfers between devices: 9.37 us -> 12.4 us  [exchange(): return lax.all_to_all(v, axis, split_axis=0, concat_axis=0, tiled=True)]
    unnamed x36 -> x38, local copies, waits for them, and re-layouts: 4.91 us -> 3.07 us
  transfers between devices with their start and end apart: 23 -> 23, of which waited for: 9 -> 7; matrix products, arithmetic and copies ran while one was open for 1% -> 0% of each run, Pallas kernels for 18% -> 18%
where the time goes in v4:
time: 177 us; the launch traced here: 175 us
  waiting for transfers between devices  50.8 us (29%)
  Pallas kernels  49.3 us (28%)
  blocking collectives  29.9 us (17%)
  starting transfers between devices  27.6 us (16%)
  between operations  13.8 us (8%)
  local copies, waits for them, and re-layouts  3.19 us (2%)
    ppermute x12, waiting for transfers between devices, around(): return lax.ppermute(v, axis, [(i, (i + step) % n) for i in range(n)])  36.6 us
    all_to_all x2, blocking collectives, exchange(): return lax.all_to_all(v, axis, split_axis=0, concat_axis=0, tiled=True)  29.9 us
    pallas_call x6, Pallas kernels, attend(): pl.pallas_call(functools.partial(attend_body, pieces=pieces, first=first,...  29.4 us
    ppermute x12, starting transfers between devices, around(): return lax.ppermute(v, axis, [(i, (i + step) % n) for i in range(n)])  20.3 us
    pallas_call x1, Pallas kernels, layer(): pl.pallas_call(layer_body, in_specs=[pl.BlockSpec(memory_space=pltpu.SMEM...  13.9 us
    all_to_all x1, waiting for transfers between devices, exchange(): return lax.all_to_all(v, axis, split_axis=0, concat_axis=0, tiled=True)  12.4 us
    all_to_all x1, starting transfers between devices, exchange(): return lax.all_to_all(v, axis, split_axis=0, concat_axis=0, tiled=True)  5.35 us
  transfers between devices with their start and end apart: 23, of which 7 were waited for; matrix products, arithmetic and copies ran while one was open for 0% of the time, Pallas kernels for 18%

profile of v4, /device:TPU:8, one launch (start us, length us, event | category | flops | bytes accessed | tf_op | source)
XLA Modules:
  0.0 175.4 jit_solution(17540718026230427916)
XLA Ops:
  6.5 1.8 %pack.1 = bf16[64,2176]{1,0:T(8,128)(2,1)} custom-call(bf16[64,704]{1,0:T(8,128)(2,1)} %gate_hbm.1, bf16[64,704]{1,0:T(8,128)(2,1)} %up_hbm.1, bf16[64,704]{1,0:T(8,128)(2,1)} %bitcast.14), custom_call_target="tpu_custom_call" | custom-call | flops 10000000 | bytes 524288 | tf_op jit(solution)/shard_map/pack/pallas_call | solution.py:116
  8.3 0.0 all-gather.3.cloned.1.call-update
  8.4 2.0 %send.1 = (bf16[576,256]{1,0:T(8,128)(2,1)}, bf16[576,256]{1,0:T(8,128)(2,1)}) custom-call(s32[1]{0:T(128)} %bitcast.1.c_ref, bf16[384,256]{1,0:T(8,128)(2,1)} %q_hbm.1, bf16[384,256]{1,0:T(8,128)(2,1)} %k_hbm.1, bf16[384,256]{1,0:T(8,128)(2,1)} %v_hbm.1), custom_call_target="tpu_custom_call" | custom-call | flops 10000000 | bytes 1048576 | tf_op jit(solution)/shard_map/send/pallas_call | solution.py:163
  10.4 0.1 collective-permute-start
  10.5 1.8 %collective-permute-done.got_ref = bf16[576,256]{1,0:T(8,128)(2,1)S(1)} collective-permute-done((bf16[576,256]{1,0:T(8,128)(2,1)}, bf16[576,256]{1,0:T(8,128)(2,1)S(1)}, u32[]{:S(2)}, u32[]{:S(2)}) %collective-permute-start) | collective-permute-done | bytes 294944 | tf_op jit(solution)/shard_map/ppermute | solution.py:337
  12.3 1.0 copy-done.2
  13.2 0.1 shard_map.109
  13.3 14.0 %all_to_all.15.head_ref = bf16[4,576,128]{2,1,0:T(8,128)(2,1)S(1)} all-to-all(bf16[4,576,128]{2,1,0:T(8,128)(2,1)S(1)} %shard_map.109), channel_id=1, replica_groups=mesh['z'=8,'y'=4,'x'=4,'c'=2] {'y'}, dimensions={0} | all-to-all | bytes 1179648 | tf_op jit(solution)/shard_map/all_to_all | solution.py:345
  27.3 0.1 shard_map.110
  27.4 0.1 collective-permute-start.1
  27.5 0.5 collective-permute-start.2
  28.0 0.1 shard_map.112.refs_0_
  28.1 1.5 collective-permute-start.7
  29.6 1.9 %collective-permute-start.8 = (bf16[304,2048]{1,0:T(8,128)(2,1)S(1)}, bf16[304,2048]{1,0:T(8,128)(2,1)S(1)}, u32[]{:S(2)}, u32[]{:S(2)}) collective-permute-start(bf16[304,2048]{1,0:T(8,128)(2,1)S(1)} %shard_map.112.refs_0_), channel_id=1, source_target_pairs={{0,6},{2,0},{4,2},{6,4},{1,7},{3,1},{5,3},{7,5},{8,14},{10,8},{12,... | collective-permute-start | bytes 3735560 | tf_op jit(solution)/shard_map/ppermute | solution.py:341
  31.4 0.0 collective-permute-start.9
  31.4 0.0 collective-permute-done.1.other_ref
  31.4 1.8 %collective-permute-start.3 = (bf16[1536,128]{1,0:T(8,128)(2,1)S(1)}, bf16[1536,128]{1,0:T(8,128)(2,1)S(1)}, u32[]{:S(2)}, u32[]{:S(2)}) collective-permute-start(bf16[1536,128]{1,0:T(8,128)(2,1)S(1)} %get-tuple-element.59.refs_1_), channel_id=1, source_target_pairs={{0,32},{32,64},{64,96},{96,128},{128,160},{160,192},{192,224},{224... | collective-permute-start | bytes 1179656 | tf_op jit(solution)/shard_map/ppermute | solution.py:341
  33.3 0.1 shard_map.111.refs_0_
  33.4 0.0 collective-permute-done.2.lam_got_ref
  33.4 5.6 %collective-permute-start.4 = (bf16[1536,128]{1,0:T(8,128)(2,1)S(1)}, bf16[1536,128]{1,0:T(8,128)(2,1)S(1)}, u32[]{:S(2)}, u32[]{:S(2)}) collective-permute-start(bf16[1536,128]{1,0:T(8,128)(2,1)S(1)} %get-tuple-element.59.refs_1_), channel_id=1, source_target_pairs={{0,224},{32,0},{64,32},{96,64},{128,96},{160,128},{192,160},{224,1... | collective-permute-start | bytes 1179656 | tf_op jit(solution)/shard_map/ppermute | solution.py:341
  39.0 3.8 %attend.6 = (f32[144,1536]{1,0:T(8,128)S(1)}, f32[144,1536]{1,0:T(8,128)S(1)}) custom-call(bf16[3072,128]{1,0:T(8,128)(2,1)S(1)} %shard_map.111.refs_0_, bf16[1536,128]{1,0:T(8,128)(2,1)S(1)} %get-tuple-element.59.refs_1_), custom_call_target="tpu_custom_call" | custom-call | flops 4831838208 | bytes 4194304 | tf_op jit(solution)/shard_map/attend/pallas_call | solution.py:83
  42.9 10.8 %collective-permute-done.3.refs_1_ = bf16[1536,128]{1,0:T(8,128)(2,1)S(1)} collective-permute-done((bf16[1536,128]{1,0:T(8,128)(2,1)S(1)}, bf16[1536,128]{1,0:T(8,128)(2,1)S(1)}, u32[]{:S(2)}, u32[]{:S(2)}) %collective-permute-start.3) | collective-permute-done | bytes 393248 | tf_op jit(solution)/shard_map/ppermute | solution.py:341
  53.6 0.0 collective-permute-done.4.refs_2_
  53.6 0.0 collective-permute-start.5
  53.6 3.2 %collective-permute-start.6 = (bf16[1536,128]{1,0:T(8,128)(2,1)S(1)}, bf16[1536,128]{1,0:T(8,128)(2,1)S(1)}, u32[]{:S(2)}, u32[]{:S(2)}) collective-permute-start(bf16[1536,128]{1,0:T(8,128)(2,1)S(1)} %collective-permute-done.4.refs_2_), channel_id=1, source_target_pairs={{0,224},{32,0},{64,32},{96,64},{128,96},{160,128},{192,160},{224,1... | collective-permute-start | bytes 1179656 | tf_op jit(solution)/shard_map/ppermute | solution.py:341
  56.9 7.1 %attend.7 = (f32[144,1536]{1,0:T(8,128)S(1)}, f32[144,1536]{1,0:T(8,128)S(1)}) custom-call(bf16[3072,128]{1,0:T(8,128)(2,1)S(1)} %shard_map.111.refs_0_, bf16[1536,128]{1,0:T(8,128)(2,1)S(1)} %collective-permute-done.3.refs_1_, bf16[1536,128]{1,0:T(8,128)(2,1)S(1)} %collective-permute-done.4.refs_2_, ...), custom_call_target="tpu_custom_call", output_to_operand_aliasing={{0}: (3, {}), {1}: (4, {})} | custom-call | flops 9663676416 | bytes 4194304 | tf_op jit(solution)/shard_map/attend/pallas_call | solution.py:83
  64.0 2.1 %collective-permute-done.5.refs_1_ = bf16[1536,128]{1,0:T(8,128)(2,1)S(1)} collective-permute-done((bf16[1536,128]{1,0:T(8,128)(2,1)S(1)}, bf16[1536,128]{1,0:T(8,128)(2,1)S(1)}, u32[]{:S(2)}, u32[]{:S(2)}) %collective-permute-start.5) | collective-permute-done | bytes 393248 | tf_op jit(solution)/shard_map/ppermute | solution.py:341
  66.1 0.0 collective-permute-done.6.refs_2_
  66.1 0.9 collective-permute-start.10
  67.0 0.0 collective-permute-done.7.refs_2_
  67.0 0.0 collective-permute-done.8.refs_4_
  67.0 0.0 collective-permute-done.9.refs_1_
  67.0 0.1 collective-permute-start.14
  67.1 0.5 collective-permute-start.15
  67.6 2.3 %collective-permute-start.11 = (bf16[1536,128]{1,0:T(8,128)(2,1)S(1)}, bf16[1536,128]{1,0:T(8,128)(2,1)S(1)}, u32[]{:S(2)}, u32[]{:S(2)}) collective-permute-start(bf16[1536,128]{1,0:T(8,128)(2,1)S(1)} %collective-permute-done.6.refs_2_), channel_id=1, source_target_pairs={{0,224},{32,0},{64,32},{96,64},{128,96},{160,128},{192,160},{224,1... | collective-permute-start | bytes 1179656 | tf_op jit(solution)/shard_map/ppermute | solution.py:341
  70.0 0.1 slice.12
  70.1 0.7 collective-permute-start.12
  70.8 16.3 %collective-permute-done.10.refs_1_ = bf16[1536,128]{1,0:T(8,128)(2,1)S(1)} collective-permute-done((bf16[1536,128]{1,0:T(8,128)(2,1)S(1)}, bf16[1536,128]{1,0:T(8,128)(2,1)S(1)}, u32[]{:S(2)}, u32[]{:S(2)}) %collective-permute-start.10) | collective-permute-done | bytes 393248 | tf_op jit(solution)/shard_map/ppermute | solution.py:341
  87.1 0.9 collective-permute-start.13
  88.0 7.1 %attend.8 = (f32[144,1536]{1,0:T(8,128)S(1)}, f32[144,1536]{1,0:T(8,128)S(1)}) custom-call(bf16[3072,128]{1,0:T(8,128)(2,1)S(1)} %shard_map.111.refs_0_, bf16[1536,128]{1,0:T(8,128)(2,1)S(1)} %collective-permute-done.5.refs_1_, bf16[1536,128]{1,0:T(8,128)(2,1)S(1)} %collective-permute-done.6.refs_2_, ...), custom_call_target="tpu_custom_call", output_to_operand_aliasing={{0}: (3, {}), {1}: (4, {})} | custom-call | flops 9663676416 | bytes 4194304 | tf_op jit(solution)/shard_map/attend/pallas_call | solution.py:83
  95.2 0.1 collective-permute-start.16
  95.3 5.6 %collective-permute-done.13.refs_8_ = bf16[144,2048]{1,0:T(8,128)(2,1)S(1)} collective-permute-done((bf16[144,2048]{1,0:T(8,128)(2,1)S(1)}, bf16[144,2048]{1,0:T(8,128)(2,1)S(1)}, u32[]{:S(2)}, u32[]{:S(2)}) %collective-permute-start.13) | collective-permute-done | bytes 589856 | tf_op jit(solution)/shard_map/ppermute | solution.py:341
  100.9 1.3 collective-permute-start.17
  102.2 0.0 collective-permute-done.15.refs_5_
  102.2 0.1 collective-permute-start.18
  102.3 0.5 collective-permute-start.19
  102.8 7.0 %attend.9 = (f32[144,1536]{1,0:T(8,128)S(1)}, f32[144,1536]{1,0:T(8,128)S(1)}) custom-call(bf16[3072,128]{1,0:T(8,128)(2,1)S(1)} %shard_map.111.refs_0_, bf16[1536,128]{1,0:T(8,128)(2,1)S(1)} %collective-permute-done.10.refs_1_, bf16[1536,128]{1,0:T(8,128)(2,1)S(1)} %collective-permute-done.11.refs_2_, ...), custom_call_target="tpu_custom_call", output_to_operand_aliasing={{0}: (3, {}), {1}: (4, {})} | custom-call | flops 9663676416 | bytes 4194304 | tf_op jit(solution)/shard_map/attend/pallas_call | solution.py:83
  109.9 0.0 collective-permute-done.16.refs_1_
  109.9 1.9 %collective-permute-done.17.refs_2_ = bf16[768,128]{1,0:T(8,128)(2,1)S(1)} collective-permute-done((bf16[768,128]{1,0:T(8,128)(2,1)S(1)}, bf16[768,128]{1,0:T(8,128)(2,1)S(1)}, u32[]{:S(2)}, u32[]{:S(2)}) %collective-permute-start.17) | collective-permute-done | bytes 196640 | tf_op jit(solution)/shard_map/ppermute | solution.py:341
  111.8 0.0 collective-permute-done.19.refs_9_
  111.8 0.0 collective-permute-done.18.refs_7_
  111.8 2.2 %attend.11 = f32[144,1536]{1,0:T(8,128)S(1)} custom-call(bf16[3072,128]{1,0:T(8,128)(2,1)S(1)} %shard_map.111.refs_0_, bf16[768,128]{1,0:T(8,128)(2,1)S(1)} %collective-permute-done.16.refs_1_, bf16[768,128]{1,0:T(8,128)(2,1)S(1)} %collective-permute-done.17.refs_2_, f32[144,1536]{1,0:T(8,128)S(1)} %get-tuple-element.93.refs_3_), custom_call_target="tpu_custom_call" | custom-call | flops 2415919104 | bytes 4194304 | tf_op jit(solution)/shard_map/attend/pallas_call | solution.py:83
  114.0 0.1 collective-permute-start.20
  114.1 1.2 copy-done.7
  115.3 2.2 %attend.10.mine_ref = f32[144,1536]{1,0:T(8,128)S(1)} custom-call(bf16[3072,128]{1,0:T(8,128)(2,1)S(1)} %shard_map.111.refs_0_, bf16[768,128]{1,0:T(8,128)(2,1)S(1)} %collective-permute-done.16.refs_1_, bf16[768,128]{1,0:T(8,128)(2,1)S(1)} %collective-permute-done.17.refs_2_, f32[144,1536]{1,0:T(8,128)S(1)} %copy-done.7), custom_call_target="tpu_custom_call" | custom-call | flops 2415919104 | bytes 4194304 | tf_op jit(solution)/shard_map/attend/pallas_call | solution.py:83
  117.5 0.0 collective-permute-done.20.other_ref
  117.5 1.8 %finish.1 = bf16[4,4,192,128]{3,2,1,0:T(8,128)(2,1)} custom-call(s32[1]{0:T(128)} %bitcast.2.y_ref, s32[1]{0:T(128)} %bitcast.1.c_ref, f32[2]{0:T(128)S(1)} %copy-done.4, f32[2]{0:T(128)S(1)} %collective-permute-done.2.lam_got_ref, f32[144,1536]{1,0:T(8,128)S(1)} %attend.10.mine_ref, f32[144,1536]{1,0:T(8,128)S(1)} %collective-permute-done.20.other_ref, ...), custom_call_target="tpu_custom_call" | custom-call | flops 100000000 | bytes 2097152 | tf_op jit(solution)/shard_map/finish/pallas_call | solution.py:232
  119.3 5.4 %all-to-all-start.1 = ((bf16[16,192,128]{2,1,0:T(8,128)(2,1)}), bf16[16,192,128]{2,1,0:T(8,128)(2,1)S(1)}, u32[]{:S(2)}, u32[]{:S(2)}) async-start(bf16[16,192,128]{2,1,0:T(8,128)(2,1)} %bitcast.4), calls=%async_computation.1 | async-start | bytes 1572864 | tf_op jit(solution)/shard_map/all_to_all | solution.py:345
  124.6 12.4 %all-to-all-done.1 = bf16[16,192,128]{2,1,0:T(8,128)(2,1)S(1)} async-done(((bf16[16,192,128]{2,1,0:T(8,128)(2,1)}), bf16[16,192,128]{2,1,0:T(8,128)(2,1)S(1)}, u32[]{:S(2)}, u32[]{:S(2)}) %all-to-all-start.1) | async-done | bytes 786464 | tf_op jit(solution)/shard_map/all_to_all | solution.py:345
  137.0 0.9 copy-done.8
  137.9 13.9 %layer.1 = (bf16[192,2048]{1,0:T(8,128)(2,1)}, f32[48,2048]{1,0:T(8,128)}) custom-call(s32[1]{0:T(128)} %bitcast.x_ref, s32[1]{0:T(128)} %bitcast.1.c_ref, bf16[4,4,192,128]{3,2,1,0:T(8,128)(2,1)} %bitcast.12, f32[1,2048]{1,0:T(1,128)} %bitcast.15, bf16[304,2048]{1,0:T(8,128)(2,1)} %copy-done, bf16[304,2048]{1,0:T(8,128)(2,1)} %copy-done.11, ...), custom_call_target="tpu_custom_call" | custom-call | flops 6442450944 | bytes 29360128 | tf_op jit(solution)/shard_map/layer/pallas_call | solution.py:315
  151.8 15.9 %all_to_all.16 = bf16[4,48,2048]{2,1,0:T(8,128)(2,1)S(1)} all-to-all(bf16[4,48,2048]{2,1,0:T(8,128)(2,1)} %bitcast.13), channel_id=1, replica_groups=mesh['z'=8,'y'=4,'x'=4,'c'=2] {'x'}, dimensions={0} | all-to-all | bytes 1572864 | tf_op jit(solution)/shard_map/all_to_all | solution.py:345
  167.7 0.1 convert_reduce_fusion
  167.9 0.7 add_convert_fusion
  (43 shorter events, 0.1 us)
Async XLA Ops:
  6.5 130.5 %all-gather.3.cloned.1.call-start = ((), (), s32[]{:S(2)}) async-start(), calls=%async_computation.3 | async-start | bytes 18104320 | tf_op jit(solution)/shard_map/all_gather | solution.py:352
  10.4 1.9 %collective-permute-start = (bf16[576,256]{1,0:T(8,128)(2,1)}, bf16[576,256]{1,0:T(8,128)(2,1)S(1)}, u32[]{:S(2)}, u32[]{:S(2)}) collective-permute-start(bf16[576,256]{1,0:T(8,128)(2,1)} %get-tuple-element.55), channel_id=1, source_target_pairs={{0,1},{1,0},{2,3},{3,2},{4,5},{5,4},{6,7},{7,6},{8,9},{9,8},{10,11... | collective-permute-start | bytes 884744 | tf_op jit(solution)/shard_map/ppermute | solution.py:337
  12.3 1.0 copy-start.2
  13.2 14.3 %copy-start.4 = (f32[2]{0:T(128)S(1)}, f32[2]{0:T(128)}, u32[]{:S(2)}) copy-start(f32[2]{0:T(128)} %lam_ref.1) | copy-start | bytes 28
  13.2 14.8 %copy-start.1 = (bf16[256,2048]{1,0:T(8,128)(2,1)S(1)}, bf16[256,2048]{1,0:T(8,128)(2,1)}, u32[]{:S(2)}) copy-start(bf16[256,2048]{1,0:T(8,128)(2,1)} %w_ref) | copy-start | bytes 3145732
  13.2 14.8 %copy-start.3 = (bf16[48,2048]{1,0:T(8,128)(2,1)S(1)}, bf16[48,2048]{1,0:T(8,128)(2,1)}, u32[]{:S(2)}) copy-start(bf16[48,2048]{1,0:T(8,128)(2,1)} %r_ref) | copy-start | bytes 589828
  27.4 4.0 %collective-permute-start.1 = (bf16[768,128]{1,0:T(8,128)(2,1)S(1)}, bf16[768,128]{1,0:T(8,128)(2,1)S(1)}, u32[]{:S(2)}, u32[]{:S(2)}) collective-permute-start(bf16[768,128]{1,0:T(8,128)(2,1)S(1)} %get-tuple-element.56.own_ref), channel_id=1, source_target_pairs={{0,1},{1,0},{2,3},{3,2},{4,5},{5,4},{6,7},{7,6},{8,9},{9,8},{10,11... | collective-permute-start | bytes 589832 | tf_op jit(solution)/shard_map/ppermute | solution.py:337
  27.5 5.9 %collective-permute-start.2 = (f32[2]{0:T(128)S(1)}, f32[2]{0:T(128)S(1)}, u32[]{:S(2)}, u32[]{:S(2)}) collective-permute-start(f32[2]{0:T(128)S(1)} %copy-done.4), channel_id=1, source_target_pairs={{0,1},{1,0},{2,3},{3,2},{4,5},{5,4},{6,7},{7,6},{8,9},{9,8},{10,11... | collective-permute-start | bytes 32 | tf_op jit(solution)/shard_map/ppermute | solution.py:337
  28.1 14.7 %copy-start = (bf16[304,2048]{1,0:T(8,128)(2,1)}, bf16[304,2048]{1,0:T(8,128)(2,1)S(1)}, u32[]{:S(2)}) copy-start(bf16[304,2048]{1,0:T(8,128)(2,1)S(1)} %shard_map.112.refs_0_) | copy-start | bytes 3735556
  28.1 38.9 %collective-permute-start.7 = (bf16[304,2048]{1,0:T(8,128)(2,1)S(1)}, bf16[304,2048]{1,0:T(8,128)(2,1)S(1)}, u32[]{:S(2)}, u32[]{:S(2)}) collective-permute-start(bf16[304,2048]{1,0:T(8,128)(2,1)S(1)} %shard_map.112.refs_0_), channel_id=1, source_target_pairs={{0,2},{2,4},{4,6},{6,0},{1,3},{3,5},{5,7},{7,1},{8,10},{10,12},{12... | collective-permute-start | bytes 3735560 | tf_op jit(solution)/shard_map/ppermute | solution.py:341
  29.6 37.4 %collective-permute-start.8 = (bf16[304,2048]{1,0:T(8,128)(2,1)S(1)}, bf16[304,2048]{1,0:T(8,128)(2,1)S(1)}, u32[]{:S(2)}, u32[]{:S(2)}) collective-permute-start(bf16[304,2048]{1,0:T(8,128)(2,1)S(1)} %shard_map.112.refs_0_), channel_id=1, source_target_pairs={{0,6},{2,0},{4,2},{6,4},{1,7},{3,1},{5,3},{7,5},{8,14},{10,8},{12,... | collective-permute-start | bytes 3735560 | tf_op jit(solution)/shard_map/ppermute | solution.py:341
  31.4 35.6 %collective-permute-start.9 = (bf16[304,2048]{1,0:T(8,128)(2,1)S(1)}, bf16[304,2048]{1,0:T(8,128)(2,1)S(1)}, u32[]{:S(2)}, u32[]{:S(2)}) collective-permute-start(bf16[304,2048]{1,0:T(8,128)(2,1)S(1)} %shard_map.112.refs_0_), channel_id=1, source_target_pairs={{0,1},{1,0},{2,3},{3,2},{4,5},{5,4},{6,7},{7,6},{8,9},{9,8},{10,11... | collective-permute-start | bytes 3735560 | tf_op jit(solution)/shard_map/ppermute | solution.py:337
  31.4 22.2 %collective-permute-start.3 = (bf16[1536,128]{1,0:T(8,128)(2,1)S(1)}, bf16[1536,128]{1,0:T(8,128)(2,1)S(1)}, u32[]{:S(2)}, u32[]{:S(2)}) collective-permute-start(bf16[1536,128]{1,0:T(8,128)(2,1)S(1)} %get-tuple-element.59.refs_1_), channel_id=1, source_target_pairs={{0,32},{32,64},{64,96},{96,128},{128,160},{160,192},{192,224},{224... | collective-permute-start | bytes 1179656 | tf_op jit(solution)/shard_map/ppermute | solution.py:341
  33.4 20.2 %collective-permute-start.4 = (bf16[1536,128]{1,0:T(8,128)(2,1)S(1)}, bf16[1536,128]{1,0:T(8,128)(2,1)S(1)}, u32[]{:S(2)}, u32[]{:S(2)}) collective-permute-start(bf16[1536,128]{1,0:T(8,128)(2,1)S(1)} %get-tuple-element.59.refs_1_), channel_id=1, source_target_pairs={{0,224},{32,0},{64,32},{96,64},{128,96},{160,128},{192,160},{224,1... | collective-permute-start | bytes 1179656 | tf_op jit(solution)/shard_map/ppermute | solution.py:341
  53.6 12.4 %collective-permute-start.5 = (bf16[1536,128]{1,0:T(8,128)(2,1)S(1)}, bf16[1536,128]{1,0:T(8,128)(2,1)S(1)}, u32[]{:S(2)}, u32[]{:S(2)}) collective-permute-start(bf16[1536,128]{1,0:T(8,128)(2,1)S(1)} %collective-permute-done.3.refs_1_), channel_id=1, source_target_pairs={{0,32},{32,64},{64,96},{96,128},{128,160},{160,192},{192,224},{224... | collective-permute-start | bytes 1179656 | tf_op jit(solution)/shard_map/ppermute | solution.py:341
  53.6 12.4 %collective-permute-start.6 = (bf16[1536,128]{1,0:T(8,128)(2,1)S(1)}, bf16[1536,128]{1,0:T(8,128)(2,1)S(1)}, u32[]{:S(2)}, u32[]{:S(2)}) collective-permute-start(bf16[1536,128]{1,0:T(8,128)(2,1)S(1)} %collective-permute-done.4.refs_2_), channel_id=1, source_target_pairs={{0,224},{32,0},{64,32},{96,64},{128,96},{160,128},{192,160},{224,1... | collective-permute-start | bytes 1179656 | tf_op jit(solution)/shard_map/ppermute | solution.py:341
  66.1 21.0 %collective-permute-start.10 = (bf16[1536,128]{1,0:T(8,128)(2,1)S(1)}, bf16[1536,128]{1,0:T(8,128)(2,1)S(1)}, u32[]{:S(2)}, u32[]{:S(2)}) collective-permute-start(bf16[1536,128]{1,0:T(8,128)(2,1)S(1)} %collective-permute-done.5.refs_1_), channel_id=1, source_target_pairs={{0,32},{32,64},{64,96},{96,128},{128,160},{160,192},{192,224},{224... | collective-permute-start | bytes 1179656 | tf_op jit(solution)/shard_map/ppermute | solution.py:341
  67.0 3.1 %copy-start.9 = (bf16[304,2048]{1,0:T(8,128)(2,1)}, bf16[304,2048]{1,0:T(8,128)(2,1)S(1)}, u32[]{:S(2)}) copy-start(bf16[304,2048]{1,0:T(8,128)(2,1)S(1)} %collective-permute-done.7.refs_2_) | copy-start | bytes 3735556
  67.0 3.1 %copy-start.10 = (bf16[304,2048]{1,0:T(8,128)(2,1)}, bf16[304,2048]{1,0:T(8,128)(2,1)S(1)}, u32[]{:S(2)}) copy-start(bf16[304,2048]{1,0:T(8,128)(2,1)S(1)} %collective-permute-done.8.refs_4_) | copy-start | bytes 3735556
  67.0 28.1 %copy-start.11 = (bf16[304,2048]{1,0:T(8,128)(2,1)}, bf16[304,2048]{1,0:T(8,128)(2,1)S(1)}, u32[]{:S(2)}) copy-start(bf16[304,2048]{1,0:T(8,128)(2,1)S(1)} %collective-permute-done.9.refs_1_) | copy-start | bytes 3735556
  67.0 35.1 %collective-permute-start.14 = (bf16[304,2048]{1,0:T(8,128)(2,1)S(1)}, bf16[304,2048]{1,0:T(8,128)(2,1)S(1)}, u32[]{:S(2)}, u32[]{:S(2)}) collective-permute-start(bf16[304,2048]{1,0:T(8,128)(2,1)S(1)} %collective-permute-done.7.refs_2_), channel_id=1, source_target_pairs={{0,1},{1,0},{2,3},{3,2},{4,5},{5,4},{6,7},{7,6},{8,9},{9,8},{10,11... | collective-permute-start | bytes 3735560 | tf_op jit(solution)/shard_map/ppermute | solution.py:337
  67.1 35.1 %collective-permute-start.15 = (bf16[304,2048]{1,0:T(8,128)(2,1)S(1)}, bf16[304,2048]{1,0:T(8,128)(2,1)S(1)}, u32[]{:S(2)}, u32[]{:S(2)}) collective-permute-start(bf16[304,2048]{1,0:T(8,128)(2,1)S(1)} %collective-permute-done.8.refs_4_), channel_id=1, source_target_pairs={{0,1},{1,0},{2,3},{3,2},{4,5},{5,4},{6,7},{7,6},{8,9},{9,8},{10,11... | collective-permute-start | bytes 3735560 | tf_op jit(solution)/shard_map/ppermute | solution.py:337
  67.6 27.5 %collective-permute-start.11 = (bf16[1536,128]{1,0:T(8,128)(2,1)S(1)}, bf16[1536,128]{1,0:T(8,128)(2,1)S(1)}, u32[]{:S(2)}, u32[]{:S(2)}) collective-permute-start(bf16[1536,128]{1,0:T(8,128)(2,1)S(1)} %collective-permute-done.6.refs_2_), channel_id=1, source_target_pairs={{0,224},{32,0},{64,32},{96,64},{128,96},{160,128},{192,160},{224,1... | collective-permute-start | bytes 1179656 | tf_op jit(solution)/shard_map/ppermute | solution.py:341
  70.1 32.1 %collective-permute-start.12 = (bf16[160,2048]{1,0:T(8,128)(2,1)S(1)}, bf16[160,2048]{1,0:T(8,128)(2,1)S(1)}, u32[]{:S(2)}, u32[]{:S(2)}) collective-permute-start(bf16[160,2048]{1,0:T(8,128)(2,1)S(1)} %slice.12), channel_id=1, source_target_pairs={{0,2},{2,4},{4,6},{6,0},{1,3},{3,5},{5,7},{7,1},{8,10},{10,12},{12... | collective-permute-start | bytes 1966088 | tf_op jit(solution)/shard_map/ppermute | solution.py:341
  87.1 13.7 %collective-permute-start.13 = (bf16[144,2048]{1,0:T(8,128)(2,1)S(1)}, bf16[144,2048]{1,0:T(8,128)(2,1)S(1)}, u32[]{:S(2)}, u32[]{:S(2)}) collective-permute-start(bf16[144,2048]{1,0:T(8,128)(2,1)S(1)} %slice.13), channel_id=1, source_target_pairs={{0,6},{2,0},{4,2},{6,4},{1,7},{3,1},{5,3},{7,5},{8,14},{10,8},{12,... | collective-permute-start | bytes 1769480 | tf_op jit(solution)/shard_map/ppermute | solution.py:341
  95.2 14.8 %collective-permute-start.16 = (bf16[768,128]{1,0:T(8,128)(2,1)S(1)}, bf16[768,128]{1,0:T(8,128)(2,1)S(1)}, u32[]{:S(2)}, u32[]{:S(2)}) collective-permute-start(bf16[768,128]{1,0:T(8,128)(2,1)S(1)} %slice.14), channel_id=1, source_target_pairs={{0,32},{32,64},{64,96},{96,128},{128,160},{160,192},{192,224},{224... | collective-permute-start | bytes 589832 | tf_op jit(solution)/shard_map/ppermute | solution.py:341
  100.8 9.0 %copy-start.16 = (bf16[144,2048]{1,0:T(8,128)(2,1)}, bf16[144,2048]{1,0:T(8,128)(2,1)S(1)}, u32[]{:S(2)}) copy-start(bf16[144,2048]{1,0:T(8,128)(2,1)S(1)} %collective-permute-done.13.refs_8_) | copy-start | bytes 1769476
  100.9 11.0 %collective-permute-start.17 = (bf16[768,128]{1,0:T(8,128)(2,1)S(1)}, bf16[768,128]{1,0:T(8,128)(2,1)S(1)}, u32[]{:S(2)}, u32[]{:S(2)}) collective-permute-start(bf16[768,128]{1,0:T(8,128)(2,1)S(1)} %slice.15), channel_id=1, source_target_pairs={{0,224},{32,0},{64,32},{96,64},{128,96},{160,128},{192,160},{224,1... | collective-permute-start | bytes 589832 | tf_op jit(solution)/shard_map/ppermute | solution.py:341
  102.2 7.7 %copy-start.14 = (bf16[160,2048]{1,0:T(8,128)(2,1)}, bf16[160,2048]{1,0:T(8,128)(2,1)S(1)}, u32[]{:S(2)}) copy-start(bf16[160,2048]{1,0:T(8,128)(2,1)S(1)} %collective-permute-done.12.refs_6_) | copy-start | bytes 1966084
  102.2 7.7 %copy-start.12 = (bf16[304,2048]{1,0:T(8,128)(2,1)}, bf16[304,2048]{1,0:T(8,128)(2,1)S(1)}, u32[]{:S(2)}) copy-start(bf16[304,2048]{1,0:T(8,128)(2,1)S(1)} %collective-permute-done.14.refs_3_) | copy-start | bytes 3735556
  102.2 7.7 %copy-start.13 = (bf16[304,2048]{1,0:T(8,128)(2,1)}, bf16[304,2048]{1,0:T(8,128)(2,1)S(1)}, u32[]{:S(2)}) copy-start(bf16[304,2048]{1,0:T(8,128)(2,1)S(1)} %collective-permute-done.15.refs_5_) | copy-start | bytes 3735556
  102.2 9.6 %collective-permute-start.18 = (bf16[160,2048]{1,0:T(8,128)(2,1)S(1)}, bf16[160,2048]{1,0:T(8,128)(2,1)S(1)}, u32[]{:S(2)}, u32[]{:S(2)}) collective-permute-start(bf16[160,2048]{1,0:T(8,128)(2,1)S(1)} %collective-permute-done.12.refs_6_), channel_id=1, source_target_pairs={{0,1},{1,0},{2,3},{3,2},{4,5},{5,4},{6,7},{7,6},{8,9},{9,8},{10,11... | collective-permute-start | bytes 1966088 | tf_op jit(solution)/shard_map/ppermute | solution.py:337
  102.3 9.5 %collective-permute-start.19 = (bf16[144,2048]{1,0:T(8,128)(2,1)S(1)}, bf16[144,2048]{1,0:T(8,128)(2,1)S(1)}, u32[]{:S(2)}, u32[]{:S(2)}) collective-permute-start(bf16[144,2048]{1,0:T(8,128)(2,1)S(1)} %collective-permute-done.13.refs_8_), channel_id=1, source_target_pairs={{0,1},{1,0},{2,3},{3,2},{4,5},{5,4},{6,7},{7,6},{8,9},{9,8},{10,11... | collective-permute-start | bytes 1769480 | tf_op jit(solution)/shard_map/ppermute | solution.py:337
  109.9 4.1 %copy-start.6 = (f32[144,1536]{1,0:T(8,128)}, f32[144,1536]{1,0:T(8,128)S(1)}, u32[]{:S(2)}) copy-start(f32[144,1536]{1,0:T(8,128)S(1)} %get-tuple-element.92.refs_3_) | copy-start | bytes 2654212
  111.8 2.2 %copy-start.17 = (bf16[144,2048]{1,0:T(8,128)(2,1)}, bf16[144,2048]{1,0:T(8,128)(2,1)S(1)}, u32[]{:S(2)}) copy-start(bf16[144,2048]{1,0:T(8,128)(2,1)S(1)} %collective-permute-done.19.refs_9_) | copy-start | bytes 1769476
  111.8 2.2 %copy-start.15 = (bf16[160,2048]{1,0:T(8,128)(2,1)}, bf16[160,2048]{1,0:T(8,128)(2,1)S(1)}, u32[]{:S(2)}) copy-start(bf16[160,2048]{1,0:T(8,128)(2,1)S(1)} %collective-permute-done.18.refs_7_) | copy-start | bytes 1966084
  114.0 3.5 %collective-permute-start.20 = (f32[144,1536]{1,0:T(8,128)S(1)}, f32[144,1536]{1,0:T(8,128)S(1)}, u32[]{:S(2)}, u32[]{:S(2)}) collective-permute-start(f32[144,1536]{1,0:T(8,128)S(1)} %attend.11), channel_id=1, source_target_pairs={{0,1},{1,0},{2,3},{3,2},{4,5},{5,4},{6,7},{7,6},{8,9},{9,8},{10,11... | collective-permute-start | bytes 2654216 | tf_op jit(solution)/shard_map/ppermute | solution.py:337
  114.1 1.2 copy-start.7
  115.3 2.2 %copy-start.5 = (f32[128]{0:T(128)S(1)}, f32[128]{0:T(128)}, u32[]{:S(2)}) copy-start(f32[128]{0:T(128)} %param.16) | copy-start | bytes 1540
  119.3 17.7 %all-to-all-start.1 = ((bf16[16,192,128]{2,1,0:T(8,128)(2,1)}), bf16[16,192,128]{2,1,0:T(8,128)(2,1)S(1)}, u32[]{:S(2)}, u32[]{:S(2)}) async-start(bf16[16,192,128]{2,1,0:T(8,128)(2,1)} %bitcast.4), calls=%async_computation.1 | async-start | bytes 1572864 | tf_op jit(solution)/shard_map/all_to_all | solution.py:345
  137.0 0.9 copy-start.8
  151.8 16.0 %copy-start.18 = (f32[48,2048]{1,0:T(8,128)S(1)}, f32[48,2048]{1,0:T(8,128)}, u32[]{:S(2)}) copy-start(f32[48,2048]{1,0:T(8,128)} %get-tuple-element.101) | copy-start | bytes 1179652
Sparse Core Ops, SparseCore 0:
  10.1 115.3 all-gather.2

commit v5 on v4

--- a/solution.py
+++ b/solution.py
@@ -200,10 +200,8 @@
 
 
 def carry_body(w_ref, r_ref, out_ref):
-    out_ref[0:128, :] = w_ref[0:128, :]
-    out_ref[128:160, :] = r_ref[0:32, :]
-    out_ref[160:288, :] = w_ref[128:256, :]
-    out_ref[288:304, :] = r_ref[32:48, :]
+    out_ref[0:256, :] = w_ref[...]
+    out_ref[256:304, :] = r_ref[...]
 
 
 def finish_body(y_ref, c_ref, lam_ref, lam_got_ref, mine_ref, other_ref, gain_ref, out_ref):
@@ -240,22 +238,25 @@
     )(y, c, lam, lam_got, mine, other, gain)
 
 
-def layer_body(x_ref, c_ref, g_ref, gain_ref, *refs):
-    hbm, w_hbm = refs[:10], refs[10]
-    out_ref, own_ref, po, wf, acc, xn, hid, sems = refs[11:]
+def layer_body(x_ref, c_ref, *refs):
+    g_hbm, gain_hbm, *hbm = refs[:10]
+    w_hbm, out_hbm, own_hbm, g_ref, gain_ref, out_ref, own_ref, po, wf, acc, xn, hid, sems = refs[10:]
     x, c = x_ref[0], c_ref[0]
     copies = []
     for half in range(2):
         lanes = slice(1024 * half, 1024 * (half + 1))
         for i, ref in enumerate(hbm):
-            k, rows = (i, slice(0, 304)) if i < 6 else (6 + i % 2, slice(0, 160) if i < 8 else slice(160, 304))
-            copies.append(pltpu.make_async_copy(ref.at[:, lanes], po.at[k, rows, lanes], sems.at[10 * half + i]))
+            copies.append(pltpu.make_async_copy(ref.at[:, lanes], po.at[i, :, lanes], sems.at[8 * half + i]))
     chunks = [(c2, a, b) for c2 in range(2) for a, b in ((0, 512), (512, 1024), (1024, 1408))]
     views = [(slice(None), c2, slice(None), slice(a, b)) for c2, a, b in chunks]
     views += [(slice(16 * i, 16 * (i + 1)), slice(None), slice(None), slice(1408, 2176)) for i in range(2)]
-    streams = [pltpu.make_async_copy(w_hbm.at[v], wf.at[v], sems.at[20 + i]) for i, v in enumerate(views)]
-    for copy in copies + streams:
+    streams = [pltpu.make_async_copy(w_hbm.at[v], wf.at[v], sems.at[16 + i]) for i, v in enumerate(views)]
+    rows_in = pltpu.make_async_copy(g_hbm, g_ref, sems.at[24])
+    gain_in = pltpu.make_async_copy(gain_hbm, gain_ref, sems.at[25])
+    for copy in [rows_in, gain_in, *copies, *streams]:
         copy.start()
+    rows_in.wait()
+    gain_in.wait()
 
     blocks = []
     for k in range(8):
@@ -263,21 +264,21 @@
         ck = c if k % 2 == 0 else 1 - c
         blocks.append(jnp.concatenate([g_ref[2 * ck, xk], g_ref[2 * ck + 1, xk]], axis=1))
     for half in range(2):
-        for copy in copies[10 * half : 10 * half + 10]:
+        for copy in copies[8 * half : 8 * half + 8]:
             copy.wait()
         for n in range(2):
             lanes = slice(1024 * half + 512 * n, 1024 * half + 512 * (n + 1))
             total = None
             for k, a in enumerate(blocks):
-                w = jnp.concatenate([po[k, 0:128, lanes], po[k, 160:288, lanes]], axis=0)
-                d = jnp.dot(a, w, preferred_element_type=F32)
+                d = jnp.dot(a, po[k, 0:256, lanes], preferred_element_type=F32)
                 total = d if total is None else total + d
             acc[:, lanes] = total
     for k, step in ((0, 0), (2, -1), (4, 1), (6, 2)):
-        at = 48 * lax.rem(x + 4 + step, 4)
-        acc[pl.ds(pl.multiple_of(at, 16), 32), :] += po[k, 128:160, :].astype(F32)
-        acc[pl.ds(pl.multiple_of(at + 32, 16), 16), :] += po[k, 288:304, :].astype(F32)
+        at = pl.ds(pl.multiple_of(48 * lax.rem(x + 4 + step, 4), 16), 48)
+        acc[at, :] += po[k, 256:304, :].astype(F32)
     own_ref[...] = acc[pl.ds(pl.multiple_of(48 * x, 16), 48), :]
+    own_out = pltpu.make_async_copy(own_ref, own_hbm, sems.at[26])
+    own_out.start()
     gain = gain_ref[...]
     for i in range(6):
         rows = acc[32 * i : 32 * (i + 1), :]
@@ -295,6 +296,7 @@
             both = jax.nn.silu(tail) * pltpu.roll(tail, 64, 1)
             lane = lax.broadcasted_iota(jnp.int32, both.shape, 1)
             hid[:, at + 128 : at + 256] = jnp.where(lane < 64, both, 0.0).astype(BF)
+    outs = []
     for half in range(2):
         streams[6 + half].wait()
 
@@ -310,22 +312,30 @@
                     total = d if total is None else total + d
                 out_ref[:, pl.ds(pl.multiple_of(512 * m + 256 * part, 256), 256)] = total.astype(BF)
 
+        lanes = slice(1024 * half, 1024 * (half + 1))
+        outs.append(pltpu.make_async_copy(out_ref.at[:, lanes], out_hbm.at[:, lanes], sems.at[27 + half]))
+        outs[half].start()
+    for copy in [own_out, *outs]:
+        copy.wait()
+
 
 def layer(x, c, g, gain, blocks, w):
     return pl.pallas_call(
         layer_body,
-        in_specs=[pl.BlockSpec(memory_space=pltpu.SMEM)] * 2
-        + whole(2)
-        + [pl.BlockSpec(memory_space=pltpu.HBM)] * 11,
-        out_specs=whole(2),
+        in_specs=[pl.BlockSpec(memory_space=pltpu.SMEM)] * 2 + [pl.BlockSpec(memory_space=pltpu.HBM)] * 11,
+        out_specs=[pl.BlockSpec(memory_space=pltpu.HBM)] * 2,
         out_shape=[jax.ShapeDtypeStruct((192, 2048), BF), jax.ShapeDtypeStruct((48, 2048), F32)],
         scratch_shapes=[
+            pltpu.VMEM(g.shape, BF),
+            pltpu.VMEM(gain.shape, F32),
+            pltpu.VMEM((192, 2048), BF),
+            pltpu.VMEM((48, 2048), F32),
             pltpu.VMEM((8, 304, 2048), BF),
             pltpu.VMEM(w.shape, BF),
             pltpu.VMEM((192, 2048), F32),
             pltpu.VMEM((192, 2048), BF),
             pltpu.VMEM((192, 1536), BF),
-            pltpu.SemaphoreType.DMA((28,)),
+            pltpu.SemaphoreType.DMA((29,)),
         ],
         compiler_params=pltpu.CompilerParams(vmem_limit_bytes=62 * 2**20),
         cost_estimate=pl.CostEstimate(flops=8 * 192 * 2048 * 2048, bytes_accessed=28 * 2**20, transcendentals=0),
@@ -378,23 +388,23 @@
     states, right2, left2 = after((states, right2, left2))
     right3, left3 = around(right2, 1), around(left2, -1)
     states, from_left, from_right, carry_c = after((states, from_left, from_right, carry_c))
-    far_a, far_b = around(from_left[:160], 1, "x", X), around(from_right[160:], -1, "x", X)
+    far = around(from_left, 1, "x", X)
     left_c, right_c = swap(from_left), swap(from_right)
     states = attend(q_all, [right2, left2], two, states)
     states, right3, left3 = after((states, right3, left3))
     last_r, last_l = around(right3[:768], 1), around(left3[768:], -1)
-    states, far_a, far_b, left_c, right_c = after((states, far_a, far_b, left_c, right_c))
-    far_a_c, far_b_c = swap(far_a), swap(far_b)
     states = attend(q_all, [right3, left3], two, states)
-    states, last_r, last_l, far_a_c, far_b_c = after((states, last_r, last_l, far_a_c, far_b_c))
+    states, last_r, last_l, left_c, right_c = after((states, last_r, last_l, left_c, right_c))
     ends = [(0, 0, 384), (1, 0, 384)]
     (theirs,) = attend(q_all, [last_r, last_l], ends, states[:1], 1)
     other = swap(theirs)
     (own,) = attend(q_all, [last_r, last_l], ends, states[1:], 1, 6)
+    own, far = after((own, far))
+    far_c = swap(far)
 
     attended = finish(y, core, mix_lambda, lam_got, own, other, head_gain.reshape(1, 128)).reshape(Y * X, 192, 128)
     spread = exchange(attended, ("y", "x")).reshape(Y, X, 192, 128)
-    blocks = [carry, carry_c, from_left, left_c, from_right, right_c, far_a, far_a_c, far_b, far_b_c]
+    blocks = [carry, carry_c, from_left, left_c, from_right, right_c, far, far_c]
     spread, weights = after((spread, weights))
     mixed, after_mix = layer(x, core, spread, norm_gain.reshape(1, 2048), blocks, weights)
     mixed = exchange(mixed.reshape(X, 48, 2048), "x").astype(F32).sum(axis=0)

time: 177 us -> 163 us (0.921)
  waiting for transfers between devices: 50.8 us -> 39.8 us
  local copies, waits for them, and re-layouts: 3.19 us -> 1.04 us
    ppermute x12 -> x11, waiting for transfers between devices: 36.6 us -> 24.8 us  [around(): return lax.ppermute(v, axis, [(i, (i + step) % n) for i in range(n)])]
    unnamed x38 -> x26, local copies, waits for them, and re-layouts: 3.07 us -> 1.01 us
    ppermute x12 -> x11, starting transfers between devices: 20.3 us -> 21.4 us  [around(): return lax.ppermute(v, axis, [(i, (i + step) % n) for i in range(n)])]
  transfers between devices with their start and end apart: 23 -> 21, of which waited for: 7 -> 7; matrix products, arithmetic and copies ran while one was open for 0% -> 0% of each run, Pallas kernels for 18% -> 19%
where the time goes in v5:
time: 163 us
  Pallas kernels  48.1 us (30%)
  waiting for transfers between devices  39.8 us (24%)
  blocking collectives  30.6 us (19%)
  starting transfers between devices  28.7 us (18%)
  between operations  13.7 us (8%)
    all_to_all x2, blocking collectives, exchange(): return lax.all_to_all(v, axis, split_axis=0, concat_axis=0, tiled=True)  30.6 us
    pallas_call x6, Pallas kernels, attend(): pl.pallas_call(functools.partial(attend_body, pieces=pieces, first=first,...  29.2 us
    ppermute x11, waiting for transfers between devices, around(): return lax.ppermute(v, axis, [(i, (i + step) % n) for i in range(n)])  24.8 us
    ppermute x11, starting transfers between devices, around(): return lax.ppermute(v, axis, [(i, (i + step) % n) for i in range(n)])  21.4 us
    pallas_call x1, Pallas kernels, layer(): pl.pallas_call(layer_body, in_specs=[pl.BlockSpec(memory_space=pltpu.SMEM...  13 us
    all_to_all x1, waiting for transfers between devices, exchange(): return lax.all_to_all(v, axis, split_axis=0, concat_axis=0, tiled=True)  12 us
    all_to_all x1, starting transfers between devices, exchange(): return lax.all_to_all(v, axis, split_axis=0, concat_axis=0, tiled=True)  5.75 us
  transfers between devices with their start and end apart: 21, of which 7 were waited for; matrix products, arithmetic and copies ran while one was open for 0% of the time, Pallas kernels for 19%

profile of v5, /device:TPU:8, one launch (start us, length us, event | category | flops | bytes accessed | tf_op | source)
XLA Modules:
  0.0 162.7 jit_solution(7001771873742504750)
XLA Ops:
  6.5 1.8 %pack.1 = bf16[64,2176]{1,0:T(8,128)(2,1)} custom-call(bf16[64,704]{1,0:T(8,128)(2,1)} %gate_hbm.1, bf16[64,704]{1,0:T(8,128)(2,1)} %up_hbm.1, bf16[64,704]{1,0:T(8,128)(2,1)} %bitcast.14), custom_call_target="tpu_custom_call" | custom-call | flops 10000000 | bytes 524288 | tf_op jit(solution)/shard_map/pack/pallas_call | solution.py:116
  8.3 0.0 all-gather.3.cloned.1.call-update
  8.4 2.0 %send.1 = (bf16[576,256]{1,0:T(8,128)(2,1)}, bf16[576,256]{1,0:T(8,128)(2,1)}) custom-call(s32[1]{0:T(128)} %bitcast.1.c_ref, bf16[384,256]{1,0:T(8,128)(2,1)} %q_hbm.1, bf16[384,256]{1,0:T(8,128)(2,1)} %k_hbm.1, bf16[384,256]{1,0:T(8,128)(2,1)} %v_hbm.1), custom_call_target="tpu_custom_call" | custom-call | flops 10000000 | bytes 1048576 | tf_op jit(solution)/shard_map/send/pallas_call | solution.py:163
  10.4 0.1 collective-permute-start
  10.5 1.8 %collective-permute-done.got_ref = bf16[576,256]{1,0:T(8,128)(2,1)S(1)} collective-permute-done((bf16[576,256]{1,0:T(8,128)(2,1)}, bf16[576,256]{1,0:T(8,128)(2,1)S(1)}, u32[]{:S(2)}, u32[]{:S(2)}) %collective-permute-start) | collective-permute-done | bytes 294944 | tf_op jit(solution)/shard_map/ppermute | solution.py:347
  12.3 1.0 copy-done.2
  13.2 0.1 shard_map.109
  13.3 14.0 %all_to_all.15.head_ref = bf16[4,576,128]{2,1,0:T(8,128)(2,1)S(1)} all-to-all(bf16[4,576,128]{2,1,0:T(8,128)(2,1)S(1)} %shard_map.109), channel_id=1, replica_groups=mesh['z'=8,'y'=4,'x'=4,'c'=2] {'y'}, dimensions={0} | all-to-all | bytes 1179648 | tf_op jit(solution)/shard_map/all_to_all | solution.py:355
  27.3 0.1 shard_map.110
  27.4 0.1 collective-permute-start.1
  27.5 0.5 collective-permute-start.2
  28.0 0.1 shard_map.112.refs_2_
  28.1 1.5 collective-permute-start.7
  29.6 1.9 %collective-permute-start.8 = (bf16[304,2048]{1,0:T(8,128)(2,1)S(1)}, bf16[304,2048]{1,0:T(8,128)(2,1)S(1)}, u32[]{:S(2)}, u32[]{:S(2)}) collective-permute-start(bf16[304,2048]{1,0:T(8,128)(2,1)S(1)} %shard_map.112.refs_2_), channel_id=1, source_target_pairs={{0,6},{2,0},{4,2},{6,4},{1,7},{3,1},{5,3},{7,5},{8,14},{10,8},{12,... | collective-permute-start | bytes 3735560 | tf_op jit(solution)/shard_map/ppermute | solution.py:351
  31.4 0.0 collective-permute-start.9
  31.4 0.0 collective-permute-done.1.other_ref
  31.4 1.8 %collective-permute-start.3 = (bf16[1536,128]{1,0:T(8,128)(2,1)S(1)}, bf16[1536,128]{1,0:T(8,128)(2,1)S(1)}, u32[]{:S(2)}, u32[]{:S(2)}) collective-permute-start(bf16[1536,128]{1,0:T(8,128)(2,1)S(1)} %get-tuple-element.55.refs_1_), channel_id=1, source_target_pairs={{0,32},{32,64},{64,96},{96,128},{128,160},{160,192},{192,224},{224... | collective-permute-start | bytes 1179656 | tf_op jit(solution)/shard_map/ppermute | solution.py:351
  33.3 0.1 shard_map.111.refs_0_
  33.4 0.0 collective-permute-done.2.lam_got_ref
  33.4 5.6 %collective-permute-start.4 = (bf16[1536,128]{1,0:T(8,128)(2,1)S(1)}, bf16[1536,128]{1,0:T(8,128)(2,1)S(1)}, u32[]{:S(2)}, u32[]{:S(2)}) collective-permute-start(bf16[1536,128]{1,0:T(8,128)(2,1)S(1)} %get-tuple-element.55.refs_1_), channel_id=1, source_target_pairs={{0,224},{32,0},{64,32},{96,64},{128,96},{160,128},{192,160},{224,1... | collective-permute-start | bytes 1179656 | tf_op jit(solution)/shard_map/ppermute | solution.py:351
  39.0 3.8 %attend.6 = (f32[144,1536]{1,0:T(8,128)S(1)}, f32[144,1536]{1,0:T(8,128)S(1)}) custom-call(bf16[3072,128]{1,0:T(8,128)(2,1)S(1)} %shard_map.111.refs_0_, bf16[1536,128]{1,0:T(8,128)(2,1)S(1)} %get-tuple-element.55.refs_1_), custom_call_target="tpu_custom_call" | custom-call | flops 4831838208 | bytes 4194304 | tf_op jit(solution)/shard_map/attend/pallas_call | solution.py:83
  42.8 10.8 %collective-permute-done.3.refs_1_ = bf16[1536,128]{1,0:T(8,128)(2,1)S(1)} collective-permute-done((bf16[1536,128]{1,0:T(8,128)(2,1)S(1)}, bf16[1536,128]{1,0:T(8,128)(2,1)S(1)}, u32[]{:S(2)}, u32[]{:S(2)}) %collective-permute-start.3) | collective-permute-done | bytes 393248 | tf_op jit(solution)/shard_map/ppermute | solution.py:351
  53.6 0.0 collective-permute-done.4.refs_2_
  53.6 0.0 collective-permute-start.5
  53.6 3.2 %collective-permute-start.6 = (bf16[1536,128]{1,0:T(8,128)(2,1)S(1)}, bf16[1536,128]{1,0:T(8,128)(2,1)S(1)}, u32[]{:S(2)}, u32[]{:S(2)}) collective-permute-start(bf16[1536,128]{1,0:T(8,128)(2,1)S(1)} %collective-permute-done.4.refs_2_), channel_id=1, source_target_pairs={{0,224},{32,0},{64,32},{96,64},{128,96},{160,128},{192,160},{224,1... | collective-permute-start | bytes 1179656 | tf_op jit(solution)/shard_map/ppermute | solution.py:351
  56.9 7.1 %attend.7 = (f32[144,1536]{1,0:T(8,128)S(1)}, f32[144,1536]{1,0:T(8,128)S(1)}) custom-call(bf16[3072,128]{1,0:T(8,128)(2,1)S(1)} %shard_map.111.refs_0_, bf16[1536,128]{1,0:T(8,128)(2,1)S(1)} %collective-permute-done.3.refs_1_, bf16[1536,128]{1,0:T(8,128)(2,1)S(1)} %collective-permute-done.4.refs_2_, ...), custom_call_target="tpu_custom_call", output_to_operand_aliasing={{0}: (3, {}), {1}: (4, {})} | custom-call | flops 9663676416 | bytes 4194304 | tf_op jit(solution)/shard_map/attend/pallas_call | solution.py:83
  63.9 2.1 %collective-permute-done.5.refs_1_ = bf16[1536,128]{1,0:T(8,128)(2,1)S(1)} collective-permute-done((bf16[1536,128]{1,0:T(8,128)(2,1)S(1)}, bf16[1536,128]{1,0:T(8,128)(2,1)S(1)}, u32[]{:S(2)}, u32[]{:S(2)}) %collective-permute-start.5) | collective-permute-done | bytes 393248 | tf_op jit(solution)/shard_map/ppermute | solution.py:351
  66.1 0.0 collective-permute-done.6.refs_2_
  66.1 0.9 collective-permute-start.10
  67.0 2.3 %collective-permute-start.11 = (bf16[1536,128]{1,0:T(8,128)(2,1)S(1)}, bf16[1536,128]{1,0:T(8,128)(2,1)S(1)}, u32[]{:S(2)}, u32[]{:S(2)}) collective-permute-start(bf16[1536,128]{1,0:T(8,128)(2,1)S(1)} %collective-permute-done.6.refs_2_), channel_id=1, source_target_pairs={{0,224},{32,0},{64,32},{96,64},{128,96},{160,128},{192,160},{224,1... | collective-permute-start | bytes 1179656 | tf_op jit(solution)/shard_map/ppermute | solution.py:351
  69.3 0.0 collective-permute-done.7.refs_4_
  69.3 0.0 collective-permute-done.8.refs_6_
  69.3 0.0 collective-permute-done.9.refs_3_
  69.4 0.1 collective-permute-start.14
  69.5 0.7 collective-permute-start.16
  70.2 0.1 collective-permute-start.15
  70.3 7.1 %attend.8 = (f32[144,1536]{1,0:T(8,128)S(1)}, f32[144,1536]{1,0:T(8,128)S(1)}) custom-call(bf16[3072,128]{1,0:T(8,128)(2,1)S(1)} %shard_map.111.refs_0_, bf16[1536,128]{1,0:T(8,128)(2,1)S(1)} %collective-permute-done.5.refs_1_, bf16[1536,128]{1,0:T(8,128)(2,1)S(1)} %collective-permute-done.6.refs_2_, ...), custom_call_target="tpu_custom_call", output_to_operand_aliasing={{0}: (3, {}), {1}: (4, {})} | custom-call | flops 9663676416 | bytes 4194304 | tf_op jit(solution)/shard_map/attend/pallas_call | solution.py:83
  77.4 0.0 copy-done.7
  77.4 0.0 copy-done.8
  77.4 9.7 %collective-permute-done.10.refs_1_ = bf16[1536,128]{1,0:T(8,128)(2,1)S(1)} collective-permute-done((bf16[1536,128]{1,0:T(8,128)(2,1)S(1)}, bf16[1536,128]{1,0:T(8,128)(2,1)S(1)}, u32[]{:S(2)}, u32[]{:S(2)}) %collective-permute-start.10) | collective-permute-done | bytes 393248 | tf_op jit(solution)/shard_map/ppermute | solution.py:351
  87.1 0.0 collective-permute-done.11.refs_2_
  87.1 1.3 collective-permute-start.12
  88.4 2.1 %collective-permute-start.13 = (bf16[768,128]{1,0:T(8,128)(2,1)S(1)}, bf16[768,128]{1,0:T(8,128)(2,1)S(1)}, u32[]{:S(2)}, u32[]{:S(2)}) collective-permute-start(bf16[768,128]{1,0:T(8,128)(2,1)S(1)} %slice.7), channel_id=1, source_target_pairs={{0,224},{32,0},{64,32},{96,64},{128,96},{160,128},{192,160},{224,1... | collective-permute-start | bytes 589832 | tf_op jit(solution)/shard_map/ppermute | solution.py:351
  90.6 7.0 %attend.9 = (f32[144,1536]{1,0:T(8,128)S(1)}, f32[144,1536]{1,0:T(8,128)S(1)}) custom-call(bf16[3072,128]{1,0:T(8,128)(2,1)S(1)} %shard_map.111.refs_0_, bf16[1536,128]{1,0:T(8,128)(2,1)S(1)} %collective-permute-done.10.refs_1_, bf16[1536,128]{1,0:T(8,128)(2,1)S(1)} %collective-permute-done.11.refs_2_, ...), custom_call_target="tpu_custom_call", output_to_operand_aliasing={{0}: (3, {}), {1}: (4, {})} | custom-call | flops 9663676416 | bytes 4194304 | tf_op jit(solution)/shard_map/attend/pallas_call | solution.py:83
  97.6 2.1 %collective-permute-done.12.refs_1_ = bf16[768,128]{1,0:T(8,128)(2,1)S(1)} collective-permute-done((bf16[768,128]{1,0:T(8,128)(2,1)S(1)}, bf16[768,128]{1,0:T(8,128)(2,1)S(1)}, u32[]{:S(2)}, u32[]{:S(2)}) %collective-permute-start.12) | collective-permute-done | bytes 196640 | tf_op jit(solution)/shard_map/ppermute | solution.py:351
  99.7 0.0 collective-permute-done.13.refs_2_
  99.7 0.0 collective-permute-done.14.refs_5_
  99.7 0.0 collective-permute-done.15.refs_7_
  99.7 2.1 %attend.11 = f32[144,1536]{1,0:T(8,128)S(1)} custom-call(bf16[3072,128]{1,0:T(8,128)(2,1)S(1)} %shard_map.111.refs_0_, bf16[768,128]{1,0:T(8,128)(2,1)S(1)} %collective-permute-done.12.refs_1_, bf16[768,128]{1,0:T(8,128)(2,1)S(1)} %collective-permute-done.13.refs_2_, f32[144,1536]{1,0:T(8,128)S(1)} %get-tuple-element.86.refs_3_), custom_call_target="tpu_custom_call" | custom-call | flops 2415919104 | bytes 4194304 | tf_op jit(solution)/shard_map/attend/pallas_call | solution.py:83
  101.9 0.0 copy-start.5
  101.9 0.1 collective-permute-start.17
  102.0 2.1 %attend.10.mine_ref = f32[144,1536]{1,0:T(8,128)S(1)} custom-call(bf16[3072,128]{1,0:T(8,128)(2,1)S(1)} %shard_map.111.refs_0_, bf16[768,128]{1,0:T(8,128)(2,1)S(1)} %collective-permute-done.12.refs_1_, bf16[768,128]{1,0:T(8,128)(2,1)S(1)} %collective-permute-done.13.refs_2_, f32[144,1536]{1,0:T(8,128)S(1)} %get-tuple-element.84.refs_3_), custom_call_target="tpu_custom_call" | custom-call | flops 2415919104 | bytes 4194304 | tf_op jit(solution)/shard_map/attend/pallas_call | solution.py:83
  104.1 0.0 collective-permute-done.16.refs_8_
  104.1 0.6 collective-permute-start.18
  104.7 0.0 collective-permute-done.17.other_ref
  104.7 1.8 %finish.1 = bf16[4,4,192,128]{3,2,1,0:T(8,128)(2,1)} custom-call(s32[1]{0:T(128)} %bitcast.2.y_ref, s32[1]{0:T(128)} %bitcast.1.c_ref, f32[2]{0:T(128)S(1)} %copy-done.4, f32[2]{0:T(128)S(1)} %collective-permute-done.2.lam_got_ref, f32[144,1536]{1,0:T(8,128)S(1)} %attend.10.mine_ref, f32[144,1536]{1,0:T(8,128)S(1)} %collective-permute-done.17.other_ref, ...), custom_call_target="tpu_custom_call" | custom-call | flops 100000000 | bytes 2097152 | tf_op jit(solution)/shard_map/finish/pallas_call | solution.py:230
  106.5 5.8 %all-to-all-start.1 = ((bf16[16,192,128]{2,1,0:T(8,128)(2,1)}), bf16[16,192,128]{2,1,0:T(8,128)(2,1)S(1)}, u32[]{:S(2)}, u32[]{:S(2)}) async-start(bf16[16,192,128]{2,1,0:T(8,128)(2,1)} %bitcast.4), calls=%async_computation.1 | async-start | bytes 1572864 | tf_op jit(solution)/shard_map/all_to_all | solution.py:355
  112.3 12.0 %all-to-all-done.1 = bf16[16,192,128]{2,1,0:T(8,128)(2,1)S(1)} async-done(((bf16[16,192,128]{2,1,0:T(8,128)(2,1)}), bf16[16,192,128]{2,1,0:T(8,128)(2,1)S(1)}, u32[]{:S(2)}, u32[]{:S(2)}) %all-to-all-start.1) | async-done | bytes 786464 | tf_op jit(solution)/shard_map/all_to_all | solution.py:355
  124.2 1.2 all-gather.3.cloned.1.call-done
  125.4 0.0 collective-permute-done.18.refs_9_
  125.4 13.0 %layer.1 = (bf16[192,2048]{1,0:T(8,128)(2,1)}, f32[48,2048]{1,0:T(8,128)}) custom-call(s32[1]{0:T(128)} %bitcast.x_ref, s32[1]{0:T(128)} %bitcast.1.c_ref, bf16[4,4,192,128]{3,2,1,0:T(8,128)(2,1)} %bitcast.12, f32[1,2048]{1,0:T(1,128)} %bitcast.15, bf16[304,2048]{1,0:T(8,128)(2,1)} %copy-done, bf16[304,2048]{1,0:T(8,128)(2,1)} %copy-done.9, ...), custom_call_target="tpu_custom_call" | custom-call | flops 6442450944 | bytes 29360128 | tf_op jit(solution)/shard_map/layer/pallas_call | solution.py:323
  138.5 16.6 %all_to_all.16 = bf16[4,48,2048]{2,1,0:T(8,128)(2,1)S(1)} all-to-all(bf16[4,48,2048]{2,1,0:T(8,128)(2,1)} %bitcast.13), channel_id=1, replica_groups=mesh['z'=8,'y'=4,'x'=4,'c'=2] {'x'}, dimensions={0} | all-to-all | bytes 1572864 | tf_op jit(solution)/shard_map/all_to_all | solution.py:355
  155.0 0.1 convert_reduce_fusion
  155.2 0.7 add_convert_fusion
  (25 shorter events, 0.1 us)
Async XLA Ops:
  6.5 118.9 %all-gather.3.cloned.1.call-start = ((), (), s32[]{:S(2)}) async-start(), calls=%async_computation.3 | async-start | bytes 18104320 | tf_op jit(solution)/shard_map/all_gather | solution.py:362
  10.4 1.9 %collective-permute-start = (bf16[576,256]{1,0:T(8,128)(2,1)}, bf16[576,256]{1,0:T(8,128)(2,1)S(1)}, u32[]{:S(2)}, u32[]{:S(2)}) collective-permute-start(bf16[576,256]{1,0:T(8,128)(2,1)} %get-tuple-element.51), channel_id=1, source_target_pairs={{0,1},{1,0},{2,3},{3,2},{4,5},{5,4},{6,7},{7,6},{8,9},{9,8},{10,11... | collective-permute-start | bytes 884744 | tf_op jit(solution)/shard_map/ppermute | solution.py:347
  12.3 1.0 copy-start.2
  13.2 14.3 %copy-start.4 = (f32[2]{0:T(128)S(1)}, f32[2]{0:T(128)}, u32[]{:S(2)}) copy-start(f32[2]{0:T(128)} %lam_ref.1) | copy-start | bytes 28
  13.2 14.8 %copy-start.1 = (bf16[256,2048]{1,0:T(8,128)(2,1)S(1)}, bf16[256,2048]{1,0:T(8,128)(2,1)}, u32[]{:S(2)}) copy-start(bf16[256,2048]{1,0:T(8,128)(2,1)} %w_ref) | copy-start | bytes 3145732
  13.2 14.8 %copy-start.3 = (bf16[48,2048]{1,0:T(8,128)(2,1)S(1)}, bf16[48,2048]{1,0:T(8,128)(2,1)}, u32[]{:S(2)}) copy-start(bf16[48,2048]{1,0:T(8,128)(2,1)} %r_ref) | copy-start | bytes 589828
  27.4 4.0 %collective-permute-start.1 = (bf16[768,128]{1,0:T(8,128)(2,1)S(1)}, bf16[768,128]{1,0:T(8,128)(2,1)S(1)}, u32[]{:S(2)}, u32[]{:S(2)}) collective-permute-start(bf16[768,128]{1,0:T(8,128)(2,1)S(1)} %get-tuple-element.52.own_ref), channel_id=1, source_target_pairs={{0,1},{1,0},{2,3},{3,2},{4,5},{5,4},{6,7},{7,6},{8,9},{9,8},{10,11... | collective-permute-start | bytes 589832 | tf_op jit(solution)/shard_map/ppermute | solution.py:347
  27.5 5.9 %collective-permute-start.2 = (f32[2]{0:T(128)S(1)}, f32[2]{0:T(128)S(1)}, u32[]{:S(2)}, u32[]{:S(2)}) collective-permute-start(f32[2]{0:T(128)S(1)} %copy-done.4), channel_id=1, source_target_pairs={{0,1},{1,0},{2,3},{3,2},{4,5},{5,4},{6,7},{7,6},{8,9},{9,8},{10,11... | collective-permute-start | bytes 32 | tf_op jit(solution)/shard_map/ppermute | solution.py:347
  28.1 14.7 %copy-start = (bf16[304,2048]{1,0:T(8,128)(2,1)}, bf16[304,2048]{1,0:T(8,128)(2,1)S(1)}, u32[]{:S(2)}) copy-start(bf16[304,2048]{1,0:T(8,128)(2,1)S(1)} %shard_map.112.refs_2_) | copy-start | bytes 3735556
  28.1 41.2 %collective-permute-start.7 = (bf16[304,2048]{1,0:T(8,128)(2,1)S(1)}, bf16[304,2048]{1,0:T(8,128)(2,1)S(1)}, u32[]{:S(2)}, u32[]{:S(2)}) collective-permute-start(bf16[304,2048]{1,0:T(8,128)(2,1)S(1)} %shard_map.112.refs_2_), channel_id=1, source_target_pairs={{0,2},{2,4},{4,6},{6,0},{1,3},{3,5},{5,7},{7,1},{8,10},{10,12},{12... | collective-permute-start | bytes 3735560 | tf_op jit(solution)/shard_map/ppermute | solution.py:351
  29.6 39.7 %collective-permute-start.8 = (bf16[304,2048]{1,0:T(8,128)(2,1)S(1)}, bf16[304,2048]{1,0:T(8,128)(2,1)S(1)}, u32[]{:S(2)}, u32[]{:S(2)}) collective-permute-start(bf16[304,2048]{1,0:T(8,128)(2,1)S(1)} %shard_map.112.refs_2_), channel_id=1, source_target_pairs={{0,6},{2,0},{4,2},{6,4},{1,7},{3,1},{5,3},{7,5},{8,14},{10,8},{12,... | collective-permute-start | bytes 3735560 | tf_op jit(solution)/shard_map/ppermute | solution.py:351
  31.4 37.9 %collective-permute-start.9 = (bf16[304,2048]{1,0:T(8,128)(2,1)S(1)}, bf16[304,2048]{1,0:T(8,128)(2,1)S(1)}, u32[]{:S(2)}, u32[]{:S(2)}) collective-permute-start(bf16[304,2048]{1,0:T(8,128)(2,1)S(1)} %shard_map.112.refs_2_), channel_id=1, source_target_pairs={{0,1},{1,0},{2,3},{3,2},{4,5},{5,4},{6,7},{7,6},{8,9},{9,8},{10,11... | collective-permute-start | bytes 3735560 | tf_op jit(solution)/shard_map/ppermute | solution.py:347
  31.4 22.2 %collective-permute-start.3 = (bf16[1536,128]{1,0:T(8,128)(2,1)S(1)}, bf16[1536,128]{1,0:T(8,128)(2,1)S(1)}, u32[]{:S(2)}, u32[]{:S(2)}) collective-permute-start(bf16[1536,128]{1,0:T(8,128)(2,1)S(1)} %get-tuple-element.55.refs_1_), channel_id=1, source_target_pairs={{0,32},{32,64},{64,96},{96,128},{128,160},{160,192},{192,224},{224... | collective-permute-start | bytes 1179656 | tf_op jit(solution)/shard_map/ppermute | solution.py:351
  33.4 20.2 %collective-permute-start.4 = (bf16[1536,128]{1,0:T(8,128)(2,1)S(1)}, bf16[1536,128]{1,0:T(8,128)(2,1)S(1)}, u32[]{:S(2)}, u32[]{:S(2)}) collective-permute-start(bf16[1536,128]{1,0:T(8,128)(2,1)S(1)} %get-tuple-element.55.refs_1_), channel_id=1, source_target_pairs={{0,224},{32,0},{64,32},{96,64},{128,96},{160,128},{192,160},{224,1... | collective-permute-start | bytes 1179656 | tf_op jit(solution)/shard_map/ppermute | solution.py:351
  53.6 12.4 %collective-permute-start.5 = (bf16[1536,128]{1,0:T(8,128)(2,1)S(1)}, bf16[1536,128]{1,0:T(8,128)(2,1)S(1)}, u32[]{:S(2)}, u32[]{:S(2)}) collective-permute-start(bf16[1536,128]{1,0:T(8,128)(2,1)S(1)} %collective-permute-done.3.refs_1_), channel_id=1, source_target_pairs={{0,32},{32,64},{64,96},{96,128},{128,160},{160,192},{192,224},{224... | collective-permute-start | bytes 1179656 | tf_op jit(solution)/shard_map/ppermute | solution.py:351
  53.6 12.4 %collective-permute-start.6 = (bf16[1536,128]{1,0:T(8,128)(2,1)S(1)}, bf16[1536,128]{1,0:T(8,128)(2,1)S(1)}, u32[]{:S(2)}, u32[]{:S(2)}) collective-permute-start(bf16[1536,128]{1,0:T(8,128)(2,1)S(1)} %collective-permute-done.4.refs_2_), channel_id=1, source_target_pairs={{0,224},{32,0},{64,32},{96,64},{128,96},{160,128},{192,160},{224,1... | collective-permute-start | bytes 1179656 | tf_op jit(solution)/shard_map/ppermute | solution.py:351
  66.1 21.0 %collective-permute-start.10 = (bf16[1536,128]{1,0:T(8,128)(2,1)S(1)}, bf16[1536,128]{1,0:T(8,128)(2,1)S(1)}, u32[]{:S(2)}, u32[]{:S(2)}) collective-permute-start(bf16[1536,128]{1,0:T(8,128)(2,1)S(1)} %collective-permute-done.5.refs_1_), channel_id=1, source_target_pairs={{0,32},{32,64},{64,96},{96,128},{128,160},{160,192},{192,224},{224... | collective-permute-start | bytes 1179656 | tf_op jit(solution)/shard_map/ppermute | solution.py:351
  67.0 20.1 %collective-permute-start.11 = (bf16[1536,128]{1,0:T(8,128)(2,1)S(1)}, bf16[1536,128]{1,0:T(8,128)(2,1)S(1)}, u32[]{:S(2)}, u32[]{:S(2)}) collective-permute-start(bf16[1536,128]{1,0:T(8,128)(2,1)S(1)} %collective-permute-done.6.refs_2_), channel_id=1, source_target_pairs={{0,224},{32,0},{64,32},{96,64},{128,96},{160,128},{192,160},{224,1... | collective-permute-start | bytes 1179656 | tf_op jit(solution)/shard_map/ppermute | solution.py:351
  69.3 8.1 %copy-start.7 = (bf16[304,2048]{1,0:T(8,128)(2,1)}, bf16[304,2048]{1,0:T(8,128)(2,1)S(1)}, u32[]{:S(2)}) copy-start(bf16[304,2048]{1,0:T(8,128)(2,1)S(1)} %collective-permute-done.7.refs_4_) | copy-start | bytes 3735556
  69.3 8.1 %copy-start.8 = (bf16[304,2048]{1,0:T(8,128)(2,1)}, bf16[304,2048]{1,0:T(8,128)(2,1)S(1)}, u32[]{:S(2)}) copy-start(bf16[304,2048]{1,0:T(8,128)(2,1)S(1)} %collective-permute-done.8.refs_6_) | copy-start | bytes 3735556
  69.3 8.1 %copy-start.9 = (bf16[304,2048]{1,0:T(8,128)(2,1)}, bf16[304,2048]{1,0:T(8,128)(2,1)S(1)}, u32[]{:S(2)}) copy-start(bf16[304,2048]{1,0:T(8,128)(2,1)S(1)} %collective-permute-done.9.refs_3_) | copy-start | bytes 3735556
  69.4 30.4 %collective-permute-start.14 = (bf16[304,2048]{1,0:T(8,128)(2,1)S(1)}, bf16[304,2048]{1,0:T(8,128)(2,1)S(1)}, u32[]{:S(2)}, u32[]{:S(2)}) collective-permute-start(bf16[304,2048]{1,0:T(8,128)(2,1)S(1)} %collective-permute-done.7.refs_4_), channel_id=1, source_target_pairs={{0,1},{1,0},{2,3},{3,2},{4,5},{5,4},{6,7},{7,6},{8,9},{9,8},{10,11... | collective-permute-start | bytes 3735560 | tf_op jit(solution)/shard_map/ppermute | solution.py:347
  69.5 34.7 %collective-permute-start.16 = (bf16[304,2048]{1,0:T(8,128)(2,1)S(1)}, bf16[304,2048]{1,0:T(8,128)(2,1)}, u32[]{:S(2)}, u32[]{:S(2)}) collective-permute-start(bf16[304,2048]{1,0:T(8,128)(2,1)S(1)} %collective-permute-done.7.refs_4_), channel_id=1, source_target_pairs={{0,2},{2,4},{4,6},{6,0},{1,3},{3,5},{5,7},{7,1},{8,10},{10,12},{12... | collective-permute-start | bytes 3735560 | tf_op jit(solution)/shard_map/ppermute | solution.py:351
  70.2 29.5 %collective-permute-start.15 = (bf16[304,2048]{1,0:T(8,128)(2,1)S(1)}, bf16[304,2048]{1,0:T(8,128)(2,1)S(1)}, u32[]{:S(2)}, u32[]{:S(2)}) collective-permute-start(bf16[304,2048]{1,0:T(8,128)(2,1)S(1)} %collective-permute-done.8.refs_6_), channel_id=1, source_target_pairs={{0,1},{1,0},{2,3},{3,2},{4,5},{5,4},{6,7},{7,6},{8,9},{9,8},{10,11... | collective-permute-start | bytes 3735560 | tf_op jit(solution)/shard_map/ppermute | solution.py:347
  87.1 12.6 %collective-permute-start.12 = (bf16[768,128]{1,0:T(8,128)(2,1)S(1)}, bf16[768,128]{1,0:T(8,128)(2,1)S(1)}, u32[]{:S(2)}, u32[]{:S(2)}) collective-permute-start(bf16[768,128]{1,0:T(8,128)(2,1)S(1)} %slice.6), channel_id=1, source_target_pairs={{0,32},{32,64},{64,96},{96,128},{128,160},{160,192},{192,224},{224... | collective-permute-start | bytes 589832 | tf_op jit(solution)/shard_map/ppermute | solution.py:351
  88.4 11.3 %collective-permute-start.13 = (bf16[768,128]{1,0:T(8,128)(2,1)S(1)}, bf16[768,128]{1,0:T(8,128)(2,1)S(1)}, u32[]{:S(2)}, u32[]{:S(2)}) collective-permute-start(bf16[768,128]{1,0:T(8,128)(2,1)S(1)} %slice.7), channel_id=1, source_target_pairs={{0,224},{32,0},{64,32},{96,64},{128,96},{160,128},{192,160},{224,1... | collective-permute-start | bytes 589832 | tf_op jit(solution)/shard_map/ppermute | solution.py:351
  99.7 2.2 %copy-start.10 = (bf16[304,2048]{1,0:T(8,128)(2,1)}, bf16[304,2048]{1,0:T(8,128)(2,1)S(1)}, u32[]{:S(2)}) copy-start(bf16[304,2048]{1,0:T(8,128)(2,1)S(1)} %collective-permute-done.14.refs_5_) | copy-start | bytes 3735556
  99.7 2.2 %copy-start.11 = (bf16[304,2048]{1,0:T(8,128)(2,1)}, bf16[304,2048]{1,0:T(8,128)(2,1)S(1)}, u32[]{:S(2)}) copy-start(bf16[304,2048]{1,0:T(8,128)(2,1)S(1)} %collective-permute-done.15.refs_7_) | copy-start | bytes 3735556
  101.9 2.8 %copy-start.5 = (f32[128]{0:T(128)S(1)}, f32[128]{0:T(128)}, u32[]{:S(2)}) copy-start(f32[128]{0:T(128)} %param.16) | copy-start | bytes 1540
  101.9 2.8 %collective-permute-start.17 = (f32[144,1536]{1,0:T(8,128)S(1)}, f32[144,1536]{1,0:T(8,128)S(1)}, u32[]{:S(2)}, u32[]{:S(2)}) collective-permute-start(f32[144,1536]{1,0:T(8,128)S(1)} %attend.11), channel_id=1, source_target_pairs={{0,1},{1,0},{2,3},{3,2},{4,5},{5,4},{6,7},{7,6},{8,9},{9,8},{10,11... | collective-permute-start | bytes 2654216 | tf_op jit(solution)/shard_map/ppermute | solution.py:347
  104.1 21.3 %collective-permute-start.18 = (bf16[304,2048]{1,0:T(8,128)(2,1)}, bf16[304,2048]{1,0:T(8,128)(2,1)}, u32[]{:S(2)}, u32[]{:S(2)}) collective-permute-start(bf16[304,2048]{1,0:T(8,128)(2,1)} %collective-permute-done.16.refs_8_), channel_id=1, source_target_pairs={{0,1},{1,0},{2,3},{3,2},{4,5},{5,4},{6,7},{7,6},{8,9},{9,8},{10,11... | collective-permute-start | bytes 3735560 | tf_op jit(solution)/shard_map/ppermute | solution.py:347
  106.5 17.7 %all-to-all-start.1 = ((bf16[16,192,128]{2,1,0:T(8,128)(2,1)}), bf16[16,192,128]{2,1,0:T(8,128)(2,1)S(1)}, u32[]{:S(2)}, u32[]{:S(2)}) async-start(bf16[16,192,128]{2,1,0:T(8,128)(2,1)} %bitcast.4), calls=%async_computation.1 | async-start | bytes 1572864 | tf_op jit(solution)/shard_map/all_to_all | solution.py:355
  124.2 1.2 copy-start.6
  138.4 16.7 %copy-start.12 = (f32[48,2048]{1,0:T(8,128)S(1)}, f32[48,2048]{1,0:T(8,128)}, u32[]{:S(2)}) copy-start(f32[48,2048]{1,0:T(8,128)} %get-tuple-element.93) | copy-start | bytes 1179652
Sparse Core Ops, SparseCore 0:
  10.1 115.3 all-gather.2

commit v6 on v5

--- a/solution.py
+++ b/solution.py
@@ -240,7 +240,8 @@
 
 def layer_body(x_ref, c_ref, *refs):
     g_hbm, gain_hbm, *hbm = refs[:10]
-    w_hbm, out_hbm, own_hbm, g_ref, gain_ref, out_ref, own_ref, po, wf, acc, xn, hid, sems = refs[10:]
+    w_hbm, *out_hbm, own_hbm = refs[10:15]
+    g_ref, gain_ref, out_ref, own_ref, po, wf, acc, xn, hid, sems = refs[15:]
     x, c = x_ref[0], c_ref[0]
     copies = []
     for half in range(2):
@@ -277,8 +278,6 @@
         at = pl.ds(pl.multiple_of(48 * lax.rem(x + 4 + step, 4), 16), 48)
         acc[at, :] += po[k, 256:304, :].astype(F32)
     own_ref[...] = acc[pl.ds(pl.multiple_of(48 * x, 16), 48), :]
-    own_out = pltpu.make_async_copy(own_ref, own_hbm, sems.at[26])
-    own_out.start()
     gain = gain_ref[...]
     for i in range(6):
         rows = acc[32 * i : 32 * (i + 1), :]
@@ -313,9 +312,15 @@
                 out_ref[:, pl.ds(pl.multiple_of(512 * m + 256 * part, 256), 256)] = total.astype(BF)
 
         lanes = slice(1024 * half, 1024 * (half + 1))
-        outs.append(pltpu.make_async_copy(out_ref.at[:, lanes], out_hbm.at[:, lanes], sems.at[27 + half]))
-        outs[half].start()
-    for copy in [own_out, *outs]:
+        for i, step in enumerate((2, 1, -1)):
+            at = pl.ds(pl.multiple_of(48 * lax.rem(x + 4 + step, 4), 16), 48)
+            outs.append(pltpu.make_async_copy(out_ref.at[at, lanes], out_hbm[i].at[:, lanes], sems.at[26 + 3 * half + i]))
+            outs[-1].start()
+        rows = out_ref[pl.ds(pl.multiple_of(48 * x, 16), 48), lanes]
+        own_ref[:, lanes] += 0.5 * rows.astype(F32)
+        outs.append(pltpu.make_async_copy(own_ref.at[:, lanes], own_hbm.at[:, lanes], sems.at[32 + half]))
+        outs[-1].start()
+    for copy in outs:
         copy.wait()
 
 
@@ -323,8 +328,8 @@
     return pl.pallas_call(
         layer_body,
         in_specs=[pl.BlockSpec(memory_space=pltpu.SMEM)] * 2 + [pl.BlockSpec(memory_space=pltpu.HBM)] * 11,
-        out_specs=[pl.BlockSpec(memory_space=pltpu.HBM)] * 2,
-        out_shape=[jax.ShapeDtypeStruct((192, 2048), BF), jax.ShapeDtypeStruct((48, 2048), F32)],
+        out_specs=[pl.BlockSpec(memory_space=pltpu.HBM)] * 4,
+        out_shape=[jax.ShapeDtypeStruct((48, 2048), BF)] * 3 + [jax.ShapeDtypeStruct((48, 2048), F32)],
         scratch_shapes=[
             pltpu.VMEM(g.shape, BF),
             pltpu.VMEM(gain.shape, F32),
@@ -335,7 +340,7 @@
             pltpu.VMEM((192, 2048), F32),
             pltpu.VMEM((192, 2048), BF),
             pltpu.VMEM((192, 1536), BF),
-            pltpu.SemaphoreType.DMA((29,)),
+            pltpu.SemaphoreType.DMA((34,)),
         ],
         compiler_params=pltpu.CompilerParams(vmem_limit_bytes=62 * 2**20),
         cost_estimate=pl.CostEstimate(flops=8 * 192 * 2048 * 2048, bytes_accessed=28 * 2**20, transcendentals=0),
@@ -406,9 +411,10 @@
     spread = exchange(attended, ("y", "x")).reshape(Y, X, 192, 128)
     blocks = [carry, carry_c, from_left, left_c, from_right, right_c, far, far_c]
     spread, weights = after((spread, weights))
-    mixed, after_mix = layer(x, core, spread, norm_gain.reshape(1, 2048), blocks, weights)
-    mixed = exchange(mixed.reshape(X, 48, 2048), "x").astype(F32).sum(axis=0)
-    return (after_mix + 0.5 * mixed).astype(BF)
+    *mixed, base = layer(x, core, spread, norm_gain.reshape(1, 2048), blocks, weights)
+    mixed = [around(m, step, "x", X) for m, step in zip(mixed, (2, 1, -1))]
+    base, total = after((base, sum(m.astype(F32) for m in mixed)))
+    return (base + 0.5 * total).astype(BF)
 
 
 def solution(mesh):

time: 163 us -> 160 us (0.982)
  blocking collectives: 30.6 us -> 14 us
  waiting for transfers between devices: 39.8 us -> 46.7 us
  starting transfers between devices: 28.7 us -> 34.9 us
    all_to_all x2 -> x1, blocking collectives: 30.6 us -> 14 us  [exchange(): return lax.all_to_all(v, axis, split_axis=0, concat_axis=0, tiled=True)]
    ppermute x11 -> x14, waiting for transfers between devices: 24.8 us -> 31.7 us  [around(): return lax.ppermute(v, axis, [(i, (i + step) % n) for i in range(n)])]
    ppermute x11 -> x14, starting transfers between devices: 21.4 us -> 27.3 us  [around(): return lax.ppermute(v, axis, [(i, (i + step) % n) for i in range(n)])]
  transfers between devices with their start and end apart: 21 -> 24, of which waited for: 7 -> 9; matrix products, arithmetic and copies ran while one was open for 0% -> 0% of each run, Pallas kernels for 19% -> 20%
where the time goes in v6:
time: 160 us; the launch traced here: 159 us
  Pallas kernels  48.2 us (30%)
  waiting for transfers between devices  46.7 us (29%)
  starting transfers between devices  34.9 us (22%)
  blocking collectives  14 us (9%)
  between operations  13.7 us (9%)
    ppermute x14, waiting for transfers between devices, around(): return lax.ppermute(v, axis, [(i, (i + step) % n) for i in range(n)])  31.7 us
    pallas_call x6, Pallas kernels, attend(): pl.pallas_call(functools.partial(attend_body, pieces=pieces, first=first,...  29.1 us
    ppermute x14, starting transfers between devices, around(): return lax.ppermute(v, axis, [(i, (i + step) % n) for i in range(n)])  27.3 us
    all_to_all x1, blocking collectives, exchange(): return lax.all_to_all(v, axis, split_axis=0, concat_axis=0, tiled=True)  14 us
    pallas_call x1, Pallas kernels, layer(): pl.pallas_call(layer_body, in_specs=[pl.BlockSpec(memory_space=pltpu.SMEM...  13.1 us
    all_to_all x1, waiting for transfers between devices, exchange(): return lax.all_to_all(v, axis, split_axis=0, concat_axis=0, tiled=True)  12 us
    all_to_all x1, starting transfers between devices, exchange(): return lax.all_to_all(v, axis, split_axis=0, concat_axis=0, tiled=True)  6.01 us
  transfers between devices with their start and end apart: 24, of which 9 were waited for; matrix products, arithmetic and copies ran while one was open for 0% of the time, Pallas kernels for 20%

profile of v6, /device:TPU:8, one launch (start us, length us, event | category | flops | bytes accessed | tf_op | source)
XLA Modules:
  0.0 159.3 jit_solution(2800403388324469827)
XLA Ops:
  6.5 1.8 %pack.1 = bf16[64,2176]{1,0:T(8,128)(2,1)} custom-call(bf16[64,704]{1,0:T(8,128)(2,1)} %gate_hbm.1, bf16[64,704]{1,0:T(8,128)(2,1)} %up_hbm.1, bf16[64,704]{1,0:T(8,128)(2,1)} %bitcast.12), custom_call_target="tpu_custom_call" | custom-call | flops 10000000 | bytes 524288 | tf_op jit(solution)/shard_map/pack/pallas_call | solution.py:116
  8.3 0.0 all-gather.3.cloned.1.call-update
  8.4 2.0 %send.1 = (bf16[576,256]{1,0:T(8,128)(2,1)}, bf16[576,256]{1,0:T(8,128)(2,1)}) custom-call(s32[1]{0:T(128)} %bitcast.1.c_ref, bf16[384,256]{1,0:T(8,128)(2,1)} %q_hbm.1, bf16[384,256]{1,0:T(8,128)(2,1)} %k_hbm.1, bf16[384,256]{1,0:T(8,128)(2,1)} %v_hbm.1), custom_call_target="tpu_custom_call" | custom-call | flops 10000000 | bytes 1048576 | tf_op jit(solution)/shard_map/send/pallas_call | solution.py:163
  10.4 0.1 collective-permute-start
  10.5 1.8 %collective-permute-done.got_ref = bf16[576,256]{1,0:T(8,128)(2,1)S(1)} collective-permute-done((bf16[576,256]{1,0:T(8,128)(2,1)}, bf16[576,256]{1,0:T(8,128)(2,1)S(1)}, u32[]{:S(2)}, u32[]{:S(2)}) %collective-permute-start) | collective-permute-done | bytes 294944 | tf_op jit(solution)/shard_map/ppermute | solution.py:352
  12.3 1.0 copy-done.2
  13.2 0.1 shard_map.109
  13.3 14.0 %all_to_all.10.head_ref = bf16[4,576,128]{2,1,0:T(8,128)(2,1)S(1)} all-to-all(bf16[4,576,128]{2,1,0:T(8,128)(2,1)S(1)} %shard_map.109), channel_id=1, replica_groups=mesh['z'=8,'y'=4,'x'=4,'c'=2] {'y'}, dimensions={0} | all-to-all | bytes 1179648 | tf_op jit(solution)/shard_map/all_to_all | solution.py:360
  27.3 0.1 shard_map.110
  27.4 0.1 collective-permute-start.1
  27.5 0.5 collective-permute-start.2
  28.0 0.1 shard_map.112.refs_2_
  28.1 1.5 collective-permute-start.7
  29.6 1.9 %collective-permute-start.8 = (bf16[304,2048]{1,0:T(8,128)(2,1)S(1)}, bf16[304,2048]{1,0:T(8,128)(2,1)S(1)}, u32[]{:S(2)}, u32[]{:S(2)}) collective-permute-start(bf16[304,2048]{1,0:T(8,128)(2,1)S(1)} %shard_map.112.refs_2_), channel_id=1, source_target_pairs={{0,6},{2,0},{4,2},{6,4},{1,7},{3,1},{5,3},{7,5},{8,14},{10,8},{12,... | collective-permute-start | bytes 3735560 | tf_op jit(solution)/shard_map/ppermute | solution.py:356
  31.4 0.0 collective-permute-start.9
  31.4 0.0 collective-permute-done.1.other_ref
  31.4 1.8 %collective-permute-start.3 = (bf16[1536,128]{1,0:T(8,128)(2,1)S(1)}, bf16[1536,128]{1,0:T(8,128)(2,1)S(1)}, u32[]{:S(2)}, u32[]{:S(2)}) collective-permute-start(bf16[1536,128]{1,0:T(8,128)(2,1)S(1)} %get-tuple-element.59.refs_1_), channel_id=1, source_target_pairs={{0,32},{32,64},{64,96},{96,128},{128,160},{160,192},{192,224},{224... | collective-permute-start | bytes 1179656 | tf_op jit(solution)/shard_map/ppermute | solution.py:356
  33.3 0.1 shard_map.111.refs_0_
  33.4 0.0 collective-permute-done.2.lam_got_ref
  33.4 5.6 %collective-permute-start.4 = (bf16[1536,128]{1,0:T(8,128)(2,1)S(1)}, bf16[1536,128]{1,0:T(8,128)(2,1)S(1)}, u32[]{:S(2)}, u32[]{:S(2)}) collective-permute-start(bf16[1536,128]{1,0:T(8,128)(2,1)S(1)} %get-tuple-element.59.refs_1_), channel_id=1, source_target_pairs={{0,224},{32,0},{64,32},{96,64},{128,96},{160,128},{192,160},{224,1... | collective-permute-start | bytes 1179656 | tf_op jit(solution)/shard_map/ppermute | solution.py:356
  39.0 3.7 %attend.6 = (f32[144,1536]{1,0:T(8,128)S(1)}, f32[144,1536]{1,0:T(8,128)S(1)}) custom-call(bf16[3072,128]{1,0:T(8,128)(2,1)S(1)} %shard_map.111.refs_0_, bf16[1536,128]{1,0:T(8,128)(2,1)S(1)} %get-tuple-element.59.refs_1_), custom_call_target="tpu_custom_call" | custom-call | flops 4831838208 | bytes 4194304 | tf_op jit(solution)/shard_map/attend/pallas_call | solution.py:83
  42.8 10.8 %collective-permute-done.3.refs_1_ = bf16[1536,128]{1,0:T(8,128)(2,1)S(1)} collective-permute-done((bf16[1536,128]{1,0:T(8,128)(2,1)S(1)}, bf16[1536,128]{1,0:T(8,128)(2,1)S(1)}, u32[]{:S(2)}, u32[]{:S(2)}) %collective-permute-start.3) | collective-permute-done | bytes 393248 | tf_op jit(solution)/shard_map/ppermute | solution.py:356
  53.6 0.0 collective-permute-done.4.refs_2_
  53.6 0.0 collective-permute-start.5
  53.6 3.2 %collective-permute-start.6 = (bf16[1536,128]{1,0:T(8,128)(2,1)S(1)}, bf16[1536,128]{1,0:T(8,128)(2,1)S(1)}, u32[]{:S(2)}, u32[]{:S(2)}) collective-permute-start(bf16[1536,128]{1,0:T(8,128)(2,1)S(1)} %collective-permute-done.4.refs_2_), channel_id=1, source_target_pairs={{0,224},{32,0},{64,32},{96,64},{128,96},{160,128},{192,160},{224,1... | collective-permute-start | bytes 1179656 | tf_op jit(solution)/shard_map/ppermute | solution.py:356
  56.8 7.0 %attend.7 = (f32[144,1536]{1,0:T(8,128)S(1)}, f32[144,1536]{1,0:T(8,128)S(1)}) custom-call(bf16[3072,128]{1,0:T(8,128)(2,1)S(1)} %shard_map.111.refs_0_, bf16[1536,128]{1,0:T(8,128)(2,1)S(1)} %collective-permute-done.3.refs_1_, bf16[1536,128]{1,0:T(8,128)(2,1)S(1)} %collective-permute-done.4.refs_2_, ...), custom_call_target="tpu_custom_call", output_to_operand_aliasing={{0}: (3, {}), {1}: (4, {})} | custom-call | flops 9663676416 | bytes 4194304 | tf_op jit(solution)/shard_map/attend/pallas_call | solution.py:83
  63.9 2.0 %collective-permute-done.5.refs_1_ = bf16[1536,128]{1,0:T(8,128)(2,1)S(1)} collective-permute-done((bf16[1536,128]{1,0:T(8,128)(2,1)S(1)}, bf16[1536,128]{1,0:T(8,128)(2,1)S(1)}, u32[]{:S(2)}, u32[]{:S(2)}) %collective-permute-start.5) | collective-permute-done | bytes 393248 | tf_op jit(solution)/shard_map/ppermute | solution.py:356
  65.9 0.0 collective-permute-done.6.refs_2_
  65.9 1.1 collective-permute-start.10
  67.0 2.1 %collective-permute-start.11 = (bf16[1536,128]{1,0:T(8,128)(2,1)S(1)}, bf16[1536,128]{1,0:T(8,128)(2,1)S(1)}, u32[]{:S(2)}, u32[]{:S(2)}) collective-permute-start(bf16[1536,128]{1,0:T(8,128)(2,1)S(1)} %collective-permute-done.6.refs_2_), channel_id=1, source_target_pairs={{0,224},{32,0},{64,32},{96,64},{128,96},{160,128},{192,160},{224,1... | collective-permute-start | bytes 1179656 | tf_op jit(solution)/shard_map/ppermute | solution.py:356
  69.1 0.0 collective-permute-done.7.refs_4_
  69.1 0.0 collective-permute-done.8.refs_6_
  69.2 0.0 collective-permute-done.9.refs_3_
  69.2 0.1 collective-permute-start.14
  69.3 0.9 collective-permute-start.16
  70.2 0.1 collective-permute-start.15
  70.3 7.0 %attend.8 = (f32[144,1536]{1,0:T(8,128)S(1)}, f32[144,1536]{1,0:T(8,128)S(1)}) custom-call(bf16[3072,128]{1,0:T(8,128)(2,1)S(1)} %shard_map.111.refs_0_, bf16[1536,128]{1,0:T(8,128)(2,1)S(1)} %collective-permute-done.5.refs_1_, bf16[1536,128]{1,0:T(8,128)(2,1)S(1)} %collective-permute-done.6.refs_2_, ...), custom_call_target="tpu_custom_call", output_to_operand_aliasing={{0}: (3, {}), {1}: (4, {})} | custom-call | flops 9663676416 | bytes 4194304 | tf_op jit(solution)/shard_map/attend/pallas_call | solution.py:83
  77.4 9.5 %collective-permute-done.10.refs_1_ = bf16[1536,128]{1,0:T(8,128)(2,1)S(1)} collective-permute-done((bf16[1536,128]{1,0:T(8,128)(2,1)S(1)}, bf16[1536,128]{1,0:T(8,128)(2,1)S(1)}, u32[]{:S(2)}, u32[]{:S(2)}) %collective-permute-start.10) | collective-permute-done | bytes 393248 | tf_op jit(solution)/shard_map/ppermute | solution.py:356
  86.9 0.0 collective-permute-done.11.refs_2_
  86.9 1.5 collective-permute-start.12
  88.4 1.9 %collective-permute-start.13 = (bf16[768,128]{1,0:T(8,128)(2,1)S(1)}, bf16[768,128]{1,0:T(8,128)(2,1)S(1)}, u32[]{:S(2)}, u32[]{:S(2)}) collective-permute-start(bf16[768,128]{1,0:T(8,128)(2,1)S(1)} %slice.7), channel_id=1, source_target_pairs={{0,224},{32,0},{64,32},{96,64},{128,96},{160,128},{192,160},{224,1... | collective-permute-start | bytes 589832 | tf_op jit(solution)/shard_map/ppermute | solution.py:356
  90.3 7.0 %attend.9 = (f32[144,1536]{1,0:T(8,128)S(1)}, f32[144,1536]{1,0:T(8,128)S(1)}) custom-call(bf16[3072,128]{1,0:T(8,128)(2,1)S(1)} %shard_map.111.refs_0_, bf16[1536,128]{1,0:T(8,128)(2,1)S(1)} %collective-permute-done.10.refs_1_, bf16[1536,128]{1,0:T(8,128)(2,1)S(1)} %collective-permute-done.11.refs_2_, ...), custom_call_target="tpu_custom_call", output_to_operand_aliasing={{0}: (3, {}), {1}: (4, {})} | custom-call | flops 9663676416 | bytes 4194304 | tf_op jit(solution)/shard_map/attend/pallas_call | solution.py:83
  97.4 2.1 %collective-permute-done.12.refs_1_ = bf16[768,128]{1,0:T(8,128)(2,1)S(1)} collective-permute-done((bf16[768,128]{1,0:T(8,128)(2,1)S(1)}, bf16[768,128]{1,0:T(8,128)(2,1)S(1)}, u32[]{:S(2)}, u32[]{:S(2)}) %collective-permute-start.12) | collective-permute-done | bytes 196640 | tf_op jit(solution)/shard_map/ppermute | solution.py:356
  99.5 0.0 collective-permute-done.15.refs_7_
  99.5 2.1 %attend.11 = f32[144,1536]{1,0:T(8,128)S(1)} custom-call(bf16[3072,128]{1,0:T(8,128)(2,1)S(1)} %shard_map.111.refs_0_, bf16[768,128]{1,0:T(8,128)(2,1)S(1)} %collective-permute-done.12.refs_1_, bf16[768,128]{1,0:T(8,128)(2,1)S(1)} %collective-permute-done.13.refs_2_, f32[144,1536]{1,0:T(8,128)S(1)} %get-tuple-element.90.refs_3_), custom_call_target="tpu_custom_call" | custom-call | flops 2415919104 | bytes 4194304 | tf_op jit(solution)/shard_map/attend/pallas_call | solution.py:83
  101.6 0.0 copy-start.5
  101.6 0.1 collective-permute-start.17
  101.7 2.1 %attend.10.mine_ref = f32[144,1536]{1,0:T(8,128)S(1)} custom-call(bf16[3072,128]{1,0:T(8,128)(2,1)S(1)} %shard_map.111.refs_0_, bf16[768,128]{1,0:T(8,128)(2,1)S(1)} %collective-permute-done.12.refs_1_, bf16[768,128]{1,0:T(8,128)(2,1)S(1)} %collective-permute-done.13.refs_2_, f32[144,1536]{1,0:T(8,128)S(1)} %get-tuple-element.88.refs_3_), custom_call_target="tpu_custom_call" | custom-call | flops 2415919104 | bytes 4194304 | tf_op jit(solution)/shard_map/attend/pallas_call | solution.py:83
  103.9 0.0 collective-permute-done.16.refs_8_
  103.9 0.6 collective-permute-start.18
  104.5 0.0 collective-permute-done.17.other_ref
  104.5 1.8 %finish.1 = bf16[4,4,192,128]{3,2,1,0:T(8,128)(2,1)} custom-call(s32[1]{0:T(128)} %bitcast.2.y_ref, s32[1]{0:T(128)} %bitcast.1.c_ref, f32[2]{0:T(128)S(1)} %copy-done.4, f32[2]{0:T(128)S(1)} %collective-permute-done.2.lam_got_ref, f32[144,1536]{1,0:T(8,128)S(1)} %attend.10.mine_ref, f32[144,1536]{1,0:T(8,128)S(1)} %collective-permute-done.17.other_ref, ...), custom_call_target="tpu_custom_call" | custom-call | flops 100000000 | bytes 2097152 | tf_op jit(solution)/shard_map/finish/pallas_call | solution.py:230
  106.3 6.0 %all-to-all-start.1 = ((bf16[16,192,128]{2,1,0:T(8,128)(2,1)}), bf16[16,192,128]{2,1,0:T(8,128)(2,1)S(1)}, u32[]{:S(2)}, u32[]{:S(2)}) async-start(bf16[16,192,128]{2,1,0:T(8,128)(2,1)} %bitcast.4), calls=%async_computation.1 | async-start | bytes 1572864 | tf_op jit(solution)/shard_map/all_to_all | solution.py:360
  112.3 12.0 %all-to-all-done.1 = bf16[16,192,128]{2,1,0:T(8,128)(2,1)S(1)} async-done(((bf16[16,192,128]{2,1,0:T(8,128)(2,1)}), bf16[16,192,128]{2,1,0:T(8,128)(2,1)S(1)}, u32[]{:S(2)}, u32[]{:S(2)}) %all-to-all-start.1) | async-done | bytes 786464 | tf_op jit(solution)/shard_map/all_to_all | solution.py:360
  124.2 1.2 all-gather.3.cloned.1.call-done
  125.4 13.1 %layer.1 = (bf16[48,2048]{1,0:T(8,128)(2,1)}, bf16[48,2048]{1,0:T(8,128)(2,1)}, bf16[48,2048]{1,0:T(8,128)(2,1)}, f32[48,2048]{1,0:T(8,128)}) custom-call(s32[1]{0:T(128)} %bitcast.x_ref, s32[1]{0:T(128)} %bitcast.1.c_ref, bf16[4,4,192,128]{3,2,1,0:T(8,128)(2,1)} %bitcast.11, f32[1,2048]{1,0:T(1,128)} %bitcast.13, bf16[304,2048]{1,0:T(8,128)(2,1)} %copy-done, ...), custom_call_target="tpu_custom_call" | custom-call | flops 6442450944 | bytes 29360128 | tf_op jit(solution)/shard_map/layer/pallas_call | solution.py:328
  138.6 2.5 %collective-permute-start.19 = (bf16[48,2048]{1,0:T(8,128)(2,1)}, bf16[48,2048]{1,0:T(8,128)(2,1)S(1)}, u32[]{:S(2)}, u32[]{:S(2)}) collective-permute-start(bf16[48,2048]{1,0:T(8,128)(2,1)} %get-tuple-element.98), channel_id=1, source_target_pairs={{0,4},{2,6},{4,0},{6,2},{1,5},{3,7},{5,1},{7,3},{8,12},{10,14},{12... | collective-permute-start | bytes 589832 | tf_op jit(solution)/shard_map/ppermute | solution.py:356
  141.1 0.3 collective-permute-start.20
  141.3 2.9 %collective-permute-start.21 = (bf16[48,2048]{1,0:T(8,128)(2,1)}, bf16[48,2048]{1,0:T(8,128)(2,1)S(1)}, u32[]{:S(2)}, u32[]{:S(2)}) collective-permute-start(bf16[48,2048]{1,0:T(8,128)(2,1)} %get-tuple-element.100), channel_id=1, source_target_pairs={{0,6},{2,0},{4,2},{6,4},{1,7},{3,1},{5,3},{7,5},{8,14},{10,8},{12,... | collective-permute-start | bytes 589832 | tf_op jit(solution)/shard_map/ppermute | solution.py:356
  144.3 3.9 %collective-permute-done.19 = bf16[48,2048]{1,0:T(8,128)(2,1)S(1)} collective-permute-done((bf16[48,2048]{1,0:T(8,128)(2,1)}, bf16[48,2048]{1,0:T(8,128)(2,1)S(1)}, u32[]{:S(2)}, u32[]{:S(2)}) %collective-permute-start.19) | collective-permute-done | bytes 196640 | tf_op jit(solution)/shard_map/ppermute | solution.py:356
  148.2 3.5 %collective-permute-done.20 = bf16[48,2048]{1,0:T(8,128)(2,1)S(1)} collective-permute-done((bf16[48,2048]{1,0:T(8,128)(2,1)}, bf16[48,2048]{1,0:T(8,128)(2,1)S(1)}, u32[]{:S(2)}, u32[]{:S(2)}) %collective-permute-start.20) | collective-permute-done | bytes 196640 | tf_op jit(solution)/shard_map/ppermute | solution.py:356
  151.6 0.0 collective-permute-done.21
  151.6 0.1 convert_add_fusion
  151.7 0.7 add_convert_fusion
  (30 shorter events, 0.1 us)
Async XLA Ops:
  6.5 118.9 %all-gather.3.cloned.1.call-start = ((), (), s32[]{:S(2)}) async-start(), calls=%async_computation.2 | async-start | bytes 18104320 | tf_op jit(solution)/shard_map/all_gather | solution.py:367
  10.4 1.9 %collective-permute-start = (bf16[576,256]{1,0:T(8,128)(2,1)}, bf16[576,256]{1,0:T(8,128)(2,1)S(1)}, u32[]{:S(2)}, u32[]{:S(2)}) collective-permute-start(bf16[576,256]{1,0:T(8,128)(2,1)} %get-tuple-element.55), channel_id=1, source_target_pairs={{0,1},{1,0},{2,3},{3,2},{4,5},{5,4},{6,7},{7,6},{8,9},{9,8},{10,11... | collective-permute-start | bytes 884744 | tf_op jit(solution)/shard_map/ppermute | solution.py:352
  12.3 1.0 copy-start.2
  13.2 14.3 %copy-start.4 = (f32[2]{0:T(128)S(1)}, f32[2]{0:T(128)}, u32[]{:S(2)}) copy-start(f32[2]{0:T(128)} %lam_ref.1) | copy-start | bytes 28
  13.2 14.8 %copy-start.1 = (bf16[256,2048]{1,0:T(8,128)(2,1)S(1)}, bf16[256,2048]{1,0:T(8,128)(2,1)}, u32[]{:S(2)}) copy-start(bf16[256,2048]{1,0:T(8,128)(2,1)} %w_ref) | copy-start | bytes 3145732
  13.2 14.8 %copy-start.3 = (bf16[48,2048]{1,0:T(8,128)(2,1)S(1)}, bf16[48,2048]{1,0:T(8,128)(2,1)}, u32[]{:S(2)}) copy-start(bf16[48,2048]{1,0:T(8,128)(2,1)} %r_ref) | copy-start | bytes 589828
  27.4 4.0 %collective-permute-start.1 = (bf16[768,128]{1,0:T(8,128)(2,1)S(1)}, bf16[768,128]{1,0:T(8,128)(2,1)S(1)}, u32[]{:S(2)}, u32[]{:S(2)}) collective-permute-start(bf16[768,128]{1,0:T(8,128)(2,1)S(1)} %get-tuple-element.56.own_ref), channel_id=1, source_target_pairs={{0,1},{1,0},{2,3},{3,2},{4,5},{5,4},{6,7},{7,6},{8,9},{9,8},{10,11... | collective-permute-start | bytes 589832 | tf_op jit(solution)/shard_map/ppermute | solution.py:352
  27.5 5.9 %collective-permute-start.2 = (f32[2]{0:T(128)S(1)}, f32[2]{0:T(128)S(1)}, u32[]{:S(2)}, u32[]{:S(2)}) collective-permute-start(f32[2]{0:T(128)S(1)} %copy-done.4), channel_id=1, source_target_pairs={{0,1},{1,0},{2,3},{3,2},{4,5},{5,4},{6,7},{7,6},{8,9},{9,8},{10,11... | collective-permute-start | bytes 32 | tf_op jit(solution)/shard_map/ppermute | solution.py:352
  28.1 14.6 %copy-start = (bf16[304,2048]{1,0:T(8,128)(2,1)}, bf16[304,2048]{1,0:T(8,128)(2,1)S(1)}, u32[]{:S(2)}) copy-start(bf16[304,2048]{1,0:T(8,128)(2,1)S(1)} %shard_map.112.refs_2_) | copy-start | bytes 3735556
  28.1 41.0 %collective-permute-start.7 = (bf16[304,2048]{1,0:T(8,128)(2,1)S(1)}, bf16[304,2048]{1,0:T(8,128)(2,1)S(1)}, u32[]{:S(2)}, u32[]{:S(2)}) collective-permute-start(bf16[304,2048]{1,0:T(8,128)(2,1)S(1)} %shard_map.112.refs_2_), channel_id=1, source_target_pairs={{0,2},{2,4},{4,6},{6,0},{1,3},{3,5},{5,7},{7,1},{8,10},{10,12},{12... | collective-permute-start | bytes 3735560 | tf_op jit(solution)/shard_map/ppermute | solution.py:356
  29.6 39.6 %collective-permute-start.8 = (bf16[304,2048]{1,0:T(8,128)(2,1)S(1)}, bf16[304,2048]{1,0:T(8,128)(2,1)S(1)}, u32[]{:S(2)}, u32[]{:S(2)}) collective-permute-start(bf16[304,2048]{1,0:T(8,128)(2,1)S(1)} %shard_map.112.refs_2_), channel_id=1, source_target_pairs={{0,6},{2,0},{4,2},{6,4},{1,7},{3,1},{5,3},{7,5},{8,14},{10,8},{12,... | collective-permute-start | bytes 3735560 | tf_op jit(solution)/shard_map/ppermute | solution.py:356
  31.4 37.7 %collective-permute-start.9 = (bf16[304,2048]{1,0:T(8,128)(2,1)S(1)}, bf16[304,2048]{1,0:T(8,128)(2,1)S(1)}, u32[]{:S(2)}, u32[]{:S(2)}) collective-permute-start(bf16[304,2048]{1,0:T(8,128)(2,1)S(1)} %shard_map.112.refs_2_), channel_id=1, source_target_pairs={{0,1},{1,0},{2,3},{3,2},{4,5},{5,4},{6,7},{7,6},{8,9},{9,8},{10,11... | collective-permute-start | bytes 3735560 | tf_op jit(solution)/shard_map/ppermute | solution.py:352
  31.4 22.1 %collective-permute-start.3 = (bf16[1536,128]{1,0:T(8,128)(2,1)S(1)}, bf16[1536,128]{1,0:T(8,128)(2,1)S(1)}, u32[]{:S(2)}, u32[]{:S(2)}) collective-permute-start(bf16[1536,128]{1,0:T(8,128)(2,1)S(1)} %get-tuple-element.59.refs_1_), channel_id=1, source_target_pairs={{0,32},{32,64},{64,96},{96,128},{128,160},{160,192},{192,224},{224... | collective-permute-start | bytes 1179656 | tf_op jit(solution)/shard_map/ppermute | solution.py:356
  33.4 20.2 %collective-permute-start.4 = (bf16[1536,128]{1,0:T(8,128)(2,1)S(1)}, bf16[1536,128]{1,0:T(8,128)(2,1)S(1)}, u32[]{:S(2)}, u32[]{:S(2)}) collective-permute-start(bf16[1536,128]{1,0:T(8,128)(2,1)S(1)} %get-tuple-element.59.refs_1_), channel_id=1, source_target_pairs={{0,224},{32,0},{64,32},{96,64},{128,96},{160,128},{192,160},{224,1... | collective-permute-start | bytes 1179656 | tf_op jit(solution)/shard_map/ppermute | solution.py:356
  53.6 12.3 %collective-permute-start.5 = (bf16[1536,128]{1,0:T(8,128)(2,1)S(1)}, bf16[1536,128]{1,0:T(8,128)(2,1)S(1)}, u32[]{:S(2)}, u32[]{:S(2)}) collective-permute-start(bf16[1536,128]{1,0:T(8,128)(2,1)S(1)} %collective-permute-done.3.refs_1_), channel_id=1, source_target_pairs={{0,32},{32,64},{64,96},{96,128},{128,160},{160,192},{192,224},{224... | collective-permute-start | bytes 1179656 | tf_op jit(solution)/shard_map/ppermute | solution.py:356
  53.6 12.3 %collective-permute-start.6 = (bf16[1536,128]{1,0:T(8,128)(2,1)S(1)}, bf16[1536,128]{1,0:T(8,128)(2,1)S(1)}, u32[]{:S(2)}, u32[]{:S(2)}) collective-permute-start(bf16[1536,128]{1,0:T(8,128)(2,1)S(1)} %collective-permute-done.4.refs_2_), channel_id=1, source_target_pairs={{0,224},{32,0},{64,32},{96,64},{128,96},{160,128},{192,160},{224,1... | collective-permute-start | bytes 1179656 | tf_op jit(solution)/shard_map/ppermute | solution.py:356
  65.9 21.0 %collective-permute-start.10 = (bf16[1536,128]{1,0:T(8,128)(2,1)S(1)}, bf16[1536,128]{1,0:T(8,128)(2,1)S(1)}, u32[]{:S(2)}, u32[]{:S(2)}) collective-permute-start(bf16[1536,128]{1,0:T(8,128)(2,1)S(1)} %collective-permute-done.5.refs_1_), channel_id=1, source_target_pairs={{0,32},{32,64},{64,96},{96,128},{128,160},{160,192},{192,224},{224... | collective-permute-start | bytes 1179656 | tf_op jit(solution)/shard_map/ppermute | solution.py:356
  67.0 19.9 %collective-permute-start.11 = (bf16[1536,128]{1,0:T(8,128)(2,1)S(1)}, bf16[1536,128]{1,0:T(8,128)(2,1)S(1)}, u32[]{:S(2)}, u32[]{:S(2)}) collective-permute-start(bf16[1536,128]{1,0:T(8,128)(2,1)S(1)} %collective-permute-done.6.refs_2_), channel_id=1, source_target_pairs={{0,224},{32,0},{64,32},{96,64},{128,96},{160,128},{192,160},{224,1... | collective-permute-start | bytes 1179656 | tf_op jit(solution)/shard_map/ppermute | solution.py:356
  69.1 8.2 %copy-start.7 = (bf16[304,2048]{1,0:T(8,128)(2,1)}, bf16[304,2048]{1,0:T(8,128)(2,1)S(1)}, u32[]{:S(2)}) copy-start(bf16[304,2048]{1,0:T(8,128)(2,1)S(1)} %collective-permute-done.7.refs_4_) | copy-start | bytes 3735556
  69.2 8.3 %copy-start.8 = (bf16[304,2048]{1,0:T(8,128)(2,1)}, bf16[304,2048]{1,0:T(8,128)(2,1)S(1)}, u32[]{:S(2)}) copy-start(bf16[304,2048]{1,0:T(8,128)(2,1)S(1)} %collective-permute-done.8.refs_6_) | copy-start | bytes 3735556
  69.2 8.2 %copy-start.9 = (bf16[304,2048]{1,0:T(8,128)(2,1)}, bf16[304,2048]{1,0:T(8,128)(2,1)S(1)}, u32[]{:S(2)}) copy-start(bf16[304,2048]{1,0:T(8,128)(2,1)S(1)} %collective-permute-done.9.refs_3_) | copy-start | bytes 3735556
  69.2 30.3 %collective-permute-start.14 = (bf16[304,2048]{1,0:T(8,128)(2,1)S(1)}, bf16[304,2048]{1,0:T(8,128)(2,1)S(1)}, u32[]{:S(2)}, u32[]{:S(2)}) collective-permute-start(bf16[304,2048]{1,0:T(8,128)(2,1)S(1)} %collective-permute-done.7.refs_4_), channel_id=1, source_target_pairs={{0,1},{1,0},{2,3},{3,2},{4,5},{5,4},{6,7},{7,6},{8,9},{9,8},{10,11... | collective-permute-start | bytes 3735560 | tf_op jit(solution)/shard_map/ppermute | solution.py:352
  69.3 34.6 %collective-permute-start.16 = (bf16[304,2048]{1,0:T(8,128)(2,1)S(1)}, bf16[304,2048]{1,0:T(8,128)(2,1)}, u32[]{:S(2)}, u32[]{:S(2)}) collective-permute-start(bf16[304,2048]{1,0:T(8,128)(2,1)S(1)} %collective-permute-done.7.refs_4_), channel_id=1, source_target_pairs={{0,2},{2,4},{4,6},{6,0},{1,3},{3,5},{5,7},{7,1},{8,10},{10,12},{12... | collective-permute-start | bytes 3735560 | tf_op jit(solution)/shard_map/ppermute | solution.py:356
  70.2 29.3 %collective-permute-start.15 = (bf16[304,2048]{1,0:T(8,128)(2,1)S(1)}, bf16[304,2048]{1,0:T(8,128)(2,1)S(1)}, u32[]{:S(2)}, u32[]{:S(2)}) collective-permute-start(bf16[304,2048]{1,0:T(8,128)(2,1)S(1)} %collective-permute-done.8.refs_6_), channel_id=1, source_target_pairs={{0,1},{1,0},{2,3},{3,2},{4,5},{5,4},{6,7},{7,6},{8,9},{9,8},{10,11... | collective-permute-start | bytes 3735560 | tf_op jit(solution)/shard_map/ppermute | solution.py:352
  86.9 12.5 %collective-permute-start.12 = (bf16[768,128]{1,0:T(8,128)(2,1)S(1)}, bf16[768,128]{1,0:T(8,128)(2,1)S(1)}, u32[]{:S(2)}, u32[]{:S(2)}) collective-permute-start(bf16[768,128]{1,0:T(8,128)(2,1)S(1)} %slice.6), channel_id=1, source_target_pairs={{0,32},{32,64},{64,96},{96,128},{128,160},{160,192},{192,224},{224... | collective-permute-start | bytes 589832 | tf_op jit(solution)/shard_map/ppermute | solution.py:356
  88.4 11.0 %collective-permute-start.13 = (bf16[768,128]{1,0:T(8,128)(2,1)S(1)}, bf16[768,128]{1,0:T(8,128)(2,1)S(1)}, u32[]{:S(2)}, u32[]{:S(2)}) collective-permute-start(bf16[768,128]{1,0:T(8,128)(2,1)S(1)} %slice.7), channel_id=1, source_target_pairs={{0,224},{32,0},{64,32},{96,64},{128,96},{160,128},{192,160},{224,1... | collective-permute-start | bytes 589832 | tf_op jit(solution)/shard_map/ppermute | solution.py:356
  99.5 2.2 %copy-start.10 = (bf16[304,2048]{1,0:T(8,128)(2,1)}, bf16[304,2048]{1,0:T(8,128)(2,1)S(1)}, u32[]{:S(2)}) copy-start(bf16[304,2048]{1,0:T(8,128)(2,1)S(1)} %collective-permute-done.14.refs_5_) | copy-start | bytes 3735556
  99.5 2.2 %copy-start.11 = (bf16[304,2048]{1,0:T(8,128)(2,1)}, bf16[304,2048]{1,0:T(8,128)(2,1)S(1)}, u32[]{:S(2)}) copy-start(bf16[304,2048]{1,0:T(8,128)(2,1)S(1)} %collective-permute-done.15.refs_7_) | copy-start | bytes 3735556
  101.6 2.8 %copy-start.5 = (f32[128]{0:T(128)S(1)}, f32[128]{0:T(128)}, u32[]{:S(2)}) copy-start(f32[128]{0:T(128)} %param.16) | copy-start | bytes 1540
  101.6 2.8 %collective-permute-start.17 = (f32[144,1536]{1,0:T(8,128)S(1)}, f32[144,1536]{1,0:T(8,128)S(1)}, u32[]{:S(2)}, u32[]{:S(2)}) collective-permute-start(f32[144,1536]{1,0:T(8,128)S(1)} %attend.11), channel_id=1, source_target_pairs={{0,1},{1,0},{2,3},{3,2},{4,5},{5,4},{6,7},{7,6},{8,9},{9,8},{10,11... | collective-permute-start | bytes 2654216 | tf_op jit(solution)/shard_map/ppermute | solution.py:352
  103.9 21.5 %collective-permute-start.18 = (bf16[304,2048]{1,0:T(8,128)(2,1)}, bf16[304,2048]{1,0:T(8,128)(2,1)}, u32[]{:S(2)}, u32[]{:S(2)}) collective-permute-start(bf16[304,2048]{1,0:T(8,128)(2,1)} %collective-permute-done.16.refs_8_), channel_id=1, source_target_pairs={{0,1},{1,0},{2,3},{3,2},{4,5},{5,4},{6,7},{7,6},{8,9},{9,8},{10,11... | collective-permute-start | bytes 3735560 | tf_op jit(solution)/shard_map/ppermute | solution.py:352
  106.3 18.0 %all-to-all-start.1 = ((bf16[16,192,128]{2,1,0:T(8,128)(2,1)}), bf16[16,192,128]{2,1,0:T(8,128)(2,1)S(1)}, u32[]{:S(2)}, u32[]{:S(2)}) async-start(bf16[16,192,128]{2,1,0:T(8,128)(2,1)} %bitcast.4), calls=%async_computation.1 | async-start | bytes 1572864 | tf_op jit(solution)/shard_map/all_to_all | solution.py:360
  124.2 1.2 copy-start.6
  138.5 13.2 %copy-start.12 = (f32[48,2048]{1,0:T(8,128)S(1)}, f32[48,2048]{1,0:T(8,128)}, u32[]{:S(2)}) copy-start(f32[48,2048]{1,0:T(8,128)} %get-tuple-element.101) | copy-start | bytes 1179652
  138.6 9.6 %collective-permute-start.19 = (bf16[48,2048]{1,0:T(8,128)(2,1)}, bf16[48,2048]{1,0:T(8,128)(2,1)S(1)}, u32[]{:S(2)}, u32[]{:S(2)}) collective-permute-start(bf16[48,2048]{1,0:T(8,128)(2,1)} %get-tuple-element.98), channel_id=1, source_target_pairs={{0,4},{2,6},{4,0},{6,2},{1,5},{3,7},{5,1},{7,3},{8,12},{10,14},{12... | collective-permute-start | bytes 589832 | tf_op jit(solution)/shard_map/ppermute | solution.py:356
  141.1 10.6 %collective-permute-start.20 = (bf16[48,2048]{1,0:T(8,128)(2,1)}, bf16[48,2048]{1,0:T(8,128)(2,1)S(1)}, u32[]{:S(2)}, u32[]{:S(2)}) collective-permute-start(bf16[48,2048]{1,0:T(8,128)(2,1)} %get-tuple-element.99), channel_id=1, source_target_pairs={{0,2},{2,4},{4,6},{6,0},{1,3},{3,5},{5,7},{7,1},{8,10},{10,12},{12... | collective-permute-start | bytes 589832 | tf_op jit(solution)/shard_map/ppermute | solution.py:356
  141.3 10.3 %collective-permute-start.21 = (bf16[48,2048]{1,0:T(8,128)(2,1)}, bf16[48,2048]{1,0:T(8,128)(2,1)S(1)}, u32[]{:S(2)}, u32[]{:S(2)}) collective-permute-start(bf16[48,2048]{1,0:T(8,128)(2,1)} %get-tuple-element.100), channel_id=1, source_target_pairs={{0,6},{2,0},{4,2},{6,4},{1,7},{3,1},{5,3},{7,5},{8,14},{10,8},{12,... | collective-permute-start | bytes 589832 | tf_op jit(solution)/shard_map/ppermute | solution.py:356
Sparse Core Ops, SparseCore 0:
  10.1 115.3 all-gather.2
